TPU v7x, 32 devices: a whole 2x2x4 slice. The times are simulated.
32 devices in a mesh: ra: 4 (over y, x), cb: 8 (over z, core).
Axes of the slice: x: 2, y: 2, z: 4, core: 2. Of those that a mesh axis runs over, the one named last changes fastest.
Arguments:
- tokens: bfloat16 [256, 4096], P(None, 'ra'), may hold values from -20 to 20, as said below
- norm_gain: float32 [2, 4096], P(None, 'ra'), may hold values from 0.1 to 1.9
- gate_weight: bfloat16 [2, 4096, 11008], P(None, 'ra', 'cb'), may hold values from -0.09375 to 0.09375
- value_weight: bfloat16 [2, 4096, 11008], P(None, 'ra', 'cb'), may hold values from -0.09375 to 0.09375
- gate_taps: float32 [2, 3, 11008], P(None, None, 'cb'), may hold values from -3.5 to 3.5
- value_taps: float32 [2, 3, 11008], P(None, None, 'cb'), may hold values from -3.5 to 3.5
- down_weight: bfloat16 [2, 11008, 4096], P(None, 'cb', 'ra'), may hold values from -0.0546875 to 0.0546875
Outputs:
- mixed: bfloat16 [256, 4096], P(None, 'ra')
Inputs may be any that keep to these rules, and one draw needn't show every extreme that they name: tokens have features drawn around zero with a scale that varies by blocks of features between about 0.3 and 3.3.
All inputs are finite; a program needn't handle non-finite values.
Results may differ from a plain program's by a relative error of at most 0.0075.
Values may be sent and summed in bfloat16 or wider, within the bound.
No kernel may reach another device: no remote copies, remote signals or barrier semaphores. Data moves between devices by JAX's collectives and lax.ppermute only.
A program may use at most 128 MiB of HBM per device.

v0:
```python
import jax
import jax.numpy as jnp
from jax import lax
from jax.sharding import PartitionSpec as P

D = 4096


epsilon = 1e-06


def conv_after(signal, earlier, kernel_taps):
    length = signal.shape[0]
    width = kernel_taps.shape[0]
    padded = jnp.concatenate([earlier, signal], axis=0)
    result = jnp.zeros(signal.shape, jnp.float32)
    for offset in range(width):
        result = result + kernel_taps[offset] * padded[offset : offset + length]
    return result


def causal_conv(signal, kernel_taps):
    width = kernel_taps.shape[0]
    return conv_after(signal, jnp.zeros((width - 1, signal.shape[1]), jnp.float32), kernel_taps)


def body(tokens, norm_gain, gate_weight, value_weight, gate_taps, value_taps, down_weight):
    stream = tokens
    for layer_index in range(gate_weight.shape[0]):
        current = stream.astype(jnp.float32)
        local_squares = jnp.sum(current * current, axis=1, keepdims=True)
        scaled = (current * norm_gain[layer_index]).astype(jnp.bfloat16)
        gate_part = jnp.dot(scaled, gate_weight[layer_index], preferred_element_type=jnp.float32)
        value_part = jnp.dot(scaled, value_weight[layer_index], preferred_element_type=jnp.float32)
        total_squares = lax.psum(local_squares, "ra")
        gate_sum, value_sum = lax.psum((gate_part, value_part), "ra")
        inverse_rms = lax.rsqrt(total_squares / D + epsilon)
        gate_conv = causal_conv(gate_sum * inverse_rms, gate_taps[layer_index])
        value_conv = causal_conv(value_sum * inverse_rms, value_taps[layer_index])
        hidden = (jax.nn.silu(gate_conv) * value_conv).astype(jnp.bfloat16)
        partial_branch = jnp.dot(
            hidden, down_weight[layer_index], preferred_element_type=jnp.float32
        )
        branch = lax.psum(partial_branch, "cb")
        stream = (0.5 * current + branch).astype(jnp.bfloat16)
    return stream


def solution(mesh):
    return jax.shard_map(
        body,
        mesh=mesh,
        in_specs=(
            P(None, "ra"),
            P(None, "ra"),
            P(None, "ra", "cb"),
            P(None, "ra", "cb"),
            P(None, None, "cb"),
            P(None, None, "cb"),
            P(None, "cb", "ra"),
        ),
        out_specs=P(None, "ra"),
        check_vma=False,
    )
```

profile of v0, /device:TPU:0, one launch (start us, length us, event | category | flops | bytes accessed | tf_op | source)
XLA Modules:
  0.0 333.7 jit_solution(11090075387825171046)
XLA Ops:
  6.5 0.0 all-reduce.17.cloned.1.call-start
  6.5 0.8 fusion.57
  7.3 0.0 copy-start
  7.3 4.0 %fusion.8 = f32[256,1376]{0,1:T(8,128)} fusion(bf16[2,1024,1376]{1,2,0:T(8,128)(2,1)} %param.10, bf16[256,1024]{1,0:T(8,128)(2,1)} %param.7, f32[1024]{0:T(1024)S(1)} %bitcast.30), kind=kOutput, calls=%fused_computation.8 | convolution fusion | flops 722206720 | bytes 4755456 | tf_op jit(solution)/shard_map/dot_general | solution.py:34
  11.4 0.0 copy-done
  11.4 3.8 %fusion.10 = f32[256,1376]{0,1:T(8,128)} fusion(bf16[2,1024,1376]{1,2,0:T(8,128)(2,1)} %param.9, bf16[256,1024]{1,0:T(8,128)(2,1)S(1)} %copy-done, f32[1024]{0:T(1024)S(1)} %bitcast.31), kind=kOutput, calls=%fused_computation.10 | convolution fusion | flops 722206720 | bytes 4755456 | tf_op jit(solution)/shard_map/dot_general | solution.py:33
  15.2 0.0 copy-start.1
  15.2 0.0 all-reduce.17.cloned.1.call-update
  15.2 0.0 all-reduce.11.cloned.1.call-start
  15.3 0.2 fusion.41
  15.5 11.5 %psum.57 = f32[256,1]{0,1:T(1,128)S(1)} all-reduce(f32[256,1]{0,1:T(1,128)S(1)} %bitcast.27), channel_id=1, replica_groups=mesh['ra'=4,'cb'=8] {'ra'}, use_global_device_ids=true, to_apply=%region_2.0 | all-reduce | flops 256 | bytes 2048 | tf_op jit(solution)/shard_map/psum | solution.py:35
  27.0 0.0 copy-done.1
  27.0 0.0 copy-done.2
  27.0 0.2 slice_reduce_fusion.2
  27.1 72.5 %all-reduce.17.cloned.1.call-done = (f32[256,1376]{0,1:T(8,128)}, f32[256,1376]{0,1:T(8,128)}) async-done(((f32[256,1376]{0,1:T(8,128)}, f32[256,1376]{0,1:T(8,128)}), (f32[256,1376]{0,1:T(8,128)}, f32[256,1376]{0,1:T(8,128)})) %all-reduce.17.cloned.1.call-update) | async-done | bytes 2818064 | tf_op jit(solution)/shard_map/psum | solution.py:36
  99.6 2.0 broadcast_multiply_fusion.3
  101.6 6.3 %fusion.6 = f32[256,1024]{1,0:T(8,128)} fusion(bf16[2,1376,1024]{2,1,0:T(8,128)(2,1)} %param.13, f32[256,1376]{0,1:T(8,128)S(1)} %get-tuple-element.28, f32[256,1376]{0,1:T(8,128)S(1)} %get-tuple-element.27, f32[1376]{0:T(1024)S(1)} %get-tuple-element.12, f32[1376]{0:T(1024)S(1)} %get-tuple-element.13, f32[1376]{0:T(1024)S(1)} %get-tuple-element.14, ...), kind=kOutput, calls=%fused_computation.6 | convolution fusion | flops 727056384 | bytes 6717696 | tf_op jit(solution)/shard_map/dot_general | solution.py:41
  107.9 0.0 all-reduce.11.cloned.1.call-update
  107.9 0.0 all-reduce.15.cloned.1.call-start
  107.9 59.4 %all-reduce.11.cloned.1.call-done = f32[256,1024]{1,0:T(8,128)} async-done(((f32[256,1024]{1,0:T(8,128)}), f32[256,1024]{1,0:T(8,128)}) %all-reduce.11.cloned.1.call-update) | async-done | bytes 1048592 | tf_op jit(solution)/shard_map/psum | solution.py:44
  167.3 1.5 fusion.45
  168.8 3.8 %fusion.4 = f32[256,1376]{0,1:T(8,128)} fusion(bf16[2,1024,1376]{1,2,0:T(8,128)(2,1)} %param.9, bf16[256,1024]{1,0:T(8,128)(2,1)S(1)} %get-tuple-element.22, f32[1024]{0:T(1024)S(1)} %bitcast.28), kind=kOutput, calls=%fused_computation.4 | convolution fusion | flops 722206720 | bytes 4755456 | tf_op jit(solution)/shard_map/dot_general | solution.py:33
  172.6 3.8 %fusion.2 = f32[256,1376]{0,1:T(8,128)} fusion(bf16[2,1024,1376]{1,2,0:T(8,128)(2,1)} %param.10, bf16[256,1024]{1,0:T(8,128)(2,1)S(1)} %get-tuple-element.22, f32[1024]{0:T(1024)S(1)} %bitcast.29), kind=kOutput, calls=%fused_computation.2 | convolution fusion | flops 722206720 | bytes 4755456 | tf_op jit(solution)/shard_map/dot_general | solution.py:34
  176.5 0.0 all-reduce.15.cloned.1.call-update
  176.5 0.0 all-reduce.13.cloned.1.call-start
  176.5 10.1 %psum.61 = f32[256,1]{0,1:T(1,128)S(1)} all-reduce(f32[256,1]{0,1:T(1,128)S(1)} %bitcast.24), channel_id=1, replica_groups=mesh['ra'=4,'cb'=8] {'ra'}, use_global_device_ids=true, to_apply=%region_7.8 | all-reduce | flops 256 | bytes 2048 | tf_op jit(solution)/shard_map/psum | solution.py:35
  186.6 70.6 %all-reduce.15.cloned.1.call-done = (f32[256,1376]{0,1:T(8,128)}, f32[256,1376]{0,1:T(8,128)}) async-done(((f32[256,1376]{0,1:T(8,128)}, f32[256,1376]{0,1:T(8,128)}), (f32[256,1376]{0,1:T(8,128)}, f32[256,1376]{0,1:T(8,128)})) %all-reduce.15.cloned.1.call-update) | async-done | bytes 2818064 | tf_op jit(solution)/shard_map/psum | solution.py:36
  257.3 2.0 broadcast_multiply_fusion.1
  259.2 6.3 %fusion = f32[256,1024]{1,0:T(8,128)} fusion(bf16[2,1376,1024]{2,1,0:T(8,128)(2,1)} %param.13, f32[256,1376]{0,1:T(8,128)S(1)} %get-tuple-element.26, f32[256,1376]{0,1:T(8,128)S(1)} %get-tuple-element.25, f32[1376]{0:T(1024)S(1)} %get-tuple-element.15, f32[1376]{0:T(1024)S(1)} %get-tuple-element.16, f32[1376]{0:T(1024)S(1)} %get-tuple-element.11, ...), kind=kOutput, calls=%fused_computation | convolution fusion | flops 727056384 | bytes 6717696 | tf_op jit(solution)/shard_map/dot_general | solution.py:41
  265.5 0.0 all-reduce.13.cloned.1.call-update
  265.5 59.4 %all-reduce.13.cloned.1.call-done = f32[256,1024]{1,0:T(8,128)} async-done(((f32[256,1024]{1,0:T(8,128)}), f32[256,1024]{1,0:T(8,128)}) %all-reduce.13.cloned.1.call-update) | async-done | bytes 1048592 | tf_op jit(solution)/shard_map/psum | solution.py:44
  324.9 2.2 fusion.43
  (3 shorter events, 0.0 us)
Async XLA Ops:
  6.5 93.1 %all-reduce.17.cloned.1.call-start = ((), (), s32[]{:S(2)}) async-start(), calls=%async_computation.3 | async-start | bytes 5636096 | tf_op jit(solution)/shard_map/psum | solution.py:36
  7.3 4.0 %copy-start = (bf16[256,1024]{1,0:T(8,128)(2,1)S(1)}, bf16[256,1024]{1,0:T(8,128)(2,1)}, u32[]{:S(2)}) copy-start(bf16[256,1024]{1,0:T(8,128)(2,1)} %param.7) | copy-start | bytes 1572868
  15.2 11.8 %copy-start.1 = (f32[2,3,1376]{2,0,1:T(2,128)S(1)}, f32[2,3,1376]{2,0,1:T(2,128)}, u32[]{:S(2)}) copy-start(f32[2,3,1376]{2,0,1:T(2,128)} %param.12) | copy-start | bytes 99076
  15.2 11.8 %copy-start.2 = (f32[2,3,1376]{2,0,1:T(2,128)S(1)}, f32[2,3,1376]{2,0,1:T(2,128)}, u32[]{:S(2)}) copy-start(f32[2,3,1376]{2,0,1:T(2,128)} %param.11) | copy-start | bytes 99076
  15.2 152.1 %all-reduce.11.cloned.1.call-start = ((), (), s32[]{:S(2)}) async-start(), calls=%async_computation | async-start | bytes 2097152 | tf_op jit(solution)/shard_map/psum | solution.py:44
  107.9 149.4 %all-reduce.15.cloned.1.call-start = ((), (), s32[]{:S(2)}) async-start(), calls=%async_computation.2 | async-start | bytes 5636096 | tf_op jit(solution)/shard_map/psum | solution.py:36
  176.5 148.4 %all-reduce.13.cloned.1.call-start = ((), (), s32[]{:S(2)}) async-start(), calls=%async_computation.1 | async-start | bytes 2097152 | tf_op jit(solution)/shard_map/psum | solution.py:44
Sparse Core Ops, SparseCore 0:
  15.3 84.2 all-reduce.16
  108.0 59.2 all-reduce.10
  176.6 80.6 all-reduce.14
  265.6 59.2 all-reduce.12
where the time goes:
time: 334 us
  waiting for transfers between devices  262 us (78%)
  matrix products  28 us (8%)
  blocking collectives  21.6 us (6%)
  between operations  13.2 us (4%)
  other arithmetic  7.81 us (2%)
    psum x2, waiting for transfers between devices, body(): gate_sum, value_sum = lax.psum((gate_part, value_part), 'ra')  143 us
    psum x2, waiting for transfers between devices, body(): branch = lax.psum(partial_branch, 'cb')  119 us
    psum x2, blocking collectives, body(): total_squares = lax.psum(local_squares, 'ra')  21.6 us
    dot_general x2, matrix products, body(): jnp.dot(hidden, down_weight[layer_index], preferred_element_type=jnp.floa...  12.5 us
    dot_general x2, matrix products, body(): jnp.dot(scaled, value_weight[layer_index], preferred_element_type=jnp.flo...  7.86 us
    dot_general x2, matrix products, body(): jnp.dot(scaled, gate_weight[layer_index], preferred_element_type=jnp.floa...  7.65 us
  transfers between devices with their start and end apart: 4, of which 4 were waited for; matrix products, arithmetic and copies ran while one was open for 0% of the time, Pallas kernels for 0%

commit v1 on v0

v1 whole, which is shorter than its diff:
```python
import jax
import jax.numpy as jnp
from jax import lax
from jax.sharding import PartitionSpec as P

epsilon = 1e-06
F32 = jnp.float32
BF16 = jnp.bfloat16


def conv_lanes(signal, taps):
    width = taps.shape[0]
    length = signal.shape[1]
    padded = jnp.pad(signal, ((0, 0), (width - 1, 0)))
    result = jnp.zeros(signal.shape, F32)
    for offset in range(width):
        result = result + taps[offset][:, None] * padded[:, offset : offset + length]
    return result


def make_body(mesh):
    n_a = mesh.shape["ra"]
    n_c = mesh.shape["cb"]
    n_z = n_c // 2

    def peer(i, s, n):
        return i ^ s if n & (n - 1) == 0 else (i + s) % n

    def source(i, s, n):
        return i ^ s if n & (n - 1) == 0 else (i - s) % n

    def send_a(value, s):
        return lax.ppermute(value, "ra", [(i, peer(i, s, n_a)) for i in range(n_a)])

    def send_z(value, s):
        pairs = [(z * 2 + k, peer(z, s, n_z) * 2 + k) for z in range(n_z) for k in range(2)]
        return lax.ppermute(value, "cb", pairs)

    def send_core(value):
        return lax.ppermute(value, "cb", [(i, i ^ 1) for i in range(n_c)])

    def body(tokens, norm_gain, gate_weight, value_weight, gate_taps, value_taps, down_weight):
        layers, width, units = gate_weight.shape
        positions = tokens.shape[0]
        total_width = width * n_a
        piece = -(-(-(-units // n_a)) // 8) * 8
        a = lax.axis_index("ra")
        c = lax.axis_index("cb")
        z, core = c // 2, c % 2
        half = positions // 2
        span = half // n_z

        def start(p):
            return jnp.minimum(p * piece, units - piece)

        stream = tokens
        for layer in range(layers):
            current = stream.astype(F32)
            squares = jnp.sum(current * current, axis=1)[None, :]
            scaled = (current * norm_gain[layer]).astype(BF16)
            total = squares
            for s in range(1, n_a):
                total = total + send_a(squares, s)
            contract = (((0,), (1,)), ((), ()))
            gate = lax.dot_general(gate_weight[layer], scaled, contract, preferred_element_type=F32)
            value = lax.dot_general(value_weight[layer], scaled, contract, preferred_element_type=F32)

            def cut(p):
                return jnp.stack(
                    [
                        lax.dynamic_slice_in_dim(gate, start(p), piece, 0),
                        lax.dynamic_slice_in_dim(value, start(p), piece, 0),
                    ]
                )

            both = cut(a)
            for s in range(1, n_a):
                both = both + send_a(cut(peer(a, s, n_a)).astype(BF16), s).astype(F32)
            both = both * lax.rsqrt(total / total_width + epsilon)
            my = start(a)
            g_taps = lax.dynamic_slice_in_dim(gate_taps[layer], my, piece, 1)
            v_taps = lax.dynamic_slice_in_dim(value_taps[layer], my, piece, 1)
            gate_conv = conv_lanes(both[0], g_taps)
            value_conv = conv_lanes(both[1], v_taps)
            mine = (jax.nn.silu(gate_conv) * value_conv).astype(BF16)
            hidden = jnp.zeros((units, positions), BF16)
            hidden = lax.dynamic_update_slice_in_dim(hidden, mine, my, 0)
            for s in range(1, n_a):
                other = send_a(mine, s)
                hidden = lax.dynamic_update_slice_in_dim(
                    hidden, other, start(source(a, s, n_a)), 0
                )
            partial = lax.dot_general(
                hidden,
                down_weight[layer],
                (((0,), (0,)), ((), ())),
                preferred_element_type=F32,
            )
            away = lax.dynamic_slice_in_dim(partial, (1 - core) * half, half, 0).astype(BF16)
            kept = lax.dynamic_slice_in_dim(partial, core * half, half, 0)
            kept = kept + send_core(away).astype(F32)
            branch = lax.dynamic_slice_in_dim(kept, z * span, span, 0)
            for s in range(1, n_z):
                out = lax.dynamic_slice_in_dim(kept, peer(z, s, n_z) * span, span, 0)
                branch = branch + send_z(out.astype(BF16), s).astype(F32)
            old = lax.dynamic_slice_in_dim(stream, core * half + z * span, span, 0)
            fresh = (0.5 * old.astype(F32) + branch).astype(BF16)
            mid = jnp.zeros((half, width), BF16)
            mid = lax.dynamic_update_slice_in_dim(mid, fresh, z * span, 0)
            for s in range(1, n_z):
                mid = lax.dynamic_update_slice_in_dim(
                    mid, send_z(fresh, s), source(z, s, n_z) * span, 0
                )
            far = send_core(mid)
            stream = jnp.where(
                core == 0,
                jnp.concatenate([mid, far], axis=0),
                jnp.concatenate([far, mid], axis=0),
            )
        return stream

    return body


def solution(mesh):
    return jax.shard_map(
        make_body(mesh),
        mesh=mesh,
        in_specs=(
            P(None, "ra"),
            P(None, "ra"),
            P(None, "ra", "cb"),
            P(None, "ra", "cb"),
            P(None, None, "cb"),
            P(None, None, "cb"),
            P(None, "cb", "ra"),
        ),
        out_specs=P(None, "ra"),
        check_vma=False,
    )
```

time: 334 us -> 137 us (0.41)
  waiting for transfers between devices: 262 us -> 56.2 us
  starting transfers between devices: 0.13 us -> 40.5 us
  blocking collectives: 21.6 us -> 0 us
  local copies, waits for them, and re-layouts: 0.97 us -> 13.8 us
  between operations: 13.2 us -> 0.55 us
  matrix products: 28 us -> 16.8 us
    psum x4 -> x0, waiting for transfers between devices: 262 us -> none  [the longest x2 143 us: body(): gate_sum, value_sum = lax.psum((gate_part, value_part), 'ra')]
    ppermute x0 -> x34, waiting for transfers between devices: none -> 56.2 us  [the longest x18 31.7 us: send_a(): return lax.ppermute(value, 'ra', [(i, peer(i, s, n_a)) for i in range(n_a)])]
    ppermute x0 -> x34, starting transfers between devices: none -> 40.5 us  [the longest x18 22.5 us: send_a(): return lax.ppermute(value, 'ra', [(i, peer(i, s, n_a)) for i in range(n_a)])]
    psum x2 -> x0, blocking collectives: 21.6 us -> none  [body(): total_squares = lax.psum(local_squares, 'ra')]
    dot_general x6, matrix products: 28 us -> 16.8 us  [the longest x2 5.7 us: body(): lax.dot_general(gate_weight[layer], scaled, contract, preferred_element_t...]
    dynamic_update_slice x0 -> x14, local copies, waits for them, and re-layouts: none -> 10.5 us  [the longest x6 7.55 us: body(): lax.dynamic_update_slice_in_dim(hidden, other, start(source(a, s, n_a)), 0)]
  transfers between devices with their start and end apart: 4 -> 34, of which waited for: 4 -> 22; matrix products, arithmetic and copies ran while one was open for 0% -> 18% of each run, Pallas kernels for 0% -> 0%
where the time goes in v1:
time: 137 us; the launch traced here: 136 us
  waiting for transfers between devices  56.2 us (41%)
  starting transfers between devices  40.5 us (30%)
  matrix products  16.8 us (12%)
  local copies, waits for them, and re-layouts  13.8 us (10%)
  other arithmetic  8.25 us (6%)
    ppermute x18, waiting for transfers between devices, send_a(): return lax.ppermute(value, 'ra', [(i, peer(i, s, n_a)) for i in range(n_a)])  31.7 us
    ppermute x18, starting transfers between devices, send_a(): return lax.ppermute(value, 'ra', [(i, peer(i, s, n_a)) for i in range(n_a)])  22.5 us
    ppermute x12, waiting for transfers between devices, send_z(): return lax.ppermute(value, 'cb', pairs)  18.6 us
    ppermute x12, starting transfers between devices, send_z(): return lax.ppermute(value, 'cb', pairs)  17.8 us
    dynamic_update_slice x6, local copies, waits for them, and re-layouts, body(): lax.dynamic_update_slice_in_dim(hidden, other, start(source(a, s, n_a)), 0)  7.55 us
    ppermute x4, waiting for transfers between devices, send_core(): return lax.ppermute(value, 'cb', [(i, i ^ 1) for i in range(n_c)])  5.92 us
    dot_general x2, matrix products, body(): lax.dot_general(gate_weight[layer], scaled, contract, preferred_element_t...  5.7 us
    dot_general x2, matrix products, body(): lax.dot_general(hidden, down_weight[layer], (((0,), (0,)), ((), ())), pre...  5.61 us
  transfers between devices with their start and end apart: 34, of which 22 were waited for; matrix products, arithmetic and copies ran while one was open for 18% of the time, Pallas kernels for 0%

profile of v1, /device:TPU:0, one launch (start us, length us, event | category | flops | bytes accessed | tf_op | source)
XLA Modules:
  0.0 136.1 jit_solution(16192635222827049202)
XLA Ops:
  1.2 3.0 %collective-permute-start.3 = (f32[1,256]{1,0:T(1,128)S(1)}, f32[1,256]{1,0:T(1,128)S(1)}, u32[]{:S(2)}, u32[]{:S(2)}) collective-permute-start(f32[1,256]{1,0:T(1,128)S(1)} %bitcast.98), channel_id=1, source_target_pairs={{0,8},{8,0},{16,24},{24,16},{1,9},{9,1},{17,25},{25,17},{2,10},{10... | collective-permute-start | bytes 3080 | tf_op jit(solution)/shard_map/ppermute | solution.py:33
  6.6 3.0 %fusion.10 = f32[256,1376]{0,1:T(8,128)S(1)} fusion(bf16[2,1024,1376]{1,2,0:T(8,128)(2,1)} %param.9, bf16[256,1024]{1,0:T(8,128)(2,1)} %param.7, f32[1024]{0:T(1024)S(1)} %bitcast.110), kind=kOutput, calls=%fused_computation.10 | convolution fusion | flops 722206720 | bytes 4755456 | tf_op jit(solution)/shard_map/dot_general | solution.py:65
  9.5 2.7 %fusion.8 = f32[256,1376]{0,1:T(8,128)S(1)} fusion(bf16[2,1024,1376]{1,2,0:T(8,128)(2,1)} %param.10, bf16[256,1024]{1,0:T(8,128)(2,1)S(1)} %copy-done, f32[1024]{0:T(1024)S(1)} %bitcast.111), kind=kOutput, calls=%fused_computation.8 | convolution fusion | flops 722206720 | bytes 4755456 | tf_op jit(solution)/shard_map/dot_general | solution.py:66
  15.7 2.9 %collective-permute-start.2 = (bf16[2,344,256]{2,1,0:T(8,128)(2,1)}, bf16[2,344,256]{2,1,0:T(8,128)(2,1)}, u32[]{:S(2)}, u32[]{:S(2)}) collective-permute-start(bf16[2,344,256]{2,1,0:T(8,128)(2,1)} %pad_maximum_fusion.2), channel_id=1, source_target_pairs={{0,24},{8,16},{16,8},{24,0},{1,25},{9,17},{17,9},{25,1},{2,26},{10... | collective-permute-start | bytes 1056776 | tf_op jit(solution)/shard_map/ppermute | solution.py:33
  20.1 10.8 %collective-permute-done.5 = f32[1,256]{1,0:T(1,128)S(1)} collective-permute-done((f32[1,256]{1,0:T(1,128)S(1)}, f32[1,256]{1,0:T(1,128)S(1)}, u32[]{:S(2)}, u32[]{:S(2)}) %collective-permute-start.5) | collective-permute-done | bytes 1056 | tf_op jit(solution)/shard_map/ppermute | solution.py:33
  34.1 1.6 %collective-permute-start.6 = (bf16[344,256]{1,0:T(8,128)(2,1)S(1)}, bf16[344,256]{1,0:T(8,128)(2,1)S(1)}, u32[]{:S(2)}, u32[]{:S(2)}) collective-permute-start(bf16[344,256]{1,0:T(8,128)(2,1)S(1)} %fusion.40), channel_id=1, source_target_pairs={{0,8},{8,0},{16,24},{24,16},{1,9},{9,1},{17,25},{25,17},{2,10},{10... | collective-permute-start | bytes 528392 | tf_op jit(solution)/shard_map/ppermute | solution.py:33
  37.7 1.6 %dynamic_update_slice.48 = bf16[1376,256]{1,0:T(8,128)(2,1)S(1)} dynamic-update-slice(bf16[1376,256]{1,0:T(8,128)(2,1)S(1)} %broadcast.32.clone, bf16[344,256]{1,0:T(8,128)(2,1)S(1)} %fusion.40, s32[]{:T(128)S(6)} %select_n.49, s32[]{:T(128)} %constant.52.clone.1) | dynamic-update-slice | bytes 352260 | tf_op jit(solution)/shard_map/dynamic_update_slice | solution.py:87
  39.2 1.8 %collective-permute-done.6 = bf16[344,256]{1,0:T(8,128)(2,1)S(1)} collective-permute-done((bf16[344,256]{1,0:T(8,128)(2,1)S(1)}, bf16[344,256]{1,0:T(8,128)(2,1)S(1)}, u32[]{:S(2)}, u32[]{:S(2)}) %collective-permute-start.6) | collective-permute-done | bytes 176160 | tf_op jit(solution)/shard_map/ppermute | solution.py:33
  46.1 2.8 %fusion.6 = f32[256,1024]{1,0:T(8,128)S(1)} fusion(bf16[1376,256]{1,0:T(8,128)(2,1)S(1)} %dynamic_update_slice.51, bf16[2,1376,1024]{2,1,0:T(8,128)(2,1)} %param.13), kind=kOutput, calls=%fused_computation.6 | convolution fusion | flops 721420288 | bytes 4571136 | tf_op jit(solution)/shard_map/dot_general | solution.py:93
  52.0 2.6 %collective-permute-start.11 = (bf16[32,1024]{1,0:T(8,128)(2,1)S(1)}, bf16[32,1024]{1,0:T(8,128)(2,1)S(1)}, u32[]{:S(2)}, u32[]{:S(2)}) collective-permute-start(bf16[32,1024]{1,0:T(8,128)(2,1)S(1)} %get-tuple-element.44), channel_id=1, source_target_pairs={{0,4},{1,5},{2,6},{3,7},{4,0},{5,1},{6,2},{7,3},{8,12},{9,13},{10,... | collective-permute-start | bytes 196616 | tf_op jit(solution)/shard_map/ppermute | solution.py:37
  55.1 4.5 %collective-permute-done.11 = bf16[32,1024]{1,0:T(8,128)(2,1)S(1)} collective-permute-done((bf16[32,1024]{1,0:T(8,128)(2,1)S(1)}, bf16[32,1024]{1,0:T(8,128)(2,1)S(1)}, u32[]{:S(2)}, u32[]{:S(2)}) %collective-permute-start.11) | collective-permute-done | bytes 65568 | tf_op jit(solution)/shard_map/ppermute | solution.py:37
  61.8 1.7 %collective-permute-start.14 = (bf16[32,1024]{1,0:T(8,128)(2,1)S(1)}, bf16[32,1024]{1,0:T(8,128)(2,1)S(1)}, u32[]{:S(2)}, u32[]{:S(2)}) collective-permute-start(bf16[32,1024]{1,0:T(8,128)(2,1)S(1)} %get-tuple-element.22), channel_id=1, source_target_pairs={{0,4},{1,5},{2,6},{3,7},{4,0},{5,1},{6,2},{7,3},{8,12},{9,13},{10,... | collective-permute-start | bytes 196616 | tf_op jit(solution)/shard_map/ppermute | solution.py:37
  63.5 1.8 %collective-permute-start.15 = (bf16[32,1024]{1,0:T(8,128)(2,1)S(1)}, bf16[32,1024]{1,0:T(8,128)(2,1)S(1)}, u32[]{:S(2)}, u32[]{:S(2)}) collective-permute-start(bf16[32,1024]{1,0:T(8,128)(2,1)S(1)} %get-tuple-element.22), channel_id=1, source_target_pairs={{0,6},{1,7},{2,4},{3,5},{4,2},{5,3},{6,0},{7,1},{8,14},{9,15},{10,... | collective-permute-start | bytes 196616 | tf_op jit(solution)/shard_map/ppermute | solution.py:37
  65.4 2.6 %collective-permute-done.14 = bf16[32,1024]{1,0:T(8,128)(2,1)S(1)} collective-permute-done((bf16[32,1024]{1,0:T(8,128)(2,1)S(1)}, bf16[32,1024]{1,0:T(8,128)(2,1)S(1)}, u32[]{:S(2)}, u32[]{:S(2)}) %collective-permute-start.14) | collective-permute-done | bytes 65568 | tf_op jit(solution)/shard_map/ppermute | solution.py:37
  68.0 1.5 %collective-permute-done.15 = bf16[32,1024]{1,0:T(8,128)(2,1)S(1)} collective-permute-done((bf16[32,1024]{1,0:T(8,128)(2,1)S(1)}, bf16[32,1024]{1,0:T(8,128)(2,1)S(1)}, u32[]{:S(2)}, u32[]{:S(2)}) %collective-permute-start.15) | collective-permute-done | bytes 65568 | tf_op jit(solution)/shard_map/ppermute | solution.py:37
  73.3 1.7 %collective-permute-start.22 = (f32[1,256]{1,0:T(1,128)S(1)}, f32[1,256]{1,0:T(1,128)S(1)}, u32[]{:S(2)}, u32[]{:S(2)}) collective-permute-start(f32[1,256]{1,0:T(1,128)S(1)} %bitcast.104), channel_id=1, source_target_pairs={{0,24},{8,16},{16,8},{24,0},{1,25},{9,17},{17,9},{25,1},{2,26},{10... | collective-permute-start | bytes 3080 | tf_op jit(solution)/shard_map/ppermute | solution.py:33
  75.0 2.7 %fusion.4 = f32[256,1376]{0,1:T(8,128)S(1)} fusion(bf16[2,1024,1376]{1,2,0:T(8,128)(2,1)} %param.9, bf16[256,1024]{1,0:T(8,128)(2,1)S(1)} %get-tuple-element.20, f32[1024]{0:T(1024)S(1)} %bitcast.108), kind=kOutput, calls=%fused_computation.4 | convolution fusion | flops 722206720 | bytes 4755456 | tf_op jit(solution)/shard_map/dot_general | solution.py:65
  77.7 2.7 %fusion.2 = f32[256,1376]{0,1:T(8,128)S(1)} fusion(bf16[2,1024,1376]{1,2,0:T(8,128)(2,1)} %param.10, bf16[256,1024]{1,0:T(8,128)(2,1)S(1)} %get-tuple-element.20, f32[1024]{0:T(1024)S(1)} %bitcast.109), kind=kOutput, calls=%fused_computation.2 | convolution fusion | flops 722206720 | bytes 4755456 | tf_op jit(solution)/shard_map/dot_general | solution.py:66
  82.8 1.7 %collective-permute-start.19 = (bf16[2,344,256]{2,1,0:T(8,128)(2,1)S(1)}, bf16[2,344,256]{2,1,0:T(8,128)(2,1)S(1)}, u32[]{:S(2)}, u32[]{:S(2)}) collective-permute-start(bf16[2,344,256]{2,1,0:T(8,128)(2,1)S(1)} %pad_maximum_fusion.5), channel_id=1, source_target_pairs={{0,24},{8,16},{16,8},{24,0},{1,25},{9,17},{17,9},{25,1},{2,26},{10... | collective-permute-start | bytes 1056776 | tf_op jit(solution)/shard_map/ppermute | solution.py:33
  84.6 7.3 %collective-permute-done.17 = bf16[2,344,256]{2,1,0:T(8,128)(2,1)S(1)} collective-permute-done((bf16[2,344,256]{2,1,0:T(8,128)(2,1)S(1)}, bf16[2,344,256]{2,1,0:T(8,128)(2,1)S(1)}, u32[]{:S(2)}, u32[]{:S(2)}) %collective-permute-start.17) | collective-permute-done | bytes 352288 | tf_op jit(solution)/shard_map/ppermute | solution.py:33
  91.9 6.3 %collective-permute-done.18 = bf16[2,344,256]{2,1,0:T(8,128)(2,1)S(1)} collective-permute-done((bf16[2,344,256]{2,1,0:T(8,128)(2,1)S(1)}, bf16[2,344,256]{2,1,0:T(8,128)(2,1)S(1)}, u32[]{:S(2)}, u32[]{:S(2)}) %collective-permute-start.18) | collective-permute-done | bytes 352288 | tf_op jit(solution)/shard_map/ppermute | solution.py:33
  101.0 1.8 %collective-permute-start.25 = (bf16[344,256]{1,0:T(8,128)(2,1)S(1)}, bf16[344,256]{1,0:T(8,128)(2,1)S(1)}, u32[]{:S(2)}, u32[]{:S(2)}) collective-permute-start(bf16[344,256]{1,0:T(8,128)(2,1)S(1)} %fusion.50), channel_id=1, source_target_pairs={{0,24},{8,16},{16,8},{24,0},{1,25},{9,17},{17,9},{25,1},{2,26},{10... | collective-permute-start | bytes 528392 | tf_op jit(solution)/shard_map/ppermute | solution.py:33
  104.2 1.7 %collective-permute-done.23 = bf16[344,256]{1,0:T(8,128)(2,1)S(1)} collective-permute-done((bf16[344,256]{1,0:T(8,128)(2,1)S(1)}, bf16[344,256]{1,0:T(8,128)(2,1)S(1)}, u32[]{:S(2)}, u32[]{:S(2)}) %collective-permute-start.23) | collective-permute-done | bytes 176160 | tf_op jit(solution)/shard_map/ppermute | solution.py:33
  107.2 1.6 %collective-permute-done.24 = bf16[344,256]{1,0:T(8,128)(2,1)S(1)} collective-permute-done((bf16[344,256]{1,0:T(8,128)(2,1)S(1)}, bf16[344,256]{1,0:T(8,128)(2,1)S(1)}, u32[]{:S(2)}, u32[]{:S(2)}) %collective-permute-start.24) | collective-permute-done | bytes 176160 | tf_op jit(solution)/shard_map/ppermute | solution.py:33
  111.2 2.8 %fusion = f32[256,1024]{1,0:T(8,128)S(1)} fusion(bf16[1376,256]{1,0:T(8,128)(2,1)S(1)} %dynamic_update_slice.59, bf16[2,1376,1024]{2,1,0:T(8,128)(2,1)} %param.13), kind=kOutput, calls=%fused_computation | convolution fusion | flops 721420288 | bytes 4571136 | tf_op jit(solution)/shard_map/dot_general | solution.py:93
  114.2 1.5 %collective-permute-done.26 = bf16[128,1024]{1,0:T(8,128)(2,1)S(1)} collective-permute-done((bf16[128,1024]{1,0:T(8,128)(2,1)S(1)}, bf16[128,1024]{1,0:T(8,128)(2,1)S(1)}, u32[]{:S(2)}, u32[]{:S(2)}) %collective-permute-start.26) | collective-permute-done | bytes 262176 | tf_op jit(solution)/shard_map/ppermute | solution.py:40
  115.9 2.5 %collective-permute-start.28 = (bf16[32,1024]{1,0:T(8,128)(2,1)S(1)}, bf16[32,1024]{1,0:T(8,128)(2,1)S(1)}, u32[]{:S(2)}, u32[]{:S(2)}) collective-permute-start(bf16[32,1024]{1,0:T(8,128)(2,1)S(1)} %get-tuple-element.41), channel_id=1, source_target_pairs={{0,4},{1,5},{2,6},{3,7},{4,0},{5,1},{6,2},{7,3},{8,12},{9,13},{10,... | collective-permute-start | bytes 196616 | tf_op jit(solution)/shard_map/ppermute | solution.py:37
  118.4 1.9 %collective-permute-start.29 = (bf16[32,1024]{1,0:T(8,128)(2,1)S(1)}, bf16[32,1024]{1,0:T(8,128)(2,1)S(1)}, u32[]{:S(2)}, u32[]{:S(2)}) collective-permute-start(bf16[32,1024]{1,0:T(8,128)(2,1)S(1)} %get-tuple-element.40), channel_id=1, source_target_pairs={{0,6},{1,7},{2,4},{3,5},{4,2},{5,3},{6,0},{7,1},{8,14},{9,15},{10,... | collective-permute-start | bytes 196616 | tf_op jit(solution)/shard_map/ppermute | solution.py:37
  121.1 2.7 %collective-permute-done.28 = bf16[32,1024]{1,0:T(8,128)(2,1)S(1)} collective-permute-done((bf16[32,1024]{1,0:T(8,128)(2,1)S(1)}, bf16[32,1024]{1,0:T(8,128)(2,1)S(1)}, u32[]{:S(2)}, u32[]{:S(2)}) %collective-permute-start.28) | collective-permute-done | bytes 65568 | tf_op jit(solution)/shard_map/ppermute | solution.py:37
  127.4 1.7 %collective-permute-start.32 = (bf16[32,1024]{1,0:T(8,128)(2,1)S(1)}, bf16[32,1024]{1,0:T(8,128)(2,1)S(1)}, u32[]{:S(2)}, u32[]{:S(2)}) collective-permute-start(bf16[32,1024]{1,0:T(8,128)(2,1)S(1)} %get-tuple-element.18), channel_id=1, source_target_pairs={{0,6},{1,7},{2,4},{3,5},{4,2},{5,3},{6,0},{7,1},{8,14},{9,15},{10,... | collective-permute-start | bytes 196616 | tf_op jit(solution)/shard_map/ppermute | solution.py:37
  129.1 3.7 %collective-permute-done.31 = bf16[32,1024]{1,0:T(8,128)(2,1)S(1)} collective-permute-done((bf16[32,1024]{1,0:T(8,128)(2,1)S(1)}, bf16[32,1024]{1,0:T(8,128)(2,1)S(1)}, u32[]{:S(2)}, u32[]{:S(2)}) %collective-permute-start.31) | collective-permute-done | bytes 65568 | tf_op jit(solution)/shard_map/ppermute | solution.py:37
  133.6 1.5 %collective-permute-done.33 = bf16[128,1024]{1,0:T(8,128)(2,1)S(1)} collective-permute-done((bf16[128,1024]{1,0:T(8,128)(2,1)S(1)}, bf16[128,1024]{1,0:T(8,128)(2,1)S(1)}, u32[]{:S(2)}, u32[]{:S(2)}) %collective-permute-start.33) | collective-permute-done | bytes 262176 | tf_op jit(solution)/shard_map/ppermute | solution.py:40
  (105 shorter events, 44.9 us)
Async XLA Ops:
  1.2 18.5 %collective-permute-start.3 = (f32[1,256]{1,0:T(1,128)S(1)}, f32[1,256]{1,0:T(1,128)S(1)}, u32[]{:S(2)}, u32[]{:S(2)}) collective-permute-start(f32[1,256]{1,0:T(1,128)S(1)} %bitcast.98), channel_id=1, source_target_pairs={{0,8},{8,0},{16,24},{24,16},{1,9},{9,1},{17,25},{25,17},{2,10},{10... | collective-permute-start | bytes 3080 | tf_op jit(solution)/shard_map/ppermute | solution.py:33
  4.3 15.8 %collective-permute-start.4 = (f32[1,256]{1,0:T(1,128)S(1)}, f32[1,256]{1,0:T(1,128)S(1)}, u32[]{:S(2)}, u32[]{:S(2)}) collective-permute-start(f32[1,256]{1,0:T(1,128)S(1)} %bitcast.99), channel_id=1, source_target_pairs={{0,16},{8,24},{16,0},{24,8},{1,17},{9,25},{17,1},{25,9},{2,18},{10... | collective-permute-start | bytes 3080 | tf_op jit(solution)/shard_map/ppermute | solution.py:33
  13.6 17.4 %collective-permute-start = (bf16[2,344,256]{2,1,0:T(8,128)(2,1)}, bf16[2,344,256]{2,1,0:T(8,128)(2,1)}, u32[]{:S(2)}, u32[]{:S(2)}) collective-permute-start(bf16[2,344,256]{2,1,0:T(8,128)(2,1)} %pad_maximum_fusion), channel_id=1, source_target_pairs={{0,8},{8,0},{16,24},{24,16},{1,9},{9,1},{17,25},{25,17},{2,10},{10... | collective-permute-start | bytes 1056776 | tf_op jit(solution)/shard_map/ppermute | solution.py:33
  14.9 17.0 %collective-permute-start.1 = (bf16[2,344,256]{2,1,0:T(8,128)(2,1)}, bf16[2,344,256]{2,1,0:T(8,128)(2,1)}, u32[]{:S(2)}, u32[]{:S(2)}) collective-permute-start(bf16[2,344,256]{2,1,0:T(8,128)(2,1)} %pad_maximum_fusion.1), channel_id=1, source_target_pairs={{0,16},{8,24},{16,0},{24,8},{1,17},{9,25},{17,1},{25,9},{2,18},{10... | collective-permute-start | bytes 1056776 | tf_op jit(solution)/shard_map/ppermute | solution.py:33
  15.7 16.2 %collective-permute-start.2 = (bf16[2,344,256]{2,1,0:T(8,128)(2,1)}, bf16[2,344,256]{2,1,0:T(8,128)(2,1)}, u32[]{:S(2)}, u32[]{:S(2)}) collective-permute-start(bf16[2,344,256]{2,1,0:T(8,128)(2,1)} %pad_maximum_fusion.2), channel_id=1, source_target_pairs={{0,24},{8,16},{16,8},{24,0},{1,25},{9,17},{17,9},{25,1},{2,26},{10... | collective-permute-start | bytes 1056776 | tf_op jit(solution)/shard_map/ppermute | solution.py:33
  19.8 11.1 %collective-permute-start.5 = (f32[1,256]{1,0:T(1,128)S(1)}, f32[1,256]{1,0:T(1,128)S(1)}, u32[]{:S(2)}, u32[]{:S(2)}) collective-permute-start(f32[1,256]{1,0:T(1,128)S(1)} %bitcast.100), channel_id=1, source_target_pairs={{0,24},{8,16},{16,8},{24,0},{1,25},{9,17},{17,9},{25,1},{2,26},{10... | collective-permute-start | bytes 3080 | tf_op jit(solution)/shard_map/ppermute | solution.py:33
  34.1 7.0 %collective-permute-start.6 = (bf16[344,256]{1,0:T(8,128)(2,1)S(1)}, bf16[344,256]{1,0:T(8,128)(2,1)S(1)}, u32[]{:S(2)}, u32[]{:S(2)}) collective-permute-start(bf16[344,256]{1,0:T(8,128)(2,1)S(1)} %fusion.40), channel_id=1, source_target_pairs={{0,8},{8,0},{16,24},{24,16},{1,9},{9,1},{17,25},{25,17},{2,10},{10... | collective-permute-start | bytes 528392 | tf_op jit(solution)/shard_map/ppermute | solution.py:33
  35.6 8.0 %collective-permute-start.7 = (bf16[344,256]{1,0:T(8,128)(2,1)S(1)}, bf16[344,256]{1,0:T(8,128)(2,1)S(1)}, u32[]{:S(2)}, u32[]{:S(2)}) collective-permute-start(bf16[344,256]{1,0:T(8,128)(2,1)S(1)} %fusion.40), channel_id=1, source_target_pairs={{0,16},{8,24},{16,0},{24,8},{1,17},{9,25},{17,1},{25,9},{2,18},{10... | collective-permute-start | bytes 528392 | tf_op jit(solution)/shard_map/ppermute | solution.py:33
  36.1 8.8 %collective-permute-start.8 = (bf16[344,256]{1,0:T(8,128)(2,1)S(1)}, bf16[344,256]{1,0:T(8,128)(2,1)S(1)}, u32[]{:S(2)}, u32[]{:S(2)}) collective-permute-start(bf16[344,256]{1,0:T(8,128)(2,1)S(1)} %fusion.40), channel_id=1, source_target_pairs={{0,24},{8,16},{16,8},{24,0},{1,25},{9,17},{17,9},{25,1},{2,26},{10... | collective-permute-start | bytes 528392 | tf_op jit(solution)/shard_map/ppermute | solution.py:33
  50.7 4.5 %collective-permute-start.10 = (bf16[32,1024]{1,0:T(8,128)(2,1)S(1)}, bf16[32,1024]{1,0:T(8,128)(2,1)S(1)}, u32[]{:S(2)}, u32[]{:S(2)}) collective-permute-start(bf16[32,1024]{1,0:T(8,128)(2,1)S(1)} %get-tuple-element.42), channel_id=1, source_target_pairs={{0,2},{1,3},{2,0},{3,1},{4,6},{5,7},{6,4},{7,5},{8,10},{9,11},{10,... | collective-permute-start | bytes 196616 | tf_op jit(solution)/shard_map/ppermute | solution.py:37
  52.0 7.5 %collective-permute-start.11 = (bf16[32,1024]{1,0:T(8,128)(2,1)S(1)}, bf16[32,1024]{1,0:T(8,128)(2,1)S(1)}, u32[]{:S(2)}, u32[]{:S(2)}) collective-permute-start(bf16[32,1024]{1,0:T(8,128)(2,1)S(1)} %get-tuple-element.44), channel_id=1, source_target_pairs={{0,4},{1,5},{2,6},{3,7},{4,0},{5,1},{6,2},{7,3},{8,12},{9,13},{10,... | collective-permute-start | bytes 196616 | tf_op jit(solution)/shard_map/ppermute | solution.py:37
  54.6 6.2 %collective-permute-start.12 = (bf16[32,1024]{1,0:T(8,128)(2,1)S(1)}, bf16[32,1024]{1,0:T(8,128)(2,1)S(1)}, u32[]{:S(2)}, u32[]{:S(2)}) collective-permute-start(bf16[32,1024]{1,0:T(8,128)(2,1)S(1)} %get-tuple-element.43), channel_id=1, source_target_pairs={{0,6},{1,7},{2,4},{3,5},{4,2},{5,3},{6,0},{7,1},{8,14},{9,15},{10,... | collective-permute-start | bytes 196616 | tf_op jit(solution)/shard_map/ppermute | solution.py:37
  60.9 4.5 %collective-permute-start.13 = (bf16[32,1024]{1,0:T(8,128)(2,1)S(1)}, bf16[32,1024]{1,0:T(8,128)(2,1)S(1)}, u32[]{:S(2)}, u32[]{:S(2)}) collective-permute-start(bf16[32,1024]{1,0:T(8,128)(2,1)S(1)} %get-tuple-element.22), channel_id=1, source_target_pairs={{0,2},{1,3},{2,0},{3,1},{4,6},{5,7},{6,4},{7,5},{8,10},{9,11},{10,... | collective-permute-start | bytes 196616 | tf_op jit(solution)/shard_map/ppermute | solution.py:37
  61.8 6.2 %collective-permute-start.14 = (bf16[32,1024]{1,0:T(8,128)(2,1)S(1)}, bf16[32,1024]{1,0:T(8,128)(2,1)S(1)}, u32[]{:S(2)}, u32[]{:S(2)}) collective-permute-start(bf16[32,1024]{1,0:T(8,128)(2,1)S(1)} %get-tuple-element.22), channel_id=1, source_target_pairs={{0,4},{1,5},{2,6},{3,7},{4,0},{5,1},{6,2},{7,3},{8,12},{9,13},{10,... | collective-permute-start | bytes 196616 | tf_op jit(solution)/shard_map/ppermute | solution.py:37
  63.5 6.1 %collective-permute-start.15 = (bf16[32,1024]{1,0:T(8,128)(2,1)S(1)}, bf16[32,1024]{1,0:T(8,128)(2,1)S(1)}, u32[]{:S(2)}, u32[]{:S(2)}) collective-permute-start(bf16[32,1024]{1,0:T(8,128)(2,1)S(1)} %get-tuple-element.22), channel_id=1, source_target_pairs={{0,6},{1,7},{2,4},{3,5},{4,2},{5,3},{6,0},{7,1},{8,14},{9,15},{10,... | collective-permute-start | bytes 196616 | tf_op jit(solution)/shard_map/ppermute | solution.py:37
  69.6 1.6 %collective-permute-start.16 = (bf16[128,1024]{1,0:T(8,128)(2,1)S(1)}, bf16[128,1024]{1,0:T(8,128)(2,1)S(1)}, u32[]{:S(2)}, u32[]{:S(2)}) collective-permute-start(bf16[128,1024]{1,0:T(8,128)(2,1)S(1)} %constant_dynamic-update-slice_fusion.4), channel_id=1, source_target_pairs={{0,1},{1,0},{2,3},{3,2},{4,5},{5,4},{6,7},{7,6},{8,9},{9,8},{10,11... | collective-permute-start | bytes 786440 | tf_op jit(solution)/shard_map/ppermute | solution.py:40
  71.4 11.4 %collective-permute-start.20 = (f32[1,256]{1,0:T(1,128)S(1)}, f32[1,256]{1,0:T(1,128)S(1)}, u32[]{:S(2)}, u32[]{:S(2)}) collective-permute-start(f32[1,256]{1,0:T(1,128)S(1)} %bitcast.102), channel_id=1, source_target_pairs={{0,8},{8,0},{16,24},{24,16},{1,9},{9,1},{17,25},{25,17},{2,10},{10... | collective-permute-start | bytes 3080 | tf_op jit(solution)/shard_map/ppermute | solution.py:33
  72.1 12.6 %collective-permute-start.21 = (f32[1,256]{1,0:T(1,128)S(1)}, f32[1,256]{1,0:T(1,128)S(1)}, u32[]{:S(2)}, u32[]{:S(2)}) collective-permute-start(f32[1,256]{1,0:T(1,128)S(1)} %bitcast.103), channel_id=1, source_target_pairs={{0,16},{8,24},{16,0},{24,8},{1,17},{9,25},{17,1},{25,9},{2,18},{10... | collective-permute-start | bytes 3080 | tf_op jit(solution)/shard_map/ppermute | solution.py:33
  73.3 11.3 %collective-permute-start.22 = (f32[1,256]{1,0:T(1,128)S(1)}, f32[1,256]{1,0:T(1,128)S(1)}, u32[]{:S(2)}, u32[]{:S(2)}) collective-permute-start(f32[1,256]{1,0:T(1,128)S(1)} %bitcast.104), channel_id=1, source_target_pairs={{0,24},{8,16},{16,8},{24,0},{1,25},{9,17},{17,9},{25,1},{2,26},{10... | collective-permute-start | bytes 3080 | tf_op jit(solution)/shard_map/ppermute | solution.py:33
  80.8 11.2 %collective-permute-start.17 = (bf16[2,344,256]{2,1,0:T(8,128)(2,1)S(1)}, bf16[2,344,256]{2,1,0:T(8,128)(2,1)S(1)}, u32[]{:S(2)}, u32[]{:S(2)}) collective-permute-start(bf16[2,344,256]{2,1,0:T(8,128)(2,1)S(1)} %pad_maximum_fusion.3), channel_id=1, source_target_pairs={{0,8},{8,0},{16,24},{24,16},{1,9},{9,1},{17,25},{25,17},{2,10},{10... | collective-permute-start | bytes 1056776 | tf_op jit(solution)/shard_map/ppermute | solution.py:33
  81.5 16.8 %collective-permute-start.18 = (bf16[2,344,256]{2,1,0:T(8,128)(2,1)S(1)}, bf16[2,344,256]{2,1,0:T(8,128)(2,1)S(1)}, u32[]{:S(2)}, u32[]{:S(2)}) collective-permute-start(bf16[2,344,256]{2,1,0:T(8,128)(2,1)S(1)} %pad_maximum_fusion.4), channel_id=1, source_target_pairs={{0,16},{8,24},{16,0},{24,8},{1,17},{9,25},{17,1},{25,9},{2,18},{10... | collective-permute-start | bytes 1056776 | tf_op jit(solution)/shard_map/ppermute | solution.py:33
  82.8 15.4 %collective-permute-start.19 = (bf16[2,344,256]{2,1,0:T(8,128)(2,1)S(1)}, bf16[2,344,256]{2,1,0:T(8,128)(2,1)S(1)}, u32[]{:S(2)}, u32[]{:S(2)}) collective-permute-start(bf16[2,344,256]{2,1,0:T(8,128)(2,1)S(1)} %pad_maximum_fusion.5), channel_id=1, source_target_pairs={{0,24},{8,16},{16,8},{24,0},{1,25},{9,17},{17,9},{25,1},{2,26},{10... | collective-permute-start | bytes 1056776 | tf_op jit(solution)/shard_map/ppermute | solution.py:33
  99.2 6.7 %collective-permute-start.23 = (bf16[344,256]{1,0:T(8,128)(2,1)S(1)}, bf16[344,256]{1,0:T(8,128)(2,1)S(1)}, u32[]{:S(2)}, u32[]{:S(2)}) collective-permute-start(bf16[344,256]{1,0:T(8,128)(2,1)S(1)} %fusion.50), channel_id=1, source_target_pairs={{0,8},{8,0},{16,24},{24,16},{1,9},{9,1},{17,25},{25,17},{2,10},{10... | collective-permute-start | bytes 528392 | tf_op jit(solution)/shard_map/ppermute | solution.py:33
  100.7 8.1 %collective-permute-start.24 = (bf16[344,256]{1,0:T(8,128)(2,1)S(1)}, bf16[344,256]{1,0:T(8,128)(2,1)S(1)}, u32[]{:S(2)}, u32[]{:S(2)}) collective-permute-start(bf16[344,256]{1,0:T(8,128)(2,1)S(1)} %fusion.50), channel_id=1, source_target_pairs={{0,16},{8,24},{16,0},{24,8},{1,17},{9,25},{17,1},{25,9},{2,18},{10... | collective-permute-start | bytes 528392 | tf_op jit(solution)/shard_map/ppermute | solution.py:33
  101.0 9.1 %collective-permute-start.25 = (bf16[344,256]{1,0:T(8,128)(2,1)S(1)}, bf16[344,256]{1,0:T(8,128)(2,1)S(1)}, u32[]{:S(2)}, u32[]{:S(2)}) collective-permute-start(bf16[344,256]{1,0:T(8,128)(2,1)S(1)} %fusion.50), channel_id=1, source_target_pairs={{0,24},{8,16},{16,8},{24,0},{1,25},{9,17},{17,9},{25,1},{2,26},{10... | collective-permute-start | bytes 528392 | tf_op jit(solution)/shard_map/ppermute | solution.py:33
  114.1 1.6 %collective-permute-start.26 = (bf16[128,1024]{1,0:T(8,128)(2,1)S(1)}, bf16[128,1024]{1,0:T(8,128)(2,1)S(1)}, u32[]{:S(2)}, u32[]{:S(2)}) collective-permute-start(bf16[128,1024]{1,0:T(8,128)(2,1)S(1)} %dynamic-slice_convert_fusion), channel_id=1, source_target_pairs={{0,1},{1,0},{2,3},{3,2},{4,5},{5,4},{6,7},{7,6},{8,9},{9,8},{10,11... | collective-permute-start | bytes 786440 | tf_op jit(solution)/shard_map/ppermute | solution.py:40
  115.8 5.3 %collective-permute-start.27 = (bf16[32,1024]{1,0:T(8,128)(2,1)S(1)}, bf16[32,1024]{1,0:T(8,128)(2,1)S(1)}, u32[]{:S(2)}, u32[]{:S(2)}) collective-permute-start(bf16[32,1024]{1,0:T(8,128)(2,1)S(1)} %get-tuple-element.39), channel_id=1, source_target_pairs={{0,2},{1,3},{2,0},{3,1},{4,6},{5,7},{6,4},{7,5},{8,10},{9,11},{10,... | collective-permute-start | bytes 196616 | tf_op jit(solution)/shard_map/ppermute | solution.py:37
  115.9 7.9 %collective-permute-start.28 = (bf16[32,1024]{1,0:T(8,128)(2,1)S(1)}, bf16[32,1024]{1,0:T(8,128)(2,1)S(1)}, u32[]{:S(2)}, u32[]{:S(2)}) collective-permute-start(bf16[32,1024]{1,0:T(8,128)(2,1)S(1)} %get-tuple-element.41), channel_id=1, source_target_pairs={{0,4},{1,5},{2,6},{3,7},{4,0},{5,1},{6,2},{7,3},{8,12},{9,13},{10,... | collective-permute-start | bytes 196616 | tf_op jit(solution)/shard_map/ppermute | solution.py:37
  118.4 6.2 %collective-permute-start.29 = (bf16[32,1024]{1,0:T(8,128)(2,1)S(1)}, bf16[32,1024]{1,0:T(8,128)(2,1)S(1)}, u32[]{:S(2)}, u32[]{:S(2)}) collective-permute-start(bf16[32,1024]{1,0:T(8,128)(2,1)S(1)} %get-tuple-element.40), channel_id=1, source_target_pairs={{0,6},{1,7},{2,4},{3,5},{4,2},{5,3},{6,0},{7,1},{8,14},{9,15},{10,... | collective-permute-start | bytes 196616 | tf_op jit(solution)/shard_map/ppermute | solution.py:37
  124.6 4.5 %collective-permute-start.30 = (bf16[32,1024]{1,0:T(8,128)(2,1)S(1)}, bf16[32,1024]{1,0:T(8,128)(2,1)S(1)}, u32[]{:S(2)}, u32[]{:S(2)}) collective-permute-start(bf16[32,1024]{1,0:T(8,128)(2,1)S(1)} %get-tuple-element.18), channel_id=1, source_target_pairs={{0,2},{1,3},{2,0},{3,1},{4,6},{5,7},{6,4},{7,5},{8,10},{9,11},{10,... | collective-permute-start | bytes 196616 | tf_op jit(solution)/shard_map/ppermute | solution.py:37
  126.1 6.8 %collective-permute-start.31 = (bf16[32,1024]{1,0:T(8,128)(2,1)S(1)}, bf16[32,1024]{1,0:T(8,128)(2,1)S(1)}, u32[]{:S(2)}, u32[]{:S(2)}) collective-permute-start(bf16[32,1024]{1,0:T(8,128)(2,1)S(1)} %get-tuple-element.18), channel_id=1, source_target_pairs={{0,4},{1,5},{2,6},{3,7},{4,0},{5,1},{6,2},{7,3},{8,12},{9,13},{10,... | collective-permute-start | bytes 196616 | tf_op jit(solution)/shard_map/ppermute | solution.py:37
  127.4 6.2 %collective-permute-start.32 = (bf16[32,1024]{1,0:T(8,128)(2,1)S(1)}, bf16[32,1024]{1,0:T(8,128)(2,1)S(1)}, u32[]{:S(2)}, u32[]{:S(2)}) collective-permute-start(bf16[32,1024]{1,0:T(8,128)(2,1)S(1)} %get-tuple-element.18), channel_id=1, source_target_pairs={{0,6},{1,7},{2,4},{3,5},{4,2},{5,3},{6,0},{7,1},{8,14},{9,15},{10,... | collective-permute-start | bytes 196616 | tf_op jit(solution)/shard_map/ppermute | solution.py:37
  (6 other events, 25.2 us)

commit v2 on v0

v2 whole, which is shorter than its diff:
```python
import functools

import jax
import jax.numpy as jnp
from jax import lax
from jax.experimental import pallas as pl
from jax.experimental.pallas import tpu as pltpu
from jax.sharding import PartitionSpec as P

epsilon = 1e-06
F32 = jnp.float32
BF16 = jnp.bfloat16
EXTRA = 8
CHUNKS = 1
VMEM = pl.BlockSpec(memory_space=pltpu.VMEM)


def cost(flops, moved):
    return pl.CostEstimate(flops=int(flops), bytes_accessed=int(moved), transcendentals=0)


def up_kernel(near_ref, far_ref, side_ref, gain_ref, gate_ref, value_ref, out_ref, rows_ref, scaled_ref, *, starts, piece, joined):
    slot = pl.program_id(0)

    @pl.when(slot == 0)
    def _():
        if joined:
            half = near_ref.shape[0]
            side = side_ref[0]
            rows_ref[pl.ds(pl.multiple_of(side * half, half), half), :] = near_ref[...]
            rows_ref[pl.ds(pl.multiple_of((1 - side) * half, half), half), :] = far_ref[...]
            current = rows_ref[...].astype(F32)
        else:
            current = near_ref[...].astype(F32)
        scaled_ref[...] = (current * gain_ref[...]).astype(BF16)
        squares = current * current
        width = squares.shape[1]
        folded = squares[:, :128]
        for k in range(1, width // 128):
            folded = folded + squares[:, k * 128 : (k + 1) * 128]
        total = jnp.sum(folded.T, axis=0, keepdims=True)
        high = total.astype(BF16)
        low = (total - high.astype(F32)).astype(BF16)
        row = lax.broadcasted_iota(jnp.int32, (EXTRA, total.shape[1]), 0)
        tail = jnp.where(row == 0, high.astype(F32), jnp.where(row == 1, low.astype(F32), 0.0))
        rows_ref[0:EXTRA, 0 : total.shape[1]] = tail.astype(BF16)

    scaled = scaled_ref[...]
    contract = (((1,), (1,)), ((), ()))
    out_ref[0, 0:piece, :] = lax.dot_general(
        gate_ref[...], scaled, contract, preferred_element_type=F32
    ).astype(BF16)
    out_ref[0, piece : 2 * piece, :] = lax.dot_general(
        value_ref[...], scaled, contract, preferred_element_type=F32
    ).astype(BF16)
    out_ref[0, 2 * piece : 2 * piece + EXTRA, :] = rows_ref[0:EXTRA, 0 : out_ref.shape[2]]


def act_kernel(parts_ref, taps_ref, prior_ref, out_ref, held_ref, *, piece, width, first, layer, kernel):
    n = parts_ref.shape[0]
    total = parts_ref[0].astype(F32)
    for s in range(1, n):
        total = total + parts_ref[s].astype(F32)
    tail = total[2 * piece : 2 * piece + EXTRA]
    squares = tail[0:1] + tail[1:2]
    inverse = lax.rsqrt(squares / width + epsilon)
    lin = total[: 2 * piece] * inverse
    if held_ref is not None:
        held_ref[...] = lin
    lane = lax.broadcasted_iota(jnp.int32, (piece, lin.shape[1]), 1)

    def conv(kind):
        current = lin[kind * piece : (kind + 1) * piece]
        result = None
        for k in range(kernel):
            shift = kernel - 1 - k
            column = (layer * 2 + kind) * kernel + k
            tap = taps_ref[:, column : column + 1]
            moved = current
            if shift:
                moved = pltpu.roll(current, shift, 1)
                if first:
                    fill = jnp.zeros_like(moved)
                else:
                    fill = pltpu.roll(prior_ref[kind * piece : (kind + 1) * piece, :], shift, 1)
                moved = jnp.where(lane < shift, fill, moved)
            term = tap * moved
            result = term if result is None else result + term
        return result

    gate, value = conv(0), conv(1)
    hidden = (gate / (1.0 + jnp.exp(-gate)) * value).astype(BF16)
    for s in range(n):
        out_ref[s] = hidden


def down_kernel(hidden_ref, weight_ref, side_ref, away_ref, kept_ref, total_ref, *, starts, piece):
    total = None
    for s, begin in enumerate(starts):
        skip = s * piece - begin
        if skip >= piece:
            continue
        term = lax.dot_general(
            hidden_ref[s, skip:piece, :],
            weight_ref[begin + skip : begin + piece, :],
            (((0,), (0,)), ((), ())),
            preferred_element_type=F32,
        )
        total = term if total is None else total + term
    total_ref[...] = total
    half = away_ref.shape[0]
    side = side_ref[0]
    away_ref[...] = total_ref[pl.ds(pl.multiple_of((1 - side) * half, half), half), :].astype(BF16)
    kept_ref[...] = total_ref[pl.ds(pl.multiple_of(side * half, half), half), :]


def make_body(mesh):
    n_a = mesh.shape["ra"]
    n_c = mesh.shape["cb"]
    n_z = n_c // 2
    z_groups = [[z * 2 + k for z in range(n_z)] for k in range(2)]

    def trade_a(value):
        return lax.all_to_all(value, "ra", 0, 0)

    def trade_z(value):
        return lax.all_to_all(value, "cb", 0, 0, axis_index_groups=z_groups)

    def trade_core(value):
        return lax.ppermute(value, "cb", [(i, i ^ 1) for i in range(n_c)])

    def body(tokens, norm_gain, gate_weight, value_weight, gate_taps, value_taps, down_weight):
        layers, width, units = gate_weight.shape
        kernel = gate_taps.shape[1]
        count = tokens.shape[0] // CHUNKS
        piece = -(-(-(-units // n_a)) // 8) * 8
        starts = [min(p * piece, units - piece) for p in range(n_a)]
        even = starts[-1] == (n_a - 1) * piece
        a = lax.axis_index("ra")
        c = lax.axis_index("cb")
        z, core = c // 2, c % 2
        side = core.astype(jnp.int32).reshape(1)
        half = count // 2
        span = half // n_z
        gate_rows = gate_weight.transpose(0, 2, 1)
        value_rows = value_weight.transpose(0, 2, 1)
        if not even:
            index = jnp.concatenate([jnp.arange(b, b + piece) for b in starts])
            gate_rows = gate_rows[:, index]
            value_rows = value_rows[:, index]

        my = jnp.minimum(a * piece, units - piece)
        taps = jnp.stack([gate_taps, value_taps], axis=1).reshape(layers * 2 * kernel, units)
        taps = lax.dynamic_slice_in_dim(taps, my, piece, 1).T

        def up(layer, near, far):
            joined = far is not None
            rows = 2 * piece + EXTRA
            body_fn = functools.partial(up_kernel, starts=starts, piece=piece, joined=joined)
            if not joined:
                far = near
            whole = lambda shape: pl.BlockSpec(shape, lambda i: (0,) * len(shape))
            return pl.pallas_call(
                body_fn,
                grid=(n_a,),
                in_specs=[
                    whole(near.shape),
                    whole(far.shape),
                    pl.BlockSpec(memory_space=pltpu.SMEM),
                    whole((1, width)),
                    pl.BlockSpec((None, piece, width), lambda i: (layer, i, 0)),
                    pl.BlockSpec((None, piece, width), lambda i: (layer, i, 0)),
                ],
                out_specs=pl.BlockSpec((1, rows, count), lambda i: (i, 0, 0)),
                out_shape=jax.ShapeDtypeStruct((n_a, rows, count), BF16),
                scratch_shapes=[
                    pltpu.VMEM((count, max(width, count)), BF16),
                    pltpu.VMEM((count, width), BF16),
                ],
                cost_estimate=cost(4 * units * width * count, 4 * units * width),
                name=f"up{layer}",
            )(near, far, side, norm_gain[layer][None, :], gate_rows, value_rows)

        def act(layer, chunk, parts, prior):
            first, last = chunk == 0, chunk == CHUNKS - 1
            args = [parts, taps]
            if not first:
                args.append(prior)
            shapes = [jax.ShapeDtypeStruct((n_a, piece, count), BF16)]
            if not last:
                shapes.append(jax.ShapeDtypeStruct((2 * piece, count), F32))

            def body_fn(*refs):
                refs = list(refs)
                if first:
                    refs.insert(2, None)
                if last:
                    refs.append(None)
                act_kernel(
                    *refs, piece=piece, width=width * n_a, first=first, layer=layer, kernel=kernel
                )

            out = pl.pallas_call(
                body_fn,
                in_specs=[VMEM] * len(args),
                out_specs=[VMEM] * len(shapes),
                out_shape=shapes,
                cost_estimate=cost(60 * 2 * piece * count, 4 * n_a * piece * count),
                name=f"act{layer}_{chunk}",
            )(*args)
            return (out[0], None) if last else out

        def down(layer, hidden):
            return pl.pallas_call(
                functools.partial(down_kernel, starts=starts, piece=piece),
                grid=(1,),
                in_specs=[
                    pl.BlockSpec((n_a, piece, count), lambda i: (0, 0, 0)),
                    pl.BlockSpec((None, units, width), lambda i: (layer, 0, 0)),
                    pl.BlockSpec(memory_space=pltpu.SMEM),
                ],
                out_specs=[pl.BlockSpec((half, width), lambda i: (0, 0))] * 2,
                out_shape=[
                    jax.ShapeDtypeStruct((half, width), BF16),
                    jax.ShapeDtypeStruct((half, width), F32),
                ],
                scratch_shapes=[pltpu.VMEM((count, width), F32)],
                cost_estimate=cost(2 * units * width * count, 2 * units * width),
                name=f"down{layer}",
            )(hidden, down_weight, side)

        near = [tokens[i * count : (i + 1) * count] for i in range(CHUNKS)]
        far = [None] * CHUNKS
        old = [
            lax.dynamic_slice_in_dim(near[i], core * half + z * span, span, 0)
            for i in range(CHUNKS)
        ]
        for layer in range(layers):
            prior = None
            for i in range(CHUNKS):
                parts = trade_a(up(layer, near[i], far[i]))
                mine, prior = act(layer, i, parts, prior)
                away, kept = down(layer, trade_a(mine))
                total = kept + trade_core(away).astype(F32)
                terms = trade_z(total.astype(BF16).reshape(n_z, span, width))
                branch = jnp.sum(terms.astype(F32), axis=0)
                old[i] = (0.5 * old[i].astype(F32) + branch).astype(BF16)
                spread = jnp.broadcast_to(old[i][None], (n_z, span, width))
                near[i] = trade_z(spread).reshape(half, width)
                far[i] = trade_core(near[i])
        parts = []
        for i in range(CHUNKS):
            parts.append(jnp.where(core == 0, near[i], far[i]))
            parts.append(jnp.where(core == 0, far[i], near[i]))
        return jnp.concatenate(parts, axis=0)

    return body


def solution(mesh):
    return jax.shard_map(
        make_body(mesh),
        mesh=mesh,
        in_specs=(
            P(None, "ra"),
            P(None, "ra"),
            P(None, "ra", "cb"),
            P(None, "ra", "cb"),
            P(None, None, "cb"),
            P(None, None, "cb"),
            P(None, "cb", "ra"),
        ),
        out_specs=P(None, "ra"),
        check_vma=False,
    )
```

time: 334 us -> 165 us (0.49)
  waiting for transfers between devices: 262 us -> 32.4 us
  blocking collectives: 21.6 us -> 85.4 us
  matrix products: 28 us -> 0 us
  Pallas kernels: 0 us -> 26.5 us
  between operations: 13.2 us -> 0.08 us
  starting transfers between devices: 0.13 us -> 10.3 us
    psum x4 -> x0, waiting for transfers between devices: 262 us -> none  [the longest x2 143 us: body(): gate_sum, value_sum = lax.psum((gate_part, value_part), 'ra')]
    all_to_all x0 -> x6, blocking collectives: none -> 85.4 us  [the longest x3 51.9 us: trade_a(): return lax.all_to_all(value, 'ra', 0, 0)]
    dot_general x6 -> x0, matrix products: 28 us -> none  [the longest x2 12.5 us: body(): jnp.dot(hidden, down_weight[layer_index], preferred_element_type=jnp.floa...]
    pallas_call x0 -> x6, Pallas kernels: none -> 26.5 us  [the longest x2 12 us: up(): pl.pallas_call(body_fn, grid=(n_a,), in_specs=[whole(near.shape), whole(f...]
    all_to_all x0 -> x2, waiting for transfers between devices: none -> 25.8 us  [the longest x1 16.6 us: trade_a(): return lax.all_to_all(value, 'ra', 0, 0)]
    psum x2 -> x0, blocking collectives: 21.6 us -> none  [body(): total_squares = lax.psum(local_squares, 'ra')]
    all_to_all x0 -> x2, starting transfers between devices: none -> 10.3 us  [the longest x1 5.36 us: trade_a(): return lax.all_to_all(value, 'ra', 0, 0)]
    ppermute x0 -> x4, waiting for transfers between devices: none -> 6.55 us  [trade_core(): return lax.ppermute(value, 'cb', [(i, i ^ 1) for i in range(n_c)])]
  transfers between devices with their start and end apart: 4 -> 6, of which waited for: 4 -> 6; matrix products, arithmetic and copies ran while one was open for 0% -> 1% of each run, Pallas kernels for 0% -> 0%
where the time goes in v2:
time: 165 us; the launch traced here: 164 us
  blocking collectives  85.4 us (52%)
  waiting for transfers between devices  32.4 us (20%)
  Pallas kernels  26.5 us (16%)
  starting transfers between devices  10.3 us (6%)
  other arithmetic  4.8 us (3%)
  local copies, waits for them, and re-layouts  4.2 us (3%)
    all_to_all x3, blocking collectives, trade_a(): return lax.all_to_all(value, 'ra', 0, 0)  51.9 us
    all_to_all x3, blocking collectives, trade_z(): return lax.all_to_all(value, 'cb', 0, 0, axis_index_groups=z_groups)  33.5 us
    all_to_all x1, waiting for transfers between devices, trade_a(): return lax.all_to_all(value, 'ra', 0, 0)  16.6 us
    pallas_call x2, Pallas kernels, up(): pl.pallas_call(body_fn, grid=(n_a,), in_specs=[whole(near.shape), whole(f...  12 us
    all_to_all x1, waiting for transfers between devices, trade_z(): return lax.all_to_all(value, 'cb', 0, 0, axis_index_groups=z_groups)  9.21 us
    pallas_call x2, Pallas kernels, down(): pl.pallas_call(functools.partial(down_kernel, starts=starts, piece=piece)...  8.39 us
    ppermute x4, waiting for transfers between devices, trade_core(): return lax.ppermute(value, 'cb', [(i, i ^ 1) for i in range(n_c)])  6.55 us
    pallas_call x2, Pallas kernels, act(): pl.pallas_call(body_fn, in_specs=[VMEM] * len(args), out_specs=[VMEM] * l...  6.1 us
  transfers between devices with their start and end apart: 6, of which 6 were waited for; matrix products, arithmetic and copies ran while one was open for 1% of the time, Pallas kernels for 0%

profile of v2, /device:TPU:0, one launch (start us, length us, event | category | flops | bytes accessed | tf_op | source)
XLA Modules:
  0.0 163.7 jit_solution(8034848137370973115)
XLA Ops:
  0.0 1.4 fusion
  1.4 6.2 %up0.1 = bf16[4,696,256]{2,1,0:T(8,128)(2,1)} custom-call(bf16[256,1024]{1,0:T(8,128)(2,1)} %far_ref.1, bf16[256,1024]{1,0:T(8,128)(2,1)} %far_ref.1, s32[1]{0:T(128)} %bitcast.side_ref, f32[1,1024]{1,0:T(1,128)} %get-tuple-element.16.gain_ref, bf16[2,1376,1024]{2,1,0:T(8,128)(2,1)} %bitcast.12, bf16[2,1376,1024]{2,1,0:T(8,128)(2,1)} %bitcast.14), custom_call_target="tpu_custom_call" | custom-call | flops 1442840576 | bytes 5636096 | tf_op jit(solution)/shard_map/up0/pallas_call | solution.py:163
  7.6 5.4 %all-to-all-start = ((bf16[4,696,256]{2,1,0:T(8,128)(2,1)}), bf16[4,696,256]{2,1,0:T(8,128)(2,1)S(1)}, u32[]{:S(2)}, u32[]{:S(2)}) async-start(bf16[4,696,256]{2,1,0:T(8,128)(2,1)} %up0.1), calls=%async_computation | async-start | bytes 2850816 | tf_op jit(solution)/shard_map/all_to_all | solution.py:124
  13.0 0.1 constant_dynamic-slice_fusion
  13.1 0.8 copy.11
  13.9 16.6 %all-to-all-done.refs_0_ = bf16[4,696,256]{2,1,0:T(8,128)(2,1)S(1)} async-done(((bf16[4,696,256]{2,1,0:T(8,128)(2,1)}), bf16[4,696,256]{2,1,0:T(8,128)(2,1)S(1)}, u32[]{:S(2)}, u32[]{:S(2)}) %all-to-all-start) | async-done | bytes 1425440 | tf_op jit(solution)/shard_map/all_to_all | solution.py:124
  30.6 1.1 copy-done
  31.7 3.0 %act0_0.1 = bf16[4,344,256]{2,1,0:T(8,128)(2,1)} custom-call(bf16[4,696,256]{2,1,0:T(8,128)(2,1)} %copy-done, f32[344,12]{1,0:T(8,128)} %bitcast.16), custom_call_target="tpu_custom_call" | custom-call | flops 10567680 | bytes 1409024 | tf_op jit(solution)/shard_map/act0_0/pallas_call | solution.py:203
  34.7 14.4 %all_to_all.40.hidden_ref = bf16[4,344,256]{2,1,0:T(8,128)(2,1)} all-to-all(bf16[4,344,256]{2,1,0:T(8,128)(2,1)} %act0_0.1), channel_id=1, replica_groups=mesh['ra'=4,'cb'=8] {'ra'}, dimensions={0} | all-to-all | bytes 1409024 | tf_op jit(solution)/shard_map/all_to_all | solution.py:124
  49.2 4.2 %down0.1 = (bf16[128,1024]{1,0:T(8,128)(2,1)}, f32[128,1024]{1,0:T(8,128)}) custom-call(bf16[4,344,256]{2,1,0:T(8,128)(2,1)} %all_to_all.40.hidden_ref, bf16[2,1376,1024]{2,1,0:T(8,128)(2,1)} %weight_ref.3, s32[1]{0:T(128)} %bitcast.side_ref), custom_call_target="tpu_custom_call" | custom-call | flops 721420288 | bytes 2818048 | tf_op jit(solution)/shard_map/down0/pallas_call | solution.py:214
  53.4 1.7 %collective-permute-done = bf16[128,1024]{1,0:T(8,128)(2,1)S(1)} collective-permute-done((bf16[128,1024]{1,0:T(8,128)(2,1)}, bf16[128,1024]{1,0:T(8,128)(2,1)S(1)}, u32[]{:S(2)}, u32[]{:S(2)}) %collective-permute-start) | collective-permute-done | bytes 262176 | tf_op jit(solution)/shard_map/ppermute | solution.py:130
  55.1 1.8 %add_convert_fusion.1 = bf16[128,1024]{1,0:T(8,128)(2,1)} fusion(f32[128,1024]{1,0:T(8,128)} %get-tuple-element.9, bf16[128,1024]{1,0:T(8,128)(2,1)S(1)} %collective-permute-done), kind=kLoop, calls=%fused_computation.4 | loop fusion | flops 393216 | bytes 1048576 | tf_op jit(solution)/shard_map/convert_element_type | solution.py:245
  56.9 5.0 %all-to-all-start.2 = ((bf16[4,32,1024]{2,1,0:T(8,128)(2,1)}), bf16[4,32,1024]{2,1,0:T(8,128)(2,1)S(1)}, u32[]{:S(2)}, u32[]{:S(2)}) async-start(bf16[4,32,1024]{2,1,0:T(8,128)(2,1)} %bitcast.6), calls=%async_computation.2 | async-start | bytes 524288 | tf_op jit(solution)/shard_map/all_to_all | solution.py:127
  61.9 9.2 %all-to-all-done.2 = bf16[4,32,1024]{2,1,0:T(8,128)(2,1)S(1)} async-done(((bf16[4,32,1024]{2,1,0:T(8,128)(2,1)}), bf16[4,32,1024]{2,1,0:T(8,128)(2,1)S(1)}, u32[]{:S(2)}, u32[]{:S(2)}) %all-to-all-start.2) | async-done | bytes 262176 | tf_op jit(solution)/shard_map/all_to_all | solution.py:127
  71.1 0.9 add_convert_fusion.3
  72.0 10.6 %all_to_all.41 = bf16[4,32,1024]{2,1,0:T(8,128)(2,1)S(1)} all-to-all(bf16[4,32,1024]{2,1,0:T(8,128)(2,1)S(1)} %broadcast_in_dim.4), channel_id=1, replica_groups={{0,2,4,6},{1,3,5,7},{8,10,12,14},{9,11,13,15},{16,18,20,22},{17,19,21,2..., dimensions={0} | all-to-all | bytes 524288 | tf_op jit(solution)/shard_map/all_to_all | solution.py:127
  82.7 1.5 collective-permute-done.1.far_ref
  84.2 0.7 copy-done.2
  84.9 5.8 %up1.1 = bf16[4,696,256]{2,1,0:T(8,128)(2,1)} custom-call(bf16[128,1024]{1,0:T(8,128)(2,1)} %bitcast.19, bf16[128,1024]{1,0:T(8,128)(2,1)} %copy-done.2, s32[1]{0:T(128)} %bitcast.side_ref, f32[1,1024]{1,0:T(1,128)} %get-tuple-element.15.gain_ref, bf16[2,1376,1024]{2,1,0:T(8,128)(2,1)} %bitcast.13, bf16[2,1376,1024]{2,1,0:T(8,128)(2,1)} %bitcast.15), custom_call_target="tpu_custom_call" | custom-call | flops 1442840576 | bytes 5636096 | tf_op jit(solution)/shard_map/up1/pallas_call | solution.py:163
  90.7 23.2 %all_to_all.42.refs_0_ = bf16[4,696,256]{2,1,0:T(8,128)(2,1)} all-to-all(bf16[4,696,256]{2,1,0:T(8,128)(2,1)} %up1.1), channel_id=1, replica_groups=mesh['ra'=4,'cb'=8] {'ra'}, dimensions={0} | all-to-all | bytes 2850816 | tf_op jit(solution)/shard_map/all_to_all | solution.py:124
  113.9 3.1 %act1_0.1 = bf16[4,344,256]{2,1,0:T(8,128)(2,1)} custom-call(bf16[4,696,256]{2,1,0:T(8,128)(2,1)} %all_to_all.42.refs_0_, f32[344,12]{1,0:T(8,128)} %bitcast.17), custom_call_target="tpu_custom_call" | custom-call | flops 10567680 | bytes 1409024 | tf_op jit(solution)/shard_map/act1_0/pallas_call | solution.py:203
  117.0 14.3 %all_to_all.43.hidden_ref = bf16[4,344,256]{2,1,0:T(8,128)(2,1)} all-to-all(bf16[4,344,256]{2,1,0:T(8,128)(2,1)} %act1_0.1), channel_id=1, replica_groups=mesh['ra'=4,'cb'=8] {'ra'}, dimensions={0} | all-to-all | bytes 1409024 | tf_op jit(solution)/shard_map/all_to_all | solution.py:124
  131.3 4.2 %down1.1 = (bf16[128,1024]{1,0:T(8,128)(2,1)}, f32[128,1024]{1,0:T(8,128)}) custom-call(bf16[4,344,256]{2,1,0:T(8,128)(2,1)} %all_to_all.43.hidden_ref, bf16[2,1376,1024]{2,1,0:T(8,128)(2,1)} %weight_ref.3, s32[1]{0:T(128)} %bitcast.side_ref), custom_call_target="tpu_custom_call" | custom-call | flops 721420288 | bytes 2818048 | tf_op jit(solution)/shard_map/down1/pallas_call | solution.py:214
  135.5 0.0 collective-permute-start.2
  135.5 1.7 %collective-permute-done.2 = bf16[128,1024]{1,0:T(8,128)(2,1)S(1)} collective-permute-done((bf16[128,1024]{1,0:T(8,128)(2,1)}, bf16[128,1024]{1,0:T(8,128)(2,1)S(1)}, u32[]{:S(2)}, u32[]{:S(2)}) %collective-permute-start.2) | collective-permute-done | bytes 262176 | tf_op jit(solution)/shard_map/ppermute | solution.py:130
  137.2 1.1 add_convert_fusion
  138.3 11.8 %all_to_all.44 = bf16[4,32,1024]{2,1,0:T(8,128)(2,1)S(1)} all-to-all(bf16[4,32,1024]{2,1,0:T(8,128)(2,1)S(1)} %bitcast.21), channel_id=1, replica_groups={{0,2,4,6},{1,3,5,7},{8,10,12,14},{9,11,13,15},{16,18,20,22},{17,19,21,2..., dimensions={0} | all-to-all | bytes 524288 | tf_op jit(solution)/shard_map/all_to_all | solution.py:127
  150.3 11.0 %all_to_all.45 = bf16[4,32,1024]{2,1,0:T(8,128)(2,1)S(1)} all-to-all(bf16[4,32,1024]{2,1,0:T(8,128)(2,1)S(1)} %broadcast_in_dim.5), channel_id=1, replica_groups={{0,2,4,6},{1,3,5,7},{8,10,12,14},{9,11,13,15},{16,18,20,22},{17,19,21,2..., dimensions={0} | all-to-all | bytes 524288 | tf_op jit(solution)/shard_map/all_to_all | solution.py:127
  161.3 0.0 collective-permute-start.3
  161.3 1.5 collective-permute-done.3
  162.8 0.1 broadcast_select_fusion.1
  162.9 0.8 pad_maximum_fusion
  (18 shorter events, 0.2 us)
Async XLA Ops:
  7.6 5.4 %copy-start.3 = (f32[2,3,1376]{2,0,1:T(2,128)S(1)}, f32[2,3,1376]{2,0,1:T(2,128)}, u32[]{:S(2)}) copy-start(f32[2,3,1376]{2,0,1:T(2,128)} %param.12) | copy-start | bytes 99076
  7.6 5.4 %copy-start.4 = (f32[2,3,1376]{2,0,1:T(2,128)S(1)}, f32[2,3,1376]{2,0,1:T(2,128)}, u32[]{:S(2)}) copy-start(f32[2,3,1376]{2,0,1:T(2,128)} %param.11) | copy-start | bytes 99076
  7.6 23.0 %all-to-all-start = ((bf16[4,696,256]{2,1,0:T(8,128)(2,1)}), bf16[4,696,256]{2,1,0:T(8,128)(2,1)S(1)}, u32[]{:S(2)}, u32[]{:S(2)}) async-start(bf16[4,696,256]{2,1,0:T(8,128)(2,1)} %up0.1), calls=%async_computation | async-start | bytes 2850816 | tf_op jit(solution)/shard_map/all_to_all | solution.py:124
  30.6 1.1 copy-start
  53.4 1.7 %collective-permute-start = (bf16[128,1024]{1,0:T(8,128)(2,1)}, bf16[128,1024]{1,0:T(8,128)(2,1)S(1)}, u32[]{:S(2)}, u32[]{:S(2)}) collective-permute-start(bf16[128,1024]{1,0:T(8,128)(2,1)} %get-tuple-element.10), channel_id=1, source_target_pairs={{0,1},{1,0},{2,3},{3,2},{4,5},{5,4},{6,7},{7,6},{8,9},{9,8},{10,11... | collective-permute-start | bytes 786440 | tf_op jit(solution)/shard_map/ppermute | solution.py:130
  56.9 14.2 %all-to-all-start.2 = ((bf16[4,32,1024]{2,1,0:T(8,128)(2,1)}), bf16[4,32,1024]{2,1,0:T(8,128)(2,1)S(1)}, u32[]{:S(2)}, u32[]{:S(2)}) async-start(bf16[4,32,1024]{2,1,0:T(8,128)(2,1)} %bitcast.6), calls=%async_computation.2 | async-start | bytes 524288 | tf_op jit(solution)/shard_map/all_to_all | solution.py:127
  82.7 1.5 copy-start.1
  82.7 1.5 collective-permute-start.1
  84.2 0.7 copy-start.2
  135.5 1.7 %collective-permute-start.2 = (bf16[128,1024]{1,0:T(8,128)(2,1)}, bf16[128,1024]{1,0:T(8,128)(2,1)S(1)}, u32[]{:S(2)}, u32[]{:S(2)}) collective-permute-start(bf16[128,1024]{1,0:T(8,128)(2,1)} %get-tuple-element.12), channel_id=1, source_target_pairs={{0,1},{1,0},{2,3},{3,2},{4,5},{5,4},{6,7},{7,6},{8,9},{9,8},{10,11... | collective-permute-start | bytes 786440 | tf_op jit(solution)/shard_map/ppermute | solution.py:130
  161.3 1.5 collective-permute-start.3

commit v3 on v0

v3 whole, which is shorter than its diff:
```python
import jax
import jax.numpy as jnp
from jax import lax
from jax.experimental import pallas as pl
from jax.experimental.pallas import tpu as pltpu
from jax.sharding import PartitionSpec as P


epsilon = 1e-06
F32 = jnp.float32
BF16 = jnp.bfloat16
EXTRA = 8
SPLITS = 2
MIB = 1 << 20
WIDE = 16
VMEM = pl.BlockSpec(memory_space=pltpu.VMEM)
SMEM = pl.BlockSpec(memory_space=pltpu.SMEM)
HBM = pl.BlockSpec(memory_space=pltpu.HBM)


def call(body, args, specs, shapes, flops, moved, scratch=(), room=16):
    return pl.pallas_call(
        body,
        in_specs=specs,
        out_specs=[VMEM] * len(shapes),
        out_shape=[jax.ShapeDtypeStruct(*shape) for shape in shapes],
        scratch_shapes=scratch,
        cost_estimate=pl.CostEstimate(
            flops=int(flops), bytes_accessed=int(moved), transcendentals=0
        ),
        compiler_params=pltpu.CompilerParams(vmem_limit_bytes=room * MIB),
    )(*args)


def aligned(value, step=8):
    return pl.multiple_of(value, step)


def prepare(current, gain, scaled_ref, tail_ref):
    scaled_ref[...] = (current * gain).astype(BF16)
    squares = current * current
    folded = squares[:, :128]
    for k in range(1, squares.shape[1] // 128):
        folded = folded + squares[:, k * 128 : (k + 1) * 128]
    total = jnp.sum(folded.T, axis=0, keepdims=True)
    high = total.astype(BF16).astype(F32)
    low = total - high
    row = lax.broadcasted_iota(jnp.int32, (EXTRA, total.shape[1]), 0)
    tail_ref[...] = jnp.where(row == 0, high, jnp.where(row == 1, low, 0.0)).astype(BF16)


def load_rows(pieces, side_ref, rows_ref):
    if len(pieces) == 1:
        return pieces[0][...].astype(F32)
    near, far = pieces
    half = near.shape[0]
    side = side_ref[0] & 1
    rows_ref[pl.ds(aligned(side * half, half), half), :] = near[...]
    rows_ref[pl.ds(aligned((1 - side) * half, half), half), :] = far[...]
    return rows_ref[...].astype(F32)


def make_body(mesh):
    n_a = mesh.shape["ra"]
    n_c = mesh.shape["cb"]
    n_z = n_c // 2

    def peer(i, s, n):
        return i ^ s if n & (n - 1) == 0 else (i + s) % n

    def source(i, s, n):
        return i ^ s if n & (n - 1) == 0 else (i - s) % n

    def send_a(value, s):
        return lax.ppermute(value, "ra", [(i, peer(i, s, n_a)) for i in range(n_a)])

    def send_z(value, s):
        pairs = [(z * 2 + k, peer(z, s, n_z) * 2 + k) for z in range(n_z) for k in range(2)]
        return lax.ppermute(value, "cb", pairs)

    def send_core(value):
        return lax.ppermute(value, "cb", [(i, i ^ 1) for i in range(n_c)])

    def body(tokens, norm_gain, gate_weight, value_weight, gate_taps, value_taps, down_weight):
        layers, width, units = gate_weight.shape
        kernel = gate_taps.shape[1]
        count = tokens.shape[0]
        piece = -(-(-(-units // n_a)) // 8) * 8
        step = -(-(-(-piece // SPLITS)) // 8) * 8
        cuts = [(lo, min(step, piece - lo)) for lo in range(0, piece, step)]
        n_h = len(cuts)
        even = n_a * piece == units
        a = lax.axis_index("ra")
        c = lax.axis_index("cb")
        half = count // 2
        span = half // n_z

        def begin(p):
            return jnp.minimum(p * piece, units - piece)

        def scalar(value):
            return value.astype(jnp.int32).reshape(1)

        me_a, me_c = scalar(a), scalar(c)

        def stay(value):
            return pltpu.with_memory_space_constraint(value, pltpu.HBM)

        gate_rows = stay(gate_weight.transpose(0, 2, 1))
        value_rows = stay(value_weight.transpose(0, 2, 1))
        down_rows = stay(down_weight)

        tap_rows = 2 * kernel * layers
        tap_rows += -tap_rows % 8
        tap_args = [gate_taps.transpose(1, 0, 2), value_taps.transpose(1, 0, 2)]

        sends = list(range(n_a - 1, 0, -1))
        order = [(h, s) for h in range(n_h) for s in sends] + [(h, 0) for h in range(n_h)]

        def up(layer, pieces, held):
            outs = {}
            extra = None
            n_p = len(pieces)
            for h, s in order:
                lo, size = cuts[h]
                rows = 2 * size + (EXTRA if h == 0 else 0)
                initial = extra is None
                load = initial and held is None

                def body_fn(*refs, s=s, h=h, lo=lo, size=size, initial=initial, load=load):
                    a_ref, weights = refs[0], list(refs[1:3])
                    at = pl.ds(aligned(begin(peer(a_ref[0], s, n_a)) + lo), size)
                    if load:
                        sem, stored = refs[-1], refs[-4:-2]
                        ahead = begin(peer(a_ref[0], s, n_a))
                        blocks = [pl.ds(aligned(ahead), piece)]
                        for t in range(n_a):
                            if t != s:
                                blocks.append(pl.ds(aligned(begin(peer(a_ref[0], t, n_a))), piece))
                        if not even:
                            blocks = [slice(None)]
                        copies = []
                        for i, block in enumerate(blocks):
                            for k in range(2):
                                copy = pltpu.make_async_copy(
                                    weights[k].at[layer, block], stored[k].at[block], sem.at[2 * i + k]
                                )
                                copy.start()
                                copies.append(copy)
                        weights = stored
                    if initial:
                        sources = refs[3 : 3 + n_p]
                        gain_ref, side_ref = refs[3 + n_p : 5 + n_p]
                        out_ref, scaled_ref, tail_ref = refs[5 + n_p : 8 + n_p]
                        rows_ref = refs[-2] if load else refs[-1]
                        current = load_rows(sources, side_ref, rows_ref)
                        prepare(current, gain_ref[layer : layer + 1, :], scaled_ref, tail_ref)
                    else:
                        scaled_ref, tail_ref, out_ref = refs[3:6]
                    scaled = scaled_ref[...]
                    for k in range(2):
                        if load:
                            copies[k].wait()
                        out_ref[k * size : (k + 1) * size, :] = lax.dot_general(
                            weights[k][at, :],
                            scaled,
                            (((1,), (1,)), ((), ())),
                            preferred_element_type=F32,
                        ).astype(BF16)
                    if h == 0:
                        out_ref[2 * size : 2 * size + EXTRA, :] = tail_ref[...]
                    if load:
                        for copy in copies[2:]:
                            copy.wait()

                if load:
                    args, specs = [me_a, gate_rows, value_rows], [SMEM, HBM, HBM]
                else:
                    args, specs = [me_a, *held], [SMEM, VMEM, VMEM]
                shapes = [((rows, count), BF16)]
                scratch = []
                if initial:
                    args += [*pieces, norm_gain, me_c]
                    specs += [VMEM] * (n_p + 1) + [SMEM]
                    shapes += [((count, width), BF16), ((EXTRA, count), BF16)]
                    scratch = [pltpu.VMEM((count, width), BF16)]
                    if load:
                        shapes += [((units, width), BF16)] * 2
                        scratch += [pltpu.SemaphoreType.DMA((2 * n_a,))]
                else:
                    args += extra
                    specs += [VMEM] * 2
                out = call(
                    body_fn,
                    args,
                    specs,
                    shapes,
                    4 * size * width * count,
                    4 * size * width,
                    scratch,
                    room=WIDE if load else 16,
                )
                if initial:
                    extra = out[1:3]
                if load:
                    held = out[3:5]
                outs[h, s] = out[0]
            return outs

        def fetch(layer, after):
            sources, picks = [down_rows], [layer]
            if layer + 1 < layers:
                sources += [gate_rows, value_rows]
                picks += [layer + 1] * 2
            n = len(sources)
            shapes = [(source.shape[1:], BF16) for source in sources]
            args, specs = [*sources, after], [HBM] * n + [VMEM]
            scratch = [pltpu.SemaphoreType.DMA((n,))]
            if layer == 0:
                args += [me_a, *tap_args]
                specs += [SMEM, VMEM, VMEM]
                shapes.append(((piece, tap_rows), F32))
                scratch.append(pltpu.VMEM((units, tap_rows), F32))

            def body_fn(*refs):
                outs = refs[len(args) : len(args) + len(shapes)]
                sem = refs[len(args) + len(shapes)]
                copies = []
                for k in range(n):
                    copy = pltpu.make_async_copy(refs[k].at[picks[k]], outs[k], sem.at[k])
                    copy.start()
                    copies.append(copy)
                if layer == 0:
                    a_ref, gate_ref, value_ref = refs[n + 1 : n + 4]
                    rows = []
                    for l in range(layers):
                        for ref in (gate_ref, value_ref):
                            rows += [ref[k, l : l + 1, :] for k in range(kernel)]
                    if tap_rows > len(rows):
                        rows.append(jnp.zeros((tap_rows - len(rows), units), F32))
                    held_ref = refs[-1]
                    held_ref[...] = jnp.concatenate(rows, axis=0).T
                    outs[n][...] = held_ref[pl.ds(aligned(begin(a_ref[0])), piece), :]
                for copy in copies:
                    copy.wait()

            return call(
                body_fn,
                args,
                specs,
                shapes,
                2 * units * width * count,
                2 * n * units * width,
                scratch,
            )

        def act(layer, h, parts, inverse, taps):
            lo, size = cuts[h]
            first, last = h == 0, h == n_h - 1
            args = [*parts, taps] + ([] if first else [inverse])
            shapes = [((size, count), BF16)]
            if first and not last:
                shapes.append(((8, count), F32))

            def body_fn(*refs):
                parts_refs, taps_ref = refs[:n_a], refs[n_a]
                out_ref = refs[len(args)]
                total = parts_refs[0][...].astype(F32)
                for ref in parts_refs[1:]:
                    total = total + ref[...].astype(F32)
                if first:
                    tail = total[2 * size :]
                    scale = lax.rsqrt((tail[0:1] + tail[1:2]) / (width * n_a) + epsilon)
                    if not last:
                        refs[len(args) + 1][...] = jnp.broadcast_to(scale, (8, count))
                else:
                    scale = refs[n_a + 1][0:1, :]
                lin = total[: 2 * size] * scale
                lane = lax.broadcasted_iota(jnp.int32, (size, count), 1)

                def conv(kind):
                    result = None
                    for k in range(kernel):
                        shift = kernel - 1 - k
                        column = (layer * 2 + kind) * kernel + k
                        moved = lin[kind * size : (kind + 1) * size]
                        if shift:
                            moved = jnp.where(lane < shift, 0.0, pltpu.roll(moved, shift, 1))
                        term = taps_ref[lo : lo + size, column : column + 1] * moved
                        result = term if result is None else result + term
                    return result

                gate, value = conv(0), conv(1)
                out_ref[...] = (gate / (1.0 + jnp.exp(-gate)) * value).astype(BF16)

            out = call(
                body_fn,
                args,
                [VMEM] * len(args),
                shapes,
                60 * 2 * size * count,
                4 * n_a * size * count,
            )
            return out[0], (out[1] if len(out) > 1 else inverse)

        def term_of(left, weight, keep):
            if keep is not None:
                row = lax.broadcasted_iota(jnp.int32, left.shape, 0)
                left = jnp.where(row >= keep, left.astype(F32), 0.0).astype(BF16)
            return lax.dot_general(
                left, weight, (((0,), (0,)), ((), ())), preferred_element_type=F32
            )

        def down_own(weight, mine):
            def body_fn(weight_ref, a_ref, *refs):
                total = None
                p = a_ref[0]
                for h, (lo, size) in enumerate(cuts):
                    at = pl.ds(aligned(begin(p) + lo), size)
                    keep = None if even else p * piece - begin(p) - lo
                    term = term_of(refs[h][...], weight_ref[at, :], keep)
                    total = term if total is None else total + term
                refs[n_h][...] = total

            return call(
                body_fn,
                [weight, me_a, *mine],
                [VMEM, SMEM] + [VMEM] * n_h,
                [((count, width), F32)],
                2 * piece * width * count,
                2 * piece * width,
            )[0]

        def down(h, weight, total, others):
            lo, size = cuts[h]
            last = h == n_h - 1
            n = len(others)
            shapes = [((count, width), F32)]
            if last:
                shapes = [((half, width), BF16), ((half, width), F32)]

            def body_fn(weight_ref, sum_ref, a_ref, side_ref, *refs):
                total = sum_ref[...]
                for s in range(1, n_a):
                    p = source(a_ref[0], s, n_a)
                    at = pl.ds(aligned(begin(p) + lo), size)
                    keep = None if even else p * piece - begin(p) - lo
                    total = total + term_of(refs[s - 1][...], weight_ref[at, :], keep)
                if not last:
                    refs[n][...] = total
                    return
                away_ref, kept_ref, hold_ref = refs[n:]
                hold_ref[...] = total
                side = side_ref[0] & 1
                away = hold_ref[pl.ds(aligned((1 - side) * half, half), half), :]
                away_ref[...] = away.astype(BF16)
                kept_ref[...] = hold_ref[pl.ds(aligned(side * half, half), half), :]

            return call(
                body_fn,
                [weight, total, me_a, me_c, *others],
                [VMEM] * 2 + [SMEM] * 2 + [VMEM] * n,
                shapes,
                2 * size * (n_a - 1) * width * count,
                2 * size * (n_a - 1) * width,
                [pltpu.VMEM((count, width), F32)] if last else (),
            )

        def deal(kept, came):
            def body_fn(kept_ref, came_ref, z_ref, *refs):
                for s in range(n_z):
                    at = pl.ds(aligned(peer(z_ref[0] >> 1, s, n_z) * span), span)
                    value = kept_ref[at, :] + came_ref[at, :].astype(F32)
                    refs[s][...] = value.astype(refs[s].dtype)

            return call(
                body_fn,
                [kept, came, me_c],
                [VMEM, VMEM, SMEM],
                [((span, width), F32 if s == 0 else BF16) for s in range(n_z)],
                4 * half * width,
                8 * half * width,
            )

        def settle(layer, own, others, old):
            def body_fn(own_ref, *refs):
                at_ref, old_ref, out_ref = refs[-3:]
                branch = own_ref[...]
                for ref in refs[:-3]:
                    branch = branch + ref[...].astype(F32)
                if layer == 0:
                    at = (at_ref[0] & 1) * half + (at_ref[0] >> 1) * span
                    before = old_ref[pl.ds(aligned(at), span), :].astype(F32)
                else:
                    before = old_ref[...].astype(F32)
                out_ref[...] = (0.5 * before + branch).astype(BF16)

            return call(
                body_fn,
                [own, *others, me_c, old],
                [VMEM] * (1 + len(others)) + [SMEM, VMEM],
                [((span, width), BF16)],
                8 * span * width,
                8 * span * width,
            )[0]

        def gather(parts):
            def body_fn(*refs):
                z_ref, out_ref = refs[n_z:]
                for s in range(n_z):
                    at = pl.ds(aligned(source(z_ref[0] >> 1, s, n_z) * span), span)
                    out_ref[at, :] = refs[s][...]

            return call(
                body_fn,
                [*parts, me_c],
                [VMEM] * n_z + [SMEM],
                [((half, width), BF16)],
                half * width,
                4 * half * width,
            )[0]

        pieces = [tokens]
        old = tokens
        held = None
        for layer in range(layers):
            outs = up(layer, pieces, held)
            weight, *held = fetch(layer, outs[n_h - 1, 0])
            if layer == 0:
                *held, taps = held
            inverse = None
            mine, others = [], []
            for h in range(n_h):
                parts = [outs[h, 0]]
                parts += [send_a(outs[h, s], s) for s in range(1, n_a)]
                hidden, inverse = act(layer, h, parts, inverse, taps)
                mine.append(hidden)
                others.append([send_a(hidden, s) for s in range(1, n_a)])
            total = down_own(weight, mine)
            for h in range(n_h):
                out = down(h, weight, total, others[h])
                total = out[0]
            away, kept = out
            dealt = deal(kept, send_core(away))
            came = [send_z(dealt[s], s) for s in range(1, n_z)]
            old = settle(layer, dealt[0], came, old)
            near = gather([old] + [send_z(old, s) for s in range(1, n_z)])
            pieces = [near, send_core(near)]

        def join(near_ref, far_ref, side_ref, out_ref):
            side = side_ref[0] & 1
            out_ref[pl.ds(aligned(side * half, half), half), :] = near_ref[...]
            out_ref[pl.ds(aligned((1 - side) * half, half), half), :] = far_ref[...]

        return call(
            join,
            [*pieces, me_c],
            [VMEM, VMEM, SMEM],
            [((count, width), BF16)],
            count * width,
            4 * count * width,
        )[0]

    return body


def solution(mesh):
    return jax.shard_map(
        make_body(mesh),
        mesh=mesh,
        in_specs=(
            P(None, "ra"),
            P(None, "ra"),
            P(None, "ra", "cb"),
            P(None, "ra", "cb"),
            P(None, None, "cb"),
            P(None, None, "cb"),
            P(None, "cb", "ra"),
        ),
        out_specs=P(None, "ra"),
        check_vma=False,
    )
```

time: 334 us -> 111 us (0.33)
  waiting for transfers between devices: 262 us -> 37.5 us
  starting transfers between devices: 0.13 us -> 48.9 us
  matrix products: 28 us -> 0 us
  Pallas kernels: 0 us -> 21.8 us
  blocking collectives: 21.6 us -> 0 us
  between operations: 13.2 us -> 0.41 us
  other arithmetic: 7.81 us -> 0 us
    psum x4 -> x0, waiting for transfers between devices: 262 us -> none  [the longest x2 143 us: body(): gate_sum, value_sum = lax.psum((gate_part, value_part), 'ra')]
    ppermute x0 -> x40, starting transfers between devices: none -> 48.9 us  [the longest x24 30.8 us: send_a(): return lax.ppermute(value, 'ra', [(i, peer(i, s, n_a)) for i in range(n_a)])]
    ppermute x0 -> x40, waiting for transfers between devices: none -> 37.5 us  [the longest x12 18.9 us: send_z(): return lax.ppermute(value, 'cb', pairs)]
    dot_general x6 -> x0, matrix products: 28 us -> none  [the longest x2 12.5 us: body(): jnp.dot(hidden, down_weight[layer_index], preferred_element_type=jnp.floa...]
    pallas_call x0 -> x35, Pallas kernels: none -> 21.8 us  [call(): pl.pallas_call(body, in_specs=specs, out_specs=[VMEM] * len(shapes), out_...]
    psum x2 -> x0, blocking collectives: 21.6 us -> none  [body(): total_squares = lax.psum(local_squares, 'ra')]
    mul x2 -> x0, other arithmetic: 3.92 us -> none  [body(): gate_conv = causal_conv(gate_sum * inverse_rms, gate_taps[layer_index])]
  transfers between devices with their start and end apart: 4 -> 40, of which waited for: 4 -> 22; matrix products, arithmetic and copies ran while one was open for 0% -> 0% of each run, Pallas kernels for 0% -> 14%
where the time goes in v3:
time: 111 us
  starting transfers between devices  48.9 us (44%)
  waiting for transfers between devices  37.5 us (34%)
  Pallas kernels  21.8 us (20%)
  local copies, waits for them, and re-layouts  1.88 us (2%)
    ppermute x24, starting transfers between devices, send_a(): return lax.ppermute(value, 'ra', [(i, peer(i, s, n_a)) for i in range(n_a)])  30.8 us
    pallas_call x35, Pallas kernels, call(): pl.pallas_call(body, in_specs=specs, out_specs=[VMEM] * len(shapes), out_...  21.8 us
    ppermute x12, waiting for transfers between devices, send_z(): return lax.ppermute(value, 'cb', pairs)  18.9 us
    ppermute x12, starting transfers between devices, send_z(): return lax.ppermute(value, 'cb', pairs)  17.8 us
    ppermute x24, waiting for transfers between devices, send_a(): return lax.ppermute(value, 'ra', [(i, peer(i, s, n_a)) for i in range(n_a)])  12.5 us
    ppermute x4, waiting for transfers between devices, send_core(): return lax.ppermute(value, 'cb', [(i, i ^ 1) for i in range(n_c)])  6.09 us
  transfers between devices with their start and end apart: 40, of which 22 were waited for; matrix products, arithmetic and copies ran while one was open for 0% of the time, Pallas kernels for 14%

profile of v3, /device:TPU:0, one launch (start us, length us, event | category | flops | bytes accessed | tf_op | source)
XLA Modules:
  0.0 110.5 jit_solution(12934165534162358885)
XLA Ops:
  1.7 2.8 %shard_map.73 = (bf16[360,256]{1,0:T(8,128)(2,1)S(1)}, bf16[256,1024]{1,0:T(8,128)(2,1)S(1)}, bf16[8,256]{1,0:T(8,128)(2,1)S(1)}, bf16[1376,1024]{1,0:T(8,128)(2,1)S(1)}, bf16[1376,1024]{1,0:T(8,128)(2,1)S(1)}) custom-call(s32[1]{0:T(128)} %bitcast.refs_0_.refs_4_.a_ref, bf16[2,1376,1024]{2,1,0:T(8,128)(2,1)} %bitcast.8, bf16[2,1376,1024]{2,1,0:T(8,128)(2,1)} %bitcast.10, ...), custom_call_target="tpu_custom_call" | custom-call | flops 184549376 | bytes 720896 | tf_op jit(solution)/shard_map/pallas_call | solution.py:22
  5.1 3.1 %collective-permute-start.1 = (bf16[360,256]{1,0:T(8,128)(2,1)S(1)}, bf16[360,256]{1,0:T(8,128)(2,1)S(1)}, u32[]{:S(2)}, u32[]{:S(2)}) collective-permute-start(bf16[360,256]{1,0:T(8,128)(2,1)S(1)} %shard_map.78), channel_id=1, source_target_pairs={{0,16},{8,24},{16,0},{24,8},{1,17},{9,25},{17,1},{25,9},{2,18},{10... | collective-permute-start | bytes 552968 | tf_op jit(solution)/shard_map/ppermute | solution.py:75
  8.6 1.6 %collective-permute-start = (bf16[360,256]{1,0:T(8,128)(2,1)S(1)}, bf16[360,256]{1,0:T(8,128)(2,1)S(1)}, u32[]{:S(2)}, u32[]{:S(2)}) collective-permute-start(bf16[360,256]{1,0:T(8,128)(2,1)S(1)} %shard_map.77), channel_id=1, source_target_pairs={{0,8},{8,0},{16,24},{24,16},{1,9},{9,1},{17,25},{25,17},{2,10},{10... | collective-permute-start | bytes 552968 | tf_op jit(solution)/shard_map/ppermute | solution.py:75
  10.7 3.0 %collective-permute-start.5 = (bf16[336,256]{1,0:T(8,128)(2,1)S(1)}, bf16[336,256]{1,0:T(8,128)(2,1)S(1)}, u32[]{:S(2)}, u32[]{:S(2)}) collective-permute-start(bf16[336,256]{1,0:T(8,128)(2,1)S(1)} %shard_map.82), channel_id=1, source_target_pairs={{0,24},{8,16},{16,8},{24,0},{1,25},{9,17},{17,9},{25,1},{2,26},{10... | collective-permute-start | bytes 516104 | tf_op jit(solution)/shard_map/ppermute | solution.py:75
  16.5 3.5 %shard_map.75 = (bf16[1376,1024]{1,0:T(8,128)(2,1)S(1)}, bf16[1376,1024]{1,0:T(8,128)(2,1)S(1)}, bf16[1376,1024]{1,0:T(8,128)(2,1)S(1)}, f32[344,16]{1,0:T(8,128)S(1)}) custom-call(bf16[2,1376,1024]{2,1,0:T(8,128)(2,1)} %refs_0_.3, bf16[2,1376,1024]{2,1,0:T(8,128)(2,1)} %bitcast.9, bf16[2,1376,1024]{2,1,0:T(8,128)(2,1)} %bitcast.11, ...), custom_call_target="tpu_custom_call" | custom-call | flops 721420288 | bytes 8454144 | tf_op jit(solution)/shard_map/pallas_call | solution.py:22
  20.5 1.9 %collective-permute-start.6 = (bf16[176,256]{1,0:T(8,128)(2,1)S(1)}, bf16[176,256]{1,0:T(8,128)(2,1)S(1)}, u32[]{:S(2)}, u32[]{:S(2)}) collective-permute-start(bf16[176,256]{1,0:T(8,128)(2,1)S(1)} %get-tuple-element.42.refs_0_), channel_id=1, source_target_pairs={{0,8},{8,0},{16,24},{24,16},{1,9},{9,1},{17,25},{25,17},{2,10},{10... | collective-permute-start | bytes 270344 | tf_op jit(solution)/shard_map/ppermute | solution.py:75
  22.4 1.5 %collective-permute-start.7 = (bf16[176,256]{1,0:T(8,128)(2,1)S(1)}, bf16[176,256]{1,0:T(8,128)(2,1)S(1)}, u32[]{:S(2)}, u32[]{:S(2)}) collective-permute-start(bf16[176,256]{1,0:T(8,128)(2,1)S(1)} %get-tuple-element.42.refs_0_), channel_id=1, source_target_pairs={{0,16},{8,24},{16,0},{24,8},{1,17},{9,25},{17,1},{25,9},{2,18},{10... | collective-permute-start | bytes 270344 | tf_op jit(solution)/shard_map/ppermute | solution.py:75
  23.9 2.3 %collective-permute-start.8 = (bf16[176,256]{1,0:T(8,128)(2,1)S(1)}, bf16[176,256]{1,0:T(8,128)(2,1)S(1)}, u32[]{:S(2)}, u32[]{:S(2)}) collective-permute-start(bf16[176,256]{1,0:T(8,128)(2,1)S(1)} %get-tuple-element.42.refs_0_), channel_id=1, source_target_pairs={{0,24},{8,16},{16,8},{24,0},{1,25},{9,17},{17,9},{25,1},{2,26},{10... | collective-permute-start | bytes 270344 | tf_op jit(solution)/shard_map/ppermute | solution.py:75
  28.1 2.8 %collective-permute-start.11 = (bf16[168,256]{1,0:T(8,128)(2,1)S(1)}, bf16[168,256]{1,0:T(8,128)(2,1)S(1)}, u32[]{:S(2)}, u32[]{:S(2)}) collective-permute-start(bf16[168,256]{1,0:T(8,128)(2,1)S(1)} %shard_map.83.refs_1_), channel_id=1, source_target_pairs={{0,24},{8,16},{16,8},{24,0},{1,25},{9,17},{17,9},{25,1},{2,26},{10... | collective-permute-start | bytes 258056 | tf_op jit(solution)/shard_map/ppermute | solution.py:75
  33.5 2.0 %collective-permute-done.9.refs_0_ = bf16[168,256]{1,0:T(8,128)(2,1)S(1)} collective-permute-done((bf16[168,256]{1,0:T(8,128)(2,1)S(1)}, bf16[168,256]{1,0:T(8,128)(2,1)S(1)}, u32[]{:S(2)}, u32[]{:S(2)}) %collective-permute-start.9) | collective-permute-done | bytes 86048 | tf_op jit(solution)/shard_map/ppermute | solution.py:75
  36.3 1.5 %collective-permute-done.12.came_ref = bf16[128,1024]{1,0:T(8,128)(2,1)S(1)} collective-permute-done((bf16[128,1024]{1,0:T(8,128)(2,1)S(1)}, bf16[128,1024]{1,0:T(8,128)(2,1)S(1)}, u32[]{:S(2)}, u32[]{:S(2)}) %collective-permute-start.12) | collective-permute-done | bytes 262176 | tf_op jit(solution)/shard_map/ppermute | solution.py:82
  37.8 1.6 %collective-permute-start.13 = (bf16[32,1024]{1,0:T(8,128)(2,1)S(1)}, bf16[32,1024]{1,0:T(8,128)(2,1)S(1)}, u32[]{:S(2)}, u32[]{:S(2)}) collective-permute-start(bf16[32,1024]{1,0:T(8,128)(2,1)S(1)} %get-tuple-element.47), channel_id=1, source_target_pairs={{0,2},{1,3},{2,0},{3,1},{4,6},{5,7},{6,4},{7,5},{8,10},{9,11},{10,... | collective-permute-start | bytes 196616 | tf_op jit(solution)/shard_map/ppermute | solution.py:79
  39.5 2.6 %collective-permute-start.14 = (bf16[32,1024]{1,0:T(8,128)(2,1)S(1)}, bf16[32,1024]{1,0:T(8,128)(2,1)S(1)}, u32[]{:S(2)}, u32[]{:S(2)}) collective-permute-start(bf16[32,1024]{1,0:T(8,128)(2,1)S(1)} %get-tuple-element.48), channel_id=1, source_target_pairs={{0,4},{1,5},{2,6},{3,7},{4,0},{5,1},{6,2},{7,3},{8,12},{9,13},{10,... | collective-permute-start | bytes 196616 | tf_op jit(solution)/shard_map/ppermute | solution.py:79
  42.3 4.7 %collective-permute-done.14.refs_1_ = bf16[32,1024]{1,0:T(8,128)(2,1)S(1)} collective-permute-done((bf16[32,1024]{1,0:T(8,128)(2,1)S(1)}, bf16[32,1024]{1,0:T(8,128)(2,1)S(1)}, u32[]{:S(2)}, u32[]{:S(2)}) %collective-permute-start.14) | collective-permute-done | bytes 65568 | tf_op jit(solution)/shard_map/ppermute | solution.py:79
  49.2 1.7 %collective-permute-start.17 = (bf16[32,1024]{1,0:T(8,128)(2,1)S(1)}, bf16[32,1024]{1,0:T(8,128)(2,1)S(1)}, u32[]{:S(2)}, u32[]{:S(2)}) collective-permute-start(bf16[32,1024]{1,0:T(8,128)(2,1)S(1)} %shard_map.88.refs_0_.refs_4_), channel_id=1, source_target_pairs={{0,4},{1,5},{2,6},{3,7},{4,0},{5,1},{6,2},{7,3},{8,12},{9,13},{10,... | collective-permute-start | bytes 196616 | tf_op jit(solution)/shard_map/ppermute | solution.py:79
  50.9 1.8 %collective-permute-start.18 = (bf16[32,1024]{1,0:T(8,128)(2,1)S(1)}, bf16[32,1024]{1,0:T(8,128)(2,1)S(1)}, u32[]{:S(2)}, u32[]{:S(2)}) collective-permute-start(bf16[32,1024]{1,0:T(8,128)(2,1)S(1)} %shard_map.88.refs_0_.refs_4_), channel_id=1, source_target_pairs={{0,6},{1,7},{2,4},{3,5},{4,2},{5,3},{6,0},{7,1},{8,14},{9,15},{10,... | collective-permute-start | bytes 196616 | tf_op jit(solution)/shard_map/ppermute | solution.py:79
  52.8 2.6 %collective-permute-done.17.refs_2_ = bf16[32,1024]{1,0:T(8,128)(2,1)S(1)} collective-permute-done((bf16[32,1024]{1,0:T(8,128)(2,1)S(1)}, bf16[32,1024]{1,0:T(8,128)(2,1)S(1)}, u32[]{:S(2)}, u32[]{:S(2)}) %collective-permute-start.17) | collective-permute-done | bytes 65568 | tf_op jit(solution)/shard_map/ppermute | solution.py:79
  55.4 1.6 %collective-permute-done.18.refs_3_ = bf16[32,1024]{1,0:T(8,128)(2,1)S(1)} collective-permute-done((bf16[32,1024]{1,0:T(8,128)(2,1)S(1)}, bf16[32,1024]{1,0:T(8,128)(2,1)S(1)}, u32[]{:S(2)}, u32[]{:S(2)}) %collective-permute-start.18) | collective-permute-done | bytes 65568 | tf_op jit(solution)/shard_map/ppermute | solution.py:79
  57.1 1.5 %collective-permute-done.19.refs_4_ = bf16[128,1024]{1,0:T(8,128)(2,1)S(1)} collective-permute-done((bf16[128,1024]{1,0:T(8,128)(2,1)S(1)}, bf16[128,1024]{1,0:T(8,128)(2,1)S(1)}, u32[]{:S(2)}, u32[]{:S(2)}) %collective-permute-start.19) | collective-permute-done | bytes 262176 | tf_op jit(solution)/shard_map/ppermute | solution.py:82
  61.8 2.0 %collective-permute-start.22 = (bf16[360,256]{1,0:T(8,128)(2,1)S(1)}, bf16[360,256]{1,0:T(8,128)(2,1)S(1)}, u32[]{:S(2)}, u32[]{:S(2)}) collective-permute-start(bf16[360,256]{1,0:T(8,128)(2,1)S(1)} %get-tuple-element.52), channel_id=1, source_target_pairs={{0,24},{8,16},{16,8},{24,0},{1,25},{9,17},{17,9},{25,1},{2,26},{10... | collective-permute-start | bytes 552968 | tf_op jit(solution)/shard_map/ppermute | solution.py:75
  65.7 1.5 %collective-permute-start.24 = (bf16[336,256]{1,0:T(8,128)(2,1)S(1)}, bf16[336,256]{1,0:T(8,128)(2,1)S(1)}, u32[]{:S(2)}, u32[]{:S(2)}) collective-permute-start(bf16[336,256]{1,0:T(8,128)(2,1)S(1)} %shard_map.98), channel_id=1, source_target_pairs={{0,16},{8,24},{16,0},{24,8},{1,17},{9,25},{17,1},{25,9},{2,18},{10... | collective-permute-start | bytes 516104 | tf_op jit(solution)/shard_map/ppermute | solution.py:75
  69.4 3.9 %collective-permute-done.22.refs_3_ = bf16[360,256]{1,0:T(8,128)(2,1)S(1)} collective-permute-done((bf16[360,256]{1,0:T(8,128)(2,1)S(1)}, bf16[360,256]{1,0:T(8,128)(2,1)S(1)}, u32[]{:S(2)}, u32[]{:S(2)}) %collective-permute-start.22) | collective-permute-done | bytes 184352 | tf_op jit(solution)/shard_map/ppermute | solution.py:75
  75.3 1.7 %collective-permute-done.25.refs_3_ = bf16[336,256]{1,0:T(8,128)(2,1)S(1)} collective-permute-done((bf16[336,256]{1,0:T(8,128)(2,1)S(1)}, bf16[336,256]{1,0:T(8,128)(2,1)S(1)}, u32[]{:S(2)}, u32[]{:S(2)}) %collective-permute-start.25) | collective-permute-done | bytes 172064 | tf_op jit(solution)/shard_map/ppermute | solution.py:75
  81.1 1.5 %collective-permute-start.30 = (bf16[168,256]{1,0:T(8,128)(2,1)S(1)}, bf16[168,256]{1,0:T(8,128)(2,1)S(1)}, u32[]{:S(2)}, u32[]{:S(2)}) collective-permute-start(bf16[168,256]{1,0:T(8,128)(2,1)S(1)} %shard_map.100.refs_1_), channel_id=1, source_target_pairs={{0,16},{8,24},{16,0},{24,8},{1,17},{9,25},{17,1},{25,9},{2,18},{10... | collective-permute-start | bytes 258056 | tf_op jit(solution)/shard_map/ppermute | solution.py:75
  83.7 1.8 %shard_map.92.weight_ref = bf16[1376,1024]{1,0:T(8,128)(2,1)S(1)} custom-call(bf16[2,1376,1024]{2,1,0:T(8,128)(2,1)} %refs_0_.3, bf16[336,256]{1,0:T(8,128)(2,1)S(1)} %shard_map.91.refs_1_.refs_0_), custom_call_target="tpu_custom_call" | custom-call | flops 721420288 | bytes 2818048 | tf_op jit(solution)/shard_map/pallas_call | solution.py:22
  88.8 1.5 %collective-permute-done.32.came_ref = bf16[128,1024]{1,0:T(8,128)(2,1)S(1)} collective-permute-done((bf16[128,1024]{1,0:T(8,128)(2,1)S(1)}, bf16[128,1024]{1,0:T(8,128)(2,1)S(1)}, u32[]{:S(2)}, u32[]{:S(2)}) %collective-permute-start.32) | collective-permute-done | bytes 262176 | tf_op jit(solution)/shard_map/ppermute | solution.py:82
  90.4 2.5 %collective-permute-start.34 = (bf16[32,1024]{1,0:T(8,128)(2,1)S(1)}, bf16[32,1024]{1,0:T(8,128)(2,1)S(1)}, u32[]{:S(2)}, u32[]{:S(2)}) collective-permute-start(bf16[32,1024]{1,0:T(8,128)(2,1)S(1)} %get-tuple-element.59), channel_id=1, source_target_pairs={{0,4},{1,5},{2,6},{3,7},{4,0},{5,1},{6,2},{7,3},{8,12},{9,13},{10,... | collective-permute-start | bytes 196616 | tf_op jit(solution)/shard_map/ppermute | solution.py:79
  92.9 1.9 %collective-permute-start.35 = (bf16[32,1024]{1,0:T(8,128)(2,1)S(1)}, bf16[32,1024]{1,0:T(8,128)(2,1)S(1)}, u32[]{:S(2)}, u32[]{:S(2)}) collective-permute-start(bf16[32,1024]{1,0:T(8,128)(2,1)S(1)} %get-tuple-element.60), channel_id=1, source_target_pairs={{0,6},{1,7},{2,4},{3,5},{4,2},{5,3},{6,0},{7,1},{8,14},{9,15},{10,... | collective-permute-start | bytes 196616 | tf_op jit(solution)/shard_map/ppermute | solution.py:79
  95.7 2.7 %collective-permute-done.34.refs_1_ = bf16[32,1024]{1,0:T(8,128)(2,1)S(1)} collective-permute-done((bf16[32,1024]{1,0:T(8,128)(2,1)S(1)}, bf16[32,1024]{1,0:T(8,128)(2,1)S(1)}, u32[]{:S(2)}, u32[]{:S(2)}) %collective-permute-start.34) | collective-permute-done | bytes 65568 | tf_op jit(solution)/shard_map/ppermute | solution.py:79
  101.9 1.7 %collective-permute-start.38 = (bf16[32,1024]{1,0:T(8,128)(2,1)S(1)}, bf16[32,1024]{1,0:T(8,128)(2,1)S(1)}, u32[]{:S(2)}, u32[]{:S(2)}) collective-permute-start(bf16[32,1024]{1,0:T(8,128)(2,1)S(1)} %shard_map.105.refs_0_), channel_id=1, source_target_pairs={{0,6},{1,7},{2,4},{3,5},{4,2},{5,3},{6,0},{7,1},{8,14},{9,15},{10,... | collective-permute-start | bytes 196616 | tf_op jit(solution)/shard_map/ppermute | solution.py:79
  103.6 3.8 %collective-permute-done.37.refs_2_ = bf16[32,1024]{1,0:T(8,128)(2,1)S(1)} collective-permute-done((bf16[32,1024]{1,0:T(8,128)(2,1)S(1)}, bf16[32,1024]{1,0:T(8,128)(2,1)S(1)}, u32[]{:S(2)}, u32[]{:S(2)}) %collective-permute-start.37) | collective-permute-done | bytes 65568 | tf_op jit(solution)/shard_map/ppermute | solution.py:79
  108.2 1.5 %collective-permute-done.39.far_ref = bf16[128,1024]{1,0:T(8,128)(2,1)S(1)} collective-permute-done((bf16[128,1024]{1,0:T(8,128)(2,1)S(1)}, bf16[128,1024]{1,0:T(8,128)(2,1)S(1)}, u32[]{:S(2)}, u32[]{:S(2)}) %collective-permute-start.39) | collective-permute-done | bytes 262176 | tf_op jit(solution)/shard_map/ppermute | solution.py:82
  (95 shorter events, 38.0 us)
Async XLA Ops:
  5.1 10.7 %collective-permute-start.1 = (bf16[360,256]{1,0:T(8,128)(2,1)S(1)}, bf16[360,256]{1,0:T(8,128)(2,1)S(1)}, u32[]{:S(2)}, u32[]{:S(2)}) collective-permute-start(bf16[360,256]{1,0:T(8,128)(2,1)S(1)} %shard_map.78), channel_id=1, source_target_pairs={{0,16},{8,24},{16,0},{24,8},{1,17},{9,25},{17,1},{25,9},{2,18},{10... | collective-permute-start | bytes 552968 | tf_op jit(solution)/shard_map/ppermute | solution.py:75
  8.6 11.4 %collective-permute-start = (bf16[360,256]{1,0:T(8,128)(2,1)S(1)}, bf16[360,256]{1,0:T(8,128)(2,1)S(1)}, u32[]{:S(2)}, u32[]{:S(2)}) collective-permute-start(bf16[360,256]{1,0:T(8,128)(2,1)S(1)} %shard_map.77), channel_id=1, source_target_pairs={{0,8},{8,0},{16,24},{24,16},{1,9},{9,1},{17,25},{25,17},{2,10},{10... | collective-permute-start | bytes 552968 | tf_op jit(solution)/shard_map/ppermute | solution.py:75
  10.2 9.9 %collective-permute-start.2 = (bf16[360,256]{1,0:T(8,128)(2,1)S(1)}, bf16[360,256]{1,0:T(8,128)(2,1)S(1)}, u32[]{:S(2)}, u32[]{:S(2)}) collective-permute-start(bf16[360,256]{1,0:T(8,128)(2,1)S(1)} %get-tuple-element.40), channel_id=1, source_target_pairs={{0,24},{8,16},{16,8},{24,0},{1,25},{9,17},{17,9},{25,1},{2,26},{10... | collective-permute-start | bytes 552968 | tf_op jit(solution)/shard_map/ppermute | solution.py:75
  10.7 13.3 %collective-permute-start.5 = (bf16[336,256]{1,0:T(8,128)(2,1)S(1)}, bf16[336,256]{1,0:T(8,128)(2,1)S(1)}, u32[]{:S(2)}, u32[]{:S(2)}) collective-permute-start(bf16[336,256]{1,0:T(8,128)(2,1)S(1)} %shard_map.82), channel_id=1, source_target_pairs={{0,24},{8,16},{16,8},{24,0},{1,25},{9,17},{17,9},{25,1},{2,26},{10... | collective-permute-start | bytes 516104 | tf_op jit(solution)/shard_map/ppermute | solution.py:75
  14.1 12.1 %collective-permute-start.4 = (bf16[336,256]{1,0:T(8,128)(2,1)S(1)}, bf16[336,256]{1,0:T(8,128)(2,1)S(1)}, u32[]{:S(2)}, u32[]{:S(2)}) collective-permute-start(bf16[336,256]{1,0:T(8,128)(2,1)S(1)} %shard_map.81), channel_id=1, source_target_pairs={{0,16},{8,24},{16,0},{24,8},{1,17},{9,25},{17,1},{25,9},{2,18},{10... | collective-permute-start | bytes 516104 | tf_op jit(solution)/shard_map/ppermute | solution.py:75
  15.7 11.8 %collective-permute-start.3 = (bf16[336,256]{1,0:T(8,128)(2,1)S(1)}, bf16[336,256]{1,0:T(8,128)(2,1)S(1)}, u32[]{:S(2)}, u32[]{:S(2)}) collective-permute-start(bf16[336,256]{1,0:T(8,128)(2,1)S(1)} %shard_map.80), channel_id=1, source_target_pairs={{0,8},{8,0},{16,24},{24,16},{1,9},{9,1},{17,25},{25,17},{2,10},{10... | collective-permute-start | bytes 516104 | tf_op jit(solution)/shard_map/ppermute | solution.py:75
  20.5 10.5 %collective-permute-start.6 = (bf16[176,256]{1,0:T(8,128)(2,1)S(1)}, bf16[176,256]{1,0:T(8,128)(2,1)S(1)}, u32[]{:S(2)}, u32[]{:S(2)}) collective-permute-start(bf16[176,256]{1,0:T(8,128)(2,1)S(1)} %get-tuple-element.42.refs_0_), channel_id=1, source_target_pairs={{0,8},{8,0},{16,24},{24,16},{1,9},{9,1},{17,25},{25,17},{2,10},{10... | collective-permute-start | bytes 270344 | tf_op jit(solution)/shard_map/ppermute | solution.py:75
  22.4 9.6 %collective-permute-start.7 = (bf16[176,256]{1,0:T(8,128)(2,1)S(1)}, bf16[176,256]{1,0:T(8,128)(2,1)S(1)}, u32[]{:S(2)}, u32[]{:S(2)}) collective-permute-start(bf16[176,256]{1,0:T(8,128)(2,1)S(1)} %get-tuple-element.42.refs_0_), channel_id=1, source_target_pairs={{0,16},{8,24},{16,0},{24,8},{1,17},{9,25},{17,1},{25,9},{2,18},{10... | collective-permute-start | bytes 270344 | tf_op jit(solution)/shard_map/ppermute | solution.py:75
  23.9 8.1 %collective-permute-start.8 = (bf16[176,256]{1,0:T(8,128)(2,1)S(1)}, bf16[176,256]{1,0:T(8,128)(2,1)S(1)}, u32[]{:S(2)}, u32[]{:S(2)}) collective-permute-start(bf16[176,256]{1,0:T(8,128)(2,1)S(1)} %get-tuple-element.42.refs_0_), channel_id=1, source_target_pairs={{0,24},{8,16},{16,8},{24,0},{1,25},{9,17},{17,9},{25,1},{2,26},{10... | collective-permute-start | bytes 270344 | tf_op jit(solution)/shard_map/ppermute | solution.py:75
  28.0 4.7 %collective-permute-start.10 = (bf16[168,256]{1,0:T(8,128)(2,1)S(1)}, bf16[168,256]{1,0:T(8,128)(2,1)S(1)}, u32[]{:S(2)}, u32[]{:S(2)}) collective-permute-start(bf16[168,256]{1,0:T(8,128)(2,1)S(1)} %shard_map.83.refs_1_), channel_id=1, source_target_pairs={{0,16},{8,24},{16,0},{24,8},{1,17},{9,25},{17,1},{25,9},{2,18},{10... | collective-permute-start | bytes 258056 | tf_op jit(solution)/shard_map/ppermute | solution.py:75
  28.1 5.4 %collective-permute-start.11 = (bf16[168,256]{1,0:T(8,128)(2,1)S(1)}, bf16[168,256]{1,0:T(8,128)(2,1)S(1)}, u32[]{:S(2)}, u32[]{:S(2)}) collective-permute-start(bf16[168,256]{1,0:T(8,128)(2,1)S(1)} %shard_map.83.refs_1_), channel_id=1, source_target_pairs={{0,24},{8,16},{16,8},{24,0},{1,25},{9,17},{17,9},{25,1},{2,26},{10... | collective-permute-start | bytes 258056 | tf_op jit(solution)/shard_map/ppermute | solution.py:75
  39.5 7.5 %collective-permute-start.14 = (bf16[32,1024]{1,0:T(8,128)(2,1)S(1)}, bf16[32,1024]{1,0:T(8,128)(2,1)S(1)}, u32[]{:S(2)}, u32[]{:S(2)}) collective-permute-start(bf16[32,1024]{1,0:T(8,128)(2,1)S(1)} %get-tuple-element.48), channel_id=1, source_target_pairs={{0,4},{1,5},{2,6},{3,7},{4,0},{5,1},{6,2},{7,3},{8,12},{9,13},{10,... | collective-permute-start | bytes 196616 | tf_op jit(solution)/shard_map/ppermute | solution.py:79
  42.1 6.2 %collective-permute-start.15 = (bf16[32,1024]{1,0:T(8,128)(2,1)S(1)}, bf16[32,1024]{1,0:T(8,128)(2,1)S(1)}, u32[]{:S(2)}, u32[]{:S(2)}) collective-permute-start(bf16[32,1024]{1,0:T(8,128)(2,1)S(1)} %get-tuple-element.49), channel_id=1, source_target_pairs={{0,6},{1,7},{2,4},{3,5},{4,2},{5,3},{6,0},{7,1},{8,14},{9,15},{10,... | collective-permute-start | bytes 196616 | tf_op jit(solution)/shard_map/ppermute | solution.py:79
  49.2 6.2 %collective-permute-start.17 = (bf16[32,1024]{1,0:T(8,128)(2,1)S(1)}, bf16[32,1024]{1,0:T(8,128)(2,1)S(1)}, u32[]{:S(2)}, u32[]{:S(2)}) collective-permute-start(bf16[32,1024]{1,0:T(8,128)(2,1)S(1)} %shard_map.88.refs_0_.refs_4_), channel_id=1, source_target_pairs={{0,4},{1,5},{2,6},{3,7},{4,0},{5,1},{6,2},{7,3},{8,12},{9,13},{10,... | collective-permute-start | bytes 196616 | tf_op jit(solution)/shard_map/ppermute | solution.py:79
  50.9 6.1 %collective-permute-start.18 = (bf16[32,1024]{1,0:T(8,128)(2,1)S(1)}, bf16[32,1024]{1,0:T(8,128)(2,1)S(1)}, u32[]{:S(2)}, u32[]{:S(2)}) collective-permute-start(bf16[32,1024]{1,0:T(8,128)(2,1)S(1)} %shard_map.88.refs_0_.refs_4_), channel_id=1, source_target_pairs={{0,6},{1,7},{2,4},{3,5},{4,2},{5,3},{6,0},{7,1},{8,14},{9,15},{10,... | collective-permute-start | bytes 196616 | tf_op jit(solution)/shard_map/ppermute | solution.py:79
  59.7 8.0 %collective-permute-start.21 = (bf16[360,256]{1,0:T(8,128)(2,1)S(1)}, bf16[360,256]{1,0:T(8,128)(2,1)S(1)}, u32[]{:S(2)}, u32[]{:S(2)}) collective-permute-start(bf16[360,256]{1,0:T(8,128)(2,1)S(1)} %shard_map.95), channel_id=1, source_target_pairs={{0,16},{8,24},{16,0},{24,8},{1,17},{9,25},{17,1},{25,9},{2,18},{10... | collective-permute-start | bytes 552968 | tf_op jit(solution)/shard_map/ppermute | solution.py:75
  60.7 8.6 %collective-permute-start.20 = (bf16[360,256]{1,0:T(8,128)(2,1)S(1)}, bf16[360,256]{1,0:T(8,128)(2,1)S(1)}, u32[]{:S(2)}, u32[]{:S(2)}) collective-permute-start(bf16[360,256]{1,0:T(8,128)(2,1)S(1)} %shard_map.94), channel_id=1, source_target_pairs={{0,8},{8,0},{16,24},{24,16},{1,9},{9,1},{17,25},{25,17},{2,10},{10... | collective-permute-start | bytes 552968 | tf_op jit(solution)/shard_map/ppermute | solution.py:75
  61.8 11.6 %collective-permute-start.22 = (bf16[360,256]{1,0:T(8,128)(2,1)S(1)}, bf16[360,256]{1,0:T(8,128)(2,1)S(1)}, u32[]{:S(2)}, u32[]{:S(2)}) collective-permute-start(bf16[360,256]{1,0:T(8,128)(2,1)S(1)} %get-tuple-element.52), channel_id=1, source_target_pairs={{0,24},{8,16},{16,8},{24,0},{1,25},{9,17},{17,9},{25,1},{2,26},{10... | collective-permute-start | bytes 552968 | tf_op jit(solution)/shard_map/ppermute | solution.py:75
  64.8 12.2 %collective-permute-start.25 = (bf16[336,256]{1,0:T(8,128)(2,1)S(1)}, bf16[336,256]{1,0:T(8,128)(2,1)S(1)}, u32[]{:S(2)}, u32[]{:S(2)}) collective-permute-start(bf16[336,256]{1,0:T(8,128)(2,1)S(1)} %shard_map.99), channel_id=1, source_target_pairs={{0,24},{8,16},{16,8},{24,0},{1,25},{9,17},{17,9},{25,1},{2,26},{10... | collective-permute-start | bytes 516104 | tf_op jit(solution)/shard_map/ppermute | solution.py:75
  65.7 13.8 %collective-permute-start.24 = (bf16[336,256]{1,0:T(8,128)(2,1)S(1)}, bf16[336,256]{1,0:T(8,128)(2,1)S(1)}, u32[]{:S(2)}, u32[]{:S(2)}) collective-permute-start(bf16[336,256]{1,0:T(8,128)(2,1)S(1)} %shard_map.98), channel_id=1, source_target_pairs={{0,16},{8,24},{16,0},{24,8},{1,17},{9,25},{17,1},{25,9},{2,18},{10... | collective-permute-start | bytes 516104 | tf_op jit(solution)/shard_map/ppermute | solution.py:75
  67.7 12.0 %collective-permute-start.23 = (bf16[336,256]{1,0:T(8,128)(2,1)S(1)}, bf16[336,256]{1,0:T(8,128)(2,1)S(1)}, u32[]{:S(2)}, u32[]{:S(2)}) collective-permute-start(bf16[336,256]{1,0:T(8,128)(2,1)S(1)} %shard_map.97), channel_id=1, source_target_pairs={{0,8},{8,0},{16,24},{24,16},{1,9},{9,1},{17,25},{25,17},{2,10},{10... | collective-permute-start | bytes 516104 | tf_op jit(solution)/shard_map/ppermute | solution.py:75
  73.8 8.8 %collective-permute-start.26 = (bf16[176,256]{1,0:T(8,128)(2,1)S(1)}, bf16[176,256]{1,0:T(8,128)(2,1)S(1)}, u32[]{:S(2)}, u32[]{:S(2)}) collective-permute-start(bf16[176,256]{1,0:T(8,128)(2,1)S(1)} %get-tuple-element.53.refs_0_), channel_id=1, source_target_pairs={{0,8},{8,0},{16,24},{24,16},{1,9},{9,1},{17,25},{25,17},{2,10},{10... | collective-permute-start | bytes 270344 | tf_op jit(solution)/shard_map/ppermute | solution.py:75
  74.7 11.2 %collective-permute-start.27 = (bf16[176,256]{1,0:T(8,128)(2,1)S(1)}, bf16[176,256]{1,0:T(8,128)(2,1)S(1)}, u32[]{:S(2)}, u32[]{:S(2)}) collective-permute-start(bf16[176,256]{1,0:T(8,128)(2,1)S(1)} %get-tuple-element.53.refs_0_), channel_id=1, source_target_pairs={{0,16},{8,24},{16,0},{24,8},{1,17},{9,25},{17,1},{25,9},{2,18},{10... | collective-permute-start | bytes 270344 | tf_op jit(solution)/shard_map/ppermute | solution.py:75
  76.9 9.0 %collective-permute-start.28 = (bf16[176,256]{1,0:T(8,128)(2,1)S(1)}, bf16[176,256]{1,0:T(8,128)(2,1)S(1)}, u32[]{:S(2)}, u32[]{:S(2)}) collective-permute-start(bf16[176,256]{1,0:T(8,128)(2,1)S(1)} %get-tuple-element.53.refs_0_), channel_id=1, source_target_pairs={{0,24},{8,16},{16,8},{24,0},{1,25},{9,17},{17,9},{25,1},{2,26},{10... | collective-permute-start | bytes 270344 | tf_op jit(solution)/shard_map/ppermute | solution.py:75
  80.1 6.5 %collective-permute-start.29 = (bf16[168,256]{1,0:T(8,128)(2,1)S(1)}, bf16[168,256]{1,0:T(8,128)(2,1)S(1)}, u32[]{:S(2)}, u32[]{:S(2)}) collective-permute-start(bf16[168,256]{1,0:T(8,128)(2,1)S(1)} %shard_map.100.refs_1_), channel_id=1, source_target_pairs={{0,8},{8,0},{16,24},{24,16},{1,9},{9,1},{17,25},{25,17},{2,10},{10... | collective-permute-start | bytes 258056 | tf_op jit(solution)/shard_map/ppermute | solution.py:75
  81.1 5.5 %collective-permute-start.30 = (bf16[168,256]{1,0:T(8,128)(2,1)S(1)}, bf16[168,256]{1,0:T(8,128)(2,1)S(1)}, u32[]{:S(2)}, u32[]{:S(2)}) collective-permute-start(bf16[168,256]{1,0:T(8,128)(2,1)S(1)} %shard_map.100.refs_1_), channel_id=1, source_target_pairs={{0,16},{8,24},{16,0},{24,8},{1,17},{9,25},{17,1},{25,9},{2,18},{10... | collective-permute-start | bytes 258056 | tf_op jit(solution)/shard_map/ppermute | solution.py:75
  82.6 5.4 %collective-permute-start.31 = (bf16[168,256]{1,0:T(8,128)(2,1)S(1)}, bf16[168,256]{1,0:T(8,128)(2,1)S(1)}, u32[]{:S(2)}, u32[]{:S(2)}) collective-permute-start(bf16[168,256]{1,0:T(8,128)(2,1)S(1)} %shard_map.100.refs_1_), channel_id=1, source_target_pairs={{0,24},{8,16},{16,8},{24,0},{1,25},{9,17},{17,9},{25,1},{2,26},{10... | collective-permute-start | bytes 258056 | tf_op jit(solution)/shard_map/ppermute | solution.py:75
  90.4 5.3 %collective-permute-start.33 = (bf16[32,1024]{1,0:T(8,128)(2,1)S(1)}, bf16[32,1024]{1,0:T(8,128)(2,1)S(1)}, u32[]{:S(2)}, u32[]{:S(2)}) collective-permute-start(bf16[32,1024]{1,0:T(8,128)(2,1)S(1)} %get-tuple-element.58), channel_id=1, source_target_pairs={{0,2},{1,3},{2,0},{3,1},{4,6},{5,7},{6,4},{7,5},{8,10},{9,11},{10,... | collective-permute-start | bytes 196616 | tf_op jit(solution)/shard_map/ppermute | solution.py:79
  90.4 7.9 %collective-permute-start.34 = (bf16[32,1024]{1,0:T(8,128)(2,1)S(1)}, bf16[32,1024]{1,0:T(8,128)(2,1)S(1)}, u32[]{:S(2)}, u32[]{:S(2)}) collective-permute-start(bf16[32,1024]{1,0:T(8,128)(2,1)S(1)} %get-tuple-element.59), channel_id=1, source_target_pairs={{0,4},{1,5},{2,6},{3,7},{4,0},{5,1},{6,2},{7,3},{8,12},{9,13},{10,... | collective-permute-start | bytes 196616 | tf_op jit(solution)/shard_map/ppermute | solution.py:79
  92.9 6.2 %collective-permute-start.35 = (bf16[32,1024]{1,0:T(8,128)(2,1)S(1)}, bf16[32,1024]{1,0:T(8,128)(2,1)S(1)}, u32[]{:S(2)}, u32[]{:S(2)}) collective-permute-start(bf16[32,1024]{1,0:T(8,128)(2,1)S(1)} %get-tuple-element.60), channel_id=1, source_target_pairs={{0,6},{1,7},{2,4},{3,5},{4,2},{5,3},{6,0},{7,1},{8,14},{9,15},{10,... | collective-permute-start | bytes 196616 | tf_op jit(solution)/shard_map/ppermute | solution.py:79
  100.6 6.8 %collective-permute-start.37 = (bf16[32,1024]{1,0:T(8,128)(2,1)S(1)}, bf16[32,1024]{1,0:T(8,128)(2,1)S(1)}, u32[]{:S(2)}, u32[]{:S(2)}) collective-permute-start(bf16[32,1024]{1,0:T(8,128)(2,1)S(1)} %shard_map.105.refs_0_), channel_id=1, source_target_pairs={{0,4},{1,5},{2,6},{3,7},{4,0},{5,1},{6,2},{7,3},{8,12},{9,13},{10,... | collective-permute-start | bytes 196616 | tf_op jit(solution)/shard_map/ppermute | solution.py:79
  101.9 6.2 %collective-permute-start.38 = (bf16[32,1024]{1,0:T(8,128)(2,1)S(1)}, bf16[32,1024]{1,0:T(8,128)(2,1)S(1)}, u32[]{:S(2)}, u32[]{:S(2)}) collective-permute-start(bf16[32,1024]{1,0:T(8,128)(2,1)S(1)} %shard_map.105.refs_0_), channel_id=1, source_target_pairs={{0,6},{1,7},{2,4},{3,5},{4,2},{5,3},{6,0},{7,1},{8,14},{9,15},{10,... | collective-permute-start | bytes 196616 | tf_op jit(solution)/shard_map/ppermute | solution.py:79
  (14 other events, 69.2 us)

commit v4 on v3

--- a/solution.py
+++ b/solution.py
@@ -12,10 +12,17 @@
 EXTRA = 8
 SPLITS = 2
 MIB = 1 << 20
-WIDE = 16
 VMEM = pl.BlockSpec(memory_space=pltpu.VMEM)
 SMEM = pl.BlockSpec(memory_space=pltpu.SMEM)
 HBM = pl.BlockSpec(memory_space=pltpu.HBM)
+
+
+def piece_of(units, members):
+    return -(-(-(-units // members)) // 8) * 8
+
+
+def splits_of(piece):
+    return SPLITS if piece >= 128 else 1
 
 
 def call(body, args, specs, shapes, flops, moved, scratch=(), room=16):
@@ -85,8 +92,9 @@
         layers, width, units = gate_weight.shape
         kernel = gate_taps.shape[1]
         count = tokens.shape[0]
-        piece = -(-(-(-units // n_a)) // 8) * 8
-        step = -(-(-(-piece // SPLITS)) // 8) * 8
+        piece = piece_of(units, n_a)
+        splits = splits_of(piece)
+        step = -(-(-(-piece // splits)) // 8) * 8
         cuts = [(lo, min(step, piece - lo)) for lo in range(0, piece, step)]
         n_h = len(cuts)
         even = n_a * piece == units
@@ -119,50 +127,116 @@
 
         def up(layer, pieces, held):
             outs = {}
-            extra = None
+            extra = taps = None
             n_p = len(pieces)
-            for h, s in order:
+            cold = held is None
+            for index, (h, s) in enumerate(order):
                 lo, size = cuts[h]
                 rows = 2 * size + (EXTRA if h == 0 else 0)
-                initial = extra is None
-                load = initial and held is None
-
-                def body_fn(*refs, s=s, h=h, lo=lo, size=size, initial=initial, load=load):
-                    a_ref, weights = refs[0], list(refs[1:3])
+                initial = index == 0
+                load = cold and index == 1
+                args = [me_a, *(held or (gate_rows, value_rows))]
+                specs = [SMEM] + [VMEM if held else HBM] * 2
+                shapes = [((rows, count), BF16)]
+                scratch = []
+                if initial and cold:
+                    args += [stay(pieces[0]), stay(norm_gain), me_c]
+                    specs += [HBM, HBM, SMEM]
+                elif initial:
+                    args += [*pieces, norm_gain, me_c]
+                    specs += [VMEM] * (n_p + 1) + [SMEM]
+                else:
+                    args += extra
+                    specs += [VMEM] * 2
+                if initial:
+                    shapes += [((count, width), BF16), ((EXTRA, count), BF16)]
+                    scratch.append(pltpu.VMEM((count, width), BF16))
+                if initial and cold:
+                    scratch += [
+                        pltpu.VMEM(norm_gain.shape, F32),
+                        pltpu.VMEM((2, size, width), BF16),
+                        pltpu.SemaphoreType.DMA((4,)),
+                    ]
+                if load:
+                    args += [stay(value) for value in tap_args]
+                    specs += [HBM, HBM]
+                    shapes += [((units, width), BF16)] * 2 + [((piece, tap_rows), F32)]
+                    scratch += [
+                        pltpu.VMEM((2, *tap_args[0].shape), F32),
+                        pltpu.VMEM((units, tap_rows), F32),
+                        pltpu.SemaphoreType.DMA((2 * n_a + 2,)),
+                    ]
+
+                def body_fn(
+                    *refs, s=s, lo=lo, size=size, h=h, initial=initial, load=load, n=len(args)
+                ):
+                    a_ref, gate_ref, value_ref = refs[:3]
+                    weights = [gate_ref, value_ref]
+                    out_ref = refs[n]
                     at = pl.ds(aligned(begin(peer(a_ref[0], s, n_a)) + lo), size)
-                    if load:
-                        sem, stored = refs[-1], refs[-4:-2]
-                        ahead = begin(peer(a_ref[0], s, n_a))
-                        blocks = [pl.ds(aligned(ahead), piece)]
-                        for t in range(n_a):
-                            if t != s:
-                                blocks.append(pl.ds(aligned(begin(peer(a_ref[0], t, n_a))), piece))
-                        if not even:
-                            blocks = [slice(None)]
-                        copies = []
+                    waits = [(), ()]
+                    copies = []
+
+                    def launch(source_ref, target_ref, sem):
+                        copy = pltpu.make_async_copy(source_ref, target_ref, sem)
+                        copy.start()
+                        return copy
+
+                    if initial and cold:
+                        rows_ref, gain_ref, block_ref, sem = refs[n + 3 :]
+                        first = [
+                            launch(refs[3], rows_ref, sem.at[0]),
+                            launch(refs[4], gain_ref, sem.at[1]),
+                        ]
+                        for k in range(2):
+                            waits[k] = (
+                                launch(weights[k].at[layer, at], block_ref.at[k], sem.at[2 + k]),
+                            )
+                        for copy in first:
+                            copy.wait()
+                        current = rows_ref[...].astype(F32)
+                        lefts = [block_ref.at[0], block_ref.at[1]]
+                    elif load:
+                        stored, taps_ref = refs[n + 1 : n + 3], refs[n + 3]
+                        raw_ref, turned_ref, sem = refs[n + 4 :]
+                        raw = [
+                            launch(refs[5 + k], raw_ref.at[k], sem.at[2 * n_a + k]) for k in range(2)
+                        ]
+                        blocks = [slice(None)]
+                        if even:
+                            targets = [s] + [t for t in range(n_a) if t != s]
+                            blocks = [
+                                pl.ds(aligned(begin(peer(a_ref[0], t, n_a))), piece)
+                                for t in targets
+                            ]
                         for i, block in enumerate(blocks):
                             for k in range(2):
-                                copy = pltpu.make_async_copy(
-                                    weights[k].at[layer, block], stored[k].at[block], sem.at[2 * i + k]
+                                copies.append(
+                                    launch(
+                                        weights[k].at[layer, block],
+                                        stored[k].at[block],
+                                        sem.at[2 * i + k],
+                                    )
                                 )
-                                copy.start()
-                                copies.append(copy)
-                        weights = stored
+                        waits = [(copies[0],), (copies[1],)]
+                        copies = copies[2:]
+                        lefts = [ref.at[at] for ref in stored]
+                    else:
+                        lefts = [ref.at[at] for ref in weights]
+                        if initial:
+                            gain_ref, side_ref = refs[3 + n_p : 5 + n_p]
+                            current = load_rows(refs[3 : 3 + n_p], side_ref, refs[n + 3])
                     if initial:
-                        sources = refs[3 : 3 + n_p]
-                        gain_ref, side_ref = refs[3 + n_p : 5 + n_p]
-                        out_ref, scaled_ref, tail_ref = refs[5 + n_p : 8 + n_p]
-                        rows_ref = refs[-2] if load else refs[-1]
-                        current = load_rows(sources, side_ref, rows_ref)
+                        scaled_ref, tail_ref = refs[n + 1 : n + 3]
                         prepare(current, gain_ref[layer : layer + 1, :], scaled_ref, tail_ref)
                     else:
-                        scaled_ref, tail_ref, out_ref = refs[3:6]
+                        scaled_ref, tail_ref = refs[3:5]
                     scaled = scaled_ref[...]
                     for k in range(2):
-                        if load:
-                            copies[k].wait()
+                        for copy in waits[k]:
+                            copy.wait()
                         out_ref[k * size : (k + 1) * size, :] = lax.dot_general(
-                            weights[k][at, :],
+                            lefts[k][...],
                             scaled,
                             (((1,), (1,)), ((), ())),
                             preferred_element_type=F32,
@@ -170,26 +244,21 @@
                     if h == 0:
                         out_ref[2 * size : 2 * size + EXTRA, :] = tail_ref[...]
                     if load:
-                        for copy in copies[2:]:
+                        for copy in raw:
                             copy.wait()
-
-                if load:
-                    args, specs = [me_a, gate_rows, value_rows], [SMEM, HBM, HBM]
-                else:
-                    args, specs = [me_a, *held], [SMEM, VMEM, VMEM]
-                shapes = [((rows, count), BF16)]
-                scratch = []
-                if initial:
-                    args += [*pieces, norm_gain, me_c]
-                    specs += [VMEM] * (n_p + 1) + [SMEM]
-                    shapes += [((count, width), BF16), ((EXTRA, count), BF16)]
-                    scratch = [pltpu.VMEM((count, width), BF16)]
-                    if load:
-                        shapes += [((units, width), BF16)] * 2
-                        scratch += [pltpu.SemaphoreType.DMA((2 * n_a,))]
-                else:
-                    args += extra
-                    specs += [VMEM] * 2
+                        lines = [
+                            raw_ref[kind, k, l : l + 1, :]
+                            for l in range(layers)
+                            for kind in range(2)
+                            for k in range(kernel)
+                        ]
+                        if tap_rows > len(lines):
+                            lines.append(jnp.zeros((tap_rows - len(lines), units), F32))
+                        turned_ref[...] = jnp.concatenate(lines, axis=0).T
+                        taps_ref[...] = turned_ref[pl.ds(aligned(begin(a_ref[0])), piece), :]
+                    for copy in copies:
+                        copy.wait()
+
                 out = call(
                     body_fn,
                     args,
@@ -198,60 +267,35 @@
                     4 * size * width * count,
                     4 * size * width,
                     scratch,
-                    room=WIDE if load else 16,
                 )
                 if initial:
                     extra = out[1:3]
                 if load:
-                    held = out[3:5]
+                    held, taps = out[1:3], out[3]
                 outs[h, s] = out[0]
-            return outs
-
-        def fetch(layer, after):
-            sources, picks = [down_rows], [layer]
-            if layer + 1 < layers:
-                sources += [gate_rows, value_rows]
-                picks += [layer + 1] * 2
+            return outs, taps
+
+        def fetch(layer, sources, after):
             n = len(sources)
-            shapes = [(source.shape[1:], BF16) for source in sources]
-            args, specs = [*sources, after], [HBM] * n + [VMEM]
-            scratch = [pltpu.SemaphoreType.DMA((n,))]
-            if layer == 0:
-                args += [me_a, *tap_args]
-                specs += [SMEM, VMEM, VMEM]
-                shapes.append(((piece, tap_rows), F32))
-                scratch.append(pltpu.VMEM((units, tap_rows), F32))
 
             def body_fn(*refs):
-                outs = refs[len(args) : len(args) + len(shapes)]
-                sem = refs[len(args) + len(shapes)]
+                sem = refs[-1]
                 copies = []
                 for k in range(n):
-                    copy = pltpu.make_async_copy(refs[k].at[picks[k]], outs[k], sem.at[k])
+                    copy = pltpu.make_async_copy(refs[k].at[layer], refs[n + 1 + k], sem.at[k])
                     copy.start()
                     copies.append(copy)
-                if layer == 0:
-                    a_ref, gate_ref, value_ref = refs[n + 1 : n + 4]
-                    rows = []
-                    for l in range(layers):
-                        for ref in (gate_ref, value_ref):
-                            rows += [ref[k, l : l + 1, :] for k in range(kernel)]
-                    if tap_rows > len(rows):
-                        rows.append(jnp.zeros((tap_rows - len(rows), units), F32))
-                    held_ref = refs[-1]
-                    held_ref[...] = jnp.concatenate(rows, axis=0).T
-                    outs[n][...] = held_ref[pl.ds(aligned(begin(a_ref[0])), piece), :]
                 for copy in copies:
                     copy.wait()
 
             return call(
                 body_fn,
-                args,
-                specs,
-                shapes,
-                2 * units * width * count,
+                [*sources, after],
+                [HBM] * n + [VMEM],
+                [(source.shape[1:], BF16) for source in sources],
+                2 * units * width * count // 3 * n,
                 2 * n * units * width,
-                scratch,
+                [pltpu.SemaphoreType.DMA((n,))],
             )
 
         def act(layer, h, parts, inverse, taps):
@@ -422,12 +466,11 @@
 
         pieces = [tokens]
         old = tokens
-        held = None
+        held = taps = None
         for layer in range(layers):
-            outs = up(layer, pieces, held)
-            weight, *held = fetch(layer, outs[n_h - 1, 0])
-            if layer == 0:
-                *held, taps = held
+            outs, came_taps = up(layer, pieces, held)
+            taps = taps if came_taps is None else came_taps
+            (weight,) = fetch(layer, [down_rows], outs[n_h - 1, 0])
             inverse = None
             mine, others = [], []
             for h in range(n_h):
@@ -443,6 +486,9 @@
             away, kept = out
             dealt = deal(kept, send_core(away))
             came = [send_z(dealt[s], s) for s in range(1, n_z)]
+            if layer + 1 < layers:
+                ahead = [gate_rows, value_rows]
+                held = fetch(layer + 1, ahead, dealt[0])
             old = settle(layer, dealt[0], came, old)
             near = gather([old] + [send_z(old, s) for s in range(1, n_z)])
             pieces = [near, send_core(near)]

time: 111 us -> 112 us (level)
  Pallas kernels: 21.8 us -> 24.4 us
  waiting for transfers between devices: 37.5 us -> 39.5 us
  local copies, waits for them, and re-layouts: 1.88 us -> 0.01 us
  starting transfers between devices: 48.9 us -> 47.5 us
    ppermute x24, waiting for transfers between devices: 12.5 us -> 17.2 us  [send_a(): return lax.ppermute(value, 'ra', [(i, peer(i, s, n_a)) for i in range(n_a)])]
    pallas_call x35 -> x36, Pallas kernels: 21.8 us -> 24.4 us  [call(): pl.pallas_call(body, in_specs=specs, out_specs=[VMEM] * len(shapes), out_...]
    ppermute x24, starting transfers between devices: 30.8 us -> 28.9 us  [send_a(): return lax.ppermute(value, 'ra', [(i, peer(i, s, n_a)) for i in range(n_a)])]
    unnamed x12 -> x4, local copies, waits for them, and re-layouts: 1.88 us -> 0.01 us
    ppermute x4, waiting for transfers between devices: 6.09 us -> 4.57 us  [send_core(): return lax.ppermute(value, 'cb', [(i, i ^ 1) for i in range(n_c)])]
  transfers between devices with their start and end apart: 40 -> 40, of which waited for: 22 -> 18; matrix products, arithmetic and copies ran while one was open for 0% -> 0% of each run, Pallas kernels for 14% -> 17%
where the time goes in v4:
time: 112 us
  starting transfers between devices  47.5 us (42%)
  waiting for transfers between devices  39.5 us (35%)
  Pallas kernels  24.4 us (22%)
    ppermute x24, starting transfers between devices, send_a(): return lax.ppermute(value, 'ra', [(i, peer(i, s, n_a)) for i in range(n_a)])  28.9 us
    pallas_call x36, Pallas kernels, call(): pl.pallas_call(body, in_specs=specs, out_specs=[VMEM] * len(shapes), out_...  24.4 us
    ppermute x12, starting transfers between devices, send_z(): return lax.ppermute(value, 'cb', pairs)  18.3 us
    ppermute x12, waiting for transfers between devices, send_z(): return lax.ppermute(value, 'cb', pairs)  17.8 us
    ppermute x24, waiting for transfers between devices, send_a(): return lax.ppermute(value, 'ra', [(i, peer(i, s, n_a)) for i in range(n_a)])  17.2 us
    ppermute x4, waiting for transfers between devices, send_core(): return lax.ppermute(value, 'cb', [(i, i ^ 1) for i in range(n_c)])  4.57 us
  transfers between devices with their start and end apart: 40, of which 18 were waited for; matrix products, arithmetic and copies ran while one was open for 0% of the time, Pallas kernels for 17%

profile of v4, /device:TPU:0, one launch (start us, length us, event | category | flops | bytes accessed | tf_op | source)
XLA Modules:
  0.0 111.8 jit_solution(17156415901228826920)
XLA Ops:
  0.0 2.2 %shard_map.73 = (bf16[360,256]{1,0:T(8,128)(2,1)S(1)}, bf16[256,1024]{1,0:T(8,128)(2,1)S(1)}, bf16[8,256]{1,0:T(8,128)(2,1)S(1)}) custom-call(s32[1]{0:T(128)} %bitcast.refs_0_.a_ref, bf16[2,1376,1024]{2,1,0:T(8,128)(2,1)} %bitcast.6, bf16[2,1376,1024]{2,1,0:T(8,128)(2,1)} %bitcast.9, bf16[256,1024]{1,0:T(8,128)(2,1)} %refs_4_.3, f32[2,1024]{1,0:T(2,128)} %refs_5_.1, ...), custom_call_target="tpu_custom_call" | custom-call | flops 184549376 | bytes 720896 | tf_op jit(solution)/shard_map/pallas_call | solution.py:29
  2.2 4.0 %collective-permute-start.2 = (bf16[360,256]{1,0:T(8,128)(2,1)S(1)}, bf16[360,256]{1,0:T(8,128)(2,1)S(1)}, u32[]{:S(2)}, u32[]{:S(2)}) collective-permute-start(bf16[360,256]{1,0:T(8,128)(2,1)S(1)} %get-tuple-element.38), channel_id=1, source_target_pairs={{0,24},{8,16},{16,8},{24,0},{1,25},{9,17},{17,9},{25,1},{2,26},{10... | collective-permute-start | bytes 552968 | tf_op jit(solution)/shard_map/ppermute | solution.py:82
  6.2 2.7 %shard_map.74 = (bf16[360,256]{1,0:T(8,128)(2,1)S(1)}, bf16[1376,1024]{1,0:T(8,128)(2,1)S(1)}, bf16[1376,1024]{1,0:T(8,128)(2,1)S(1)}, f32[344,16]{1,0:T(8,128)S(1)}) custom-call(s32[1]{0:T(128)} %bitcast.refs_0_.a_ref, bf16[2,1376,1024]{2,1,0:T(8,128)(2,1)} %bitcast.7, bf16[2,1376,1024]{2,1,0:T(8,128)(2,1)} %bitcast.10, ...), custom_call_target="tpu_custom_call" | custom-call | flops 184549376 | bytes 720896 | tf_op jit(solution)/shard_map/pallas_call | solution.py:29
  10.6 2.0 %collective-permute-start.3 = (bf16[336,256]{1,0:T(8,128)(2,1)S(1)}, bf16[336,256]{1,0:T(8,128)(2,1)S(1)}, u32[]{:S(2)}, u32[]{:S(2)}) collective-permute-start(bf16[336,256]{1,0:T(8,128)(2,1)S(1)} %shard_map.80), channel_id=1, source_target_pairs={{0,8},{8,0},{16,24},{24,16},{1,9},{9,1},{17,25},{25,17},{2,10},{10... | collective-permute-start | bytes 516104 | tf_op jit(solution)/shard_map/ppermute | solution.py:82
  13.1 1.6 %collective-permute-start.4 = (bf16[336,256]{1,0:T(8,128)(2,1)S(1)}, bf16[336,256]{1,0:T(8,128)(2,1)S(1)}, u32[]{:S(2)}, u32[]{:S(2)}) collective-permute-start(bf16[336,256]{1,0:T(8,128)(2,1)S(1)} %shard_map.81), channel_id=1, source_target_pairs={{0,16},{8,24},{16,0},{24,8},{1,17},{9,25},{17,1},{25,9},{2,18},{10... | collective-permute-start | bytes 516104 | tf_op jit(solution)/shard_map/ppermute | solution.py:82
  17.7 1.8 %collective-permute-start.8 = (bf16[176,256]{1,0:T(8,128)(2,1)S(1)}, bf16[176,256]{1,0:T(8,128)(2,1)S(1)}, u32[]{:S(2)}, u32[]{:S(2)}) collective-permute-start(bf16[176,256]{1,0:T(8,128)(2,1)S(1)} %get-tuple-element.40.refs_0_), channel_id=1, source_target_pairs={{0,24},{8,16},{16,8},{24,0},{1,25},{9,17},{17,9},{25,1},{2,26},{10... | collective-permute-start | bytes 270344 | tf_op jit(solution)/shard_map/ppermute | solution.py:82
  21.7 4.6 %collective-permute-done.4.refs_2_ = bf16[336,256]{1,0:T(8,128)(2,1)S(1)} collective-permute-done((bf16[336,256]{1,0:T(8,128)(2,1)S(1)}, bf16[336,256]{1,0:T(8,128)(2,1)S(1)}, u32[]{:S(2)}, u32[]{:S(2)}) %collective-permute-start.4) | collective-permute-done | bytes 172064 | tf_op jit(solution)/shard_map/ppermute | solution.py:82
  26.7 1.9 %collective-permute-start.11 = (bf16[168,256]{1,0:T(8,128)(2,1)S(1)}, bf16[168,256]{1,0:T(8,128)(2,1)S(1)}, u32[]{:S(2)}, u32[]{:S(2)}) collective-permute-start(bf16[168,256]{1,0:T(8,128)(2,1)S(1)} %shard_map.83.refs_1_), channel_id=1, source_target_pairs={{0,24},{8,16},{16,8},{24,0},{1,25},{9,17},{17,9},{25,1},{2,26},{10... | collective-permute-start | bytes 258056 | tf_op jit(solution)/shard_map/ppermute | solution.py:82
  30.3 1.8 %shard_map.76.weight_ref = bf16[1376,1024]{1,0:T(8,128)(2,1)S(1)} custom-call(bf16[2,1376,1024]{2,1,0:T(8,128)(2,1)} %refs_0_.3, bf16[336,256]{1,0:T(8,128)(2,1)S(1)} %shard_map.75.refs_1_.refs_0_), custom_call_target="tpu_custom_call" | custom-call | flops 240473424 | bytes 2818048 | tf_op jit(solution)/shard_map/pallas_call | solution.py:29
  37.0 2.3 %collective-permute-start.13 = (bf16[32,1024]{1,0:T(8,128)(2,1)S(1)}, bf16[32,1024]{1,0:T(8,128)(2,1)S(1)}, u32[]{:S(2)}, u32[]{:S(2)}) collective-permute-start(bf16[32,1024]{1,0:T(8,128)(2,1)S(1)} %get-tuple-element.47), channel_id=1, source_target_pairs={{0,2},{1,3},{2,0},{3,1},{4,6},{5,7},{6,4},{7,5},{8,10},{9,11},{10,... | collective-permute-start | bytes 196616 | tf_op jit(solution)/shard_map/ppermute | solution.py:86
  39.3 2.6 %collective-permute-start.14 = (bf16[32,1024]{1,0:T(8,128)(2,1)S(1)}, bf16[32,1024]{1,0:T(8,128)(2,1)S(1)}, u32[]{:S(2)}, u32[]{:S(2)}) collective-permute-start(bf16[32,1024]{1,0:T(8,128)(2,1)S(1)} %get-tuple-element.48), channel_id=1, source_target_pairs={{0,4},{1,5},{2,6},{3,7},{4,0},{5,1},{6,2},{7,3},{8,12},{9,13},{10,... | collective-permute-start | bytes 196616 | tf_op jit(solution)/shard_map/ppermute | solution.py:86
  41.9 4.9 %collective-permute-done.14.refs_1_ = bf16[32,1024]{1,0:T(8,128)(2,1)S(1)} collective-permute-done((bf16[32,1024]{1,0:T(8,128)(2,1)S(1)}, bf16[32,1024]{1,0:T(8,128)(2,1)S(1)}, u32[]{:S(2)}, u32[]{:S(2)}) %collective-permute-start.14) | collective-permute-done | bytes 65568 | tf_op jit(solution)/shard_map/ppermute | solution.py:86
  48.1 2.1 %collective-permute-start.18 = (bf16[32,1024]{1,0:T(8,128)(2,1)S(1)}, bf16[32,1024]{1,0:T(8,128)(2,1)S(1)}, u32[]{:S(2)}, u32[]{:S(2)}) collective-permute-start(bf16[32,1024]{1,0:T(8,128)(2,1)S(1)} %shard_map.89.refs_0_.refs_4_), channel_id=1, source_target_pairs={{0,6},{1,7},{2,4},{3,5},{4,2},{5,3},{6,0},{7,1},{8,14},{9,15},{10,... | collective-permute-start | bytes 196616 | tf_op jit(solution)/shard_map/ppermute | solution.py:86
  50.5 2.1 %collective-permute-start.16 = (bf16[32,1024]{1,0:T(8,128)(2,1)S(1)}, bf16[32,1024]{1,0:T(8,128)(2,1)S(1)}, u32[]{:S(2)}, u32[]{:S(2)}) collective-permute-start(bf16[32,1024]{1,0:T(8,128)(2,1)S(1)} %shard_map.89.refs_0_.refs_4_), channel_id=1, source_target_pairs={{0,2},{1,3},{2,0},{3,1},{4,6},{5,7},{6,4},{7,5},{8,10},{9,11},{10,... | collective-permute-start | bytes 196616 | tf_op jit(solution)/shard_map/ppermute | solution.py:86
  52.6 1.8 %collective-permute-done.18.refs_3_ = bf16[32,1024]{1,0:T(8,128)(2,1)S(1)} collective-permute-done((bf16[32,1024]{1,0:T(8,128)(2,1)S(1)}, bf16[32,1024]{1,0:T(8,128)(2,1)S(1)}, u32[]{:S(2)}, u32[]{:S(2)}) %collective-permute-start.18) | collective-permute-done | bytes 65568 | tf_op jit(solution)/shard_map/ppermute | solution.py:86
  54.4 1.5 %collective-permute-done.17.refs_2_ = bf16[32,1024]{1,0:T(8,128)(2,1)S(1)} collective-permute-done((bf16[32,1024]{1,0:T(8,128)(2,1)S(1)}, bf16[32,1024]{1,0:T(8,128)(2,1)S(1)}, u32[]{:S(2)}, u32[]{:S(2)}) %collective-permute-start.17) | collective-permute-done | bytes 65568 | tf_op jit(solution)/shard_map/ppermute | solution.py:86
  56.1 2.7 %shard_map.88 = (bf16[1376,1024]{1,0:T(8,128)(2,1)S(1)}, bf16[1376,1024]{1,0:T(8,128)(2,1)S(1)}) custom-call(bf16[2,1376,1024]{2,1,0:T(8,128)(2,1)} %bitcast.8, bf16[2,1376,1024]{2,1,0:T(8,128)(2,1)} %bitcast.11, f32[32,1024]{1,0:T(8,128)S(1)} %get-tuple-element.44.refs_2_.own_ref), custom_call_target="tpu_custom_call" | custom-call | flops 480946848 | bytes 5636096 | tf_op jit(solution)/shard_map/pallas_call | solution.py:29
  61.4 2.6 %collective-permute-start.22 = (bf16[360,256]{1,0:T(8,128)(2,1)S(1)}, bf16[360,256]{1,0:T(8,128)(2,1)S(1)}, u32[]{:S(2)}, u32[]{:S(2)}) collective-permute-start(bf16[360,256]{1,0:T(8,128)(2,1)S(1)} %get-tuple-element.52), channel_id=1, source_target_pairs={{0,24},{8,16},{16,8},{24,0},{1,25},{9,17},{17,9},{25,1},{2,26},{10... | collective-permute-start | bytes 552968 | tf_op jit(solution)/shard_map/ppermute | solution.py:82
  67.4 1.7 %collective-permute-start.25 = (bf16[336,256]{1,0:T(8,128)(2,1)S(1)}, bf16[336,256]{1,0:T(8,128)(2,1)S(1)}, u32[]{:S(2)}, u32[]{:S(2)}) collective-permute-start(bf16[336,256]{1,0:T(8,128)(2,1)S(1)} %shard_map.100), channel_id=1, source_target_pairs={{0,24},{8,16},{16,8},{24,0},{1,25},{9,17},{17,9},{25,1},{2,26},{10... | collective-permute-start | bytes 516104 | tf_op jit(solution)/shard_map/ppermute | solution.py:82
  69.6 2.8 %collective-permute-done.21.refs_2_ = bf16[360,256]{1,0:T(8,128)(2,1)S(1)} collective-permute-done((bf16[360,256]{1,0:T(8,128)(2,1)S(1)}, bf16[360,256]{1,0:T(8,128)(2,1)S(1)}, u32[]{:S(2)}, u32[]{:S(2)}) %collective-permute-start.21) | collective-permute-done | bytes 184352 | tf_op jit(solution)/shard_map/ppermute | solution.py:82
  73.9 2.0 %collective-permute-start.27 = (bf16[176,256]{1,0:T(8,128)(2,1)S(1)}, bf16[176,256]{1,0:T(8,128)(2,1)S(1)}, u32[]{:S(2)}, u32[]{:S(2)}) collective-permute-start(bf16[176,256]{1,0:T(8,128)(2,1)S(1)} %get-tuple-element.53.refs_0_), channel_id=1, source_target_pairs={{0,16},{8,24},{16,0},{24,8},{1,17},{9,25},{17,1},{25,9},{2,18},{10... | collective-permute-start | bytes 270344 | tf_op jit(solution)/shard_map/ppermute | solution.py:82
  76.9 4.8 %collective-permute-done.24.refs_2_ = bf16[336,256]{1,0:T(8,128)(2,1)S(1)} collective-permute-done((bf16[336,256]{1,0:T(8,128)(2,1)S(1)}, bf16[336,256]{1,0:T(8,128)(2,1)S(1)}, u32[]{:S(2)}, u32[]{:S(2)}) %collective-permute-start.24) | collective-permute-done | bytes 172064 | tf_op jit(solution)/shard_map/ppermute | solution.py:82
  83.2 2.0 %collective-permute-start.30 = (bf16[168,256]{1,0:T(8,128)(2,1)S(1)}, bf16[168,256]{1,0:T(8,128)(2,1)S(1)}, u32[]{:S(2)}, u32[]{:S(2)}) collective-permute-start(bf16[168,256]{1,0:T(8,128)(2,1)S(1)} %shard_map.101.refs_1_), channel_id=1, source_target_pairs={{0,16},{8,24},{16,0},{24,8},{1,17},{9,25},{17,1},{25,9},{2,18},{10... | collective-permute-start | bytes 258056 | tf_op jit(solution)/shard_map/ppermute | solution.py:82
  85.7 1.8 %shard_map.93.weight_ref = bf16[1376,1024]{1,0:T(8,128)(2,1)S(1)} custom-call(bf16[2,1376,1024]{2,1,0:T(8,128)(2,1)} %refs_0_.3, bf16[336,256]{1,0:T(8,128)(2,1)S(1)} %shard_map.92.refs_1_.refs_0_), custom_call_target="tpu_custom_call" | custom-call | flops 240473424 | bytes 2818048 | tf_op jit(solution)/shard_map/pallas_call | solution.py:29
  90.5 1.5 %collective-permute-done.32.came_ref = bf16[128,1024]{1,0:T(8,128)(2,1)S(1)} collective-permute-done((bf16[128,1024]{1,0:T(8,128)(2,1)S(1)}, bf16[128,1024]{1,0:T(8,128)(2,1)S(1)}, u32[]{:S(2)}, u32[]{:S(2)}) %collective-permute-start.32) | collective-permute-done | bytes 262176 | tf_op jit(solution)/shard_map/ppermute | solution.py:89
  93.0 1.6 %collective-permute-start.34 = (bf16[32,1024]{1,0:T(8,128)(2,1)S(1)}, bf16[32,1024]{1,0:T(8,128)(2,1)S(1)}, u32[]{:S(2)}, u32[]{:S(2)}) collective-permute-start(bf16[32,1024]{1,0:T(8,128)(2,1)S(1)} %get-tuple-element.59), channel_id=1, source_target_pairs={{0,4},{1,5},{2,6},{3,7},{4,0},{5,1},{6,2},{7,3},{8,12},{9,13},{10,... | collective-permute-start | bytes 196616 | tf_op jit(solution)/shard_map/ppermute | solution.py:86
  94.6 1.9 %collective-permute-start.35 = (bf16[32,1024]{1,0:T(8,128)(2,1)S(1)}, bf16[32,1024]{1,0:T(8,128)(2,1)S(1)}, u32[]{:S(2)}, u32[]{:S(2)}) collective-permute-start(bf16[32,1024]{1,0:T(8,128)(2,1)S(1)} %get-tuple-element.60), channel_id=1, source_target_pairs={{0,6},{1,7},{2,4},{3,5},{4,2},{5,3},{6,0},{7,1},{8,14},{9,15},{10,... | collective-permute-start | bytes 196616 | tf_op jit(solution)/shard_map/ppermute | solution.py:86
  96.5 4.8 %collective-permute-done.34.refs_1_ = bf16[32,1024]{1,0:T(8,128)(2,1)S(1)} collective-permute-done((bf16[32,1024]{1,0:T(8,128)(2,1)S(1)}, bf16[32,1024]{1,0:T(8,128)(2,1)S(1)}, u32[]{:S(2)}, u32[]{:S(2)}) %collective-permute-start.34) | collective-permute-done | bytes 65568 | tf_op jit(solution)/shard_map/ppermute | solution.py:86
  101.4 2.0 %collective-permute-start.38 = (bf16[32,1024]{1,0:T(8,128)(2,1)S(1)}, bf16[32,1024]{1,0:T(8,128)(2,1)S(1)}, u32[]{:S(2)}, u32[]{:S(2)}) collective-permute-start(bf16[32,1024]{1,0:T(8,128)(2,1)S(1)} %shard_map.106.refs_0_), channel_id=1, source_target_pairs={{0,6},{1,7},{2,4},{3,5},{4,2},{5,3},{6,0},{7,1},{8,14},{9,15},{10,... | collective-permute-start | bytes 196616 | tf_op jit(solution)/shard_map/ppermute | solution.py:86
  104.2 1.7 %collective-permute-start.36 = (bf16[32,1024]{1,0:T(8,128)(2,1)S(1)}, bf16[32,1024]{1,0:T(8,128)(2,1)S(1)}, u32[]{:S(2)}, u32[]{:S(2)}) collective-permute-start(bf16[32,1024]{1,0:T(8,128)(2,1)S(1)} %shard_map.106.refs_0_), channel_id=1, source_target_pairs={{0,2},{1,3},{2,0},{3,1},{4,6},{5,7},{6,4},{7,5},{8,10},{9,11},{10,... | collective-permute-start | bytes 196616 | tf_op jit(solution)/shard_map/ppermute | solution.py:86
  105.8 1.8 %collective-permute-done.38.refs_3_ = bf16[32,1024]{1,0:T(8,128)(2,1)S(1)} collective-permute-done((bf16[32,1024]{1,0:T(8,128)(2,1)S(1)}, bf16[32,1024]{1,0:T(8,128)(2,1)S(1)}, u32[]{:S(2)}, u32[]{:S(2)}) %collective-permute-start.38) | collective-permute-done | bytes 65568 | tf_op jit(solution)/shard_map/ppermute | solution.py:86
  107.6 1.7 %collective-permute-done.37.refs_2_ = bf16[32,1024]{1,0:T(8,128)(2,1)S(1)} collective-permute-done((bf16[32,1024]{1,0:T(8,128)(2,1)S(1)}, bf16[32,1024]{1,0:T(8,128)(2,1)S(1)}, u32[]{:S(2)}, u32[]{:S(2)}) %collective-permute-start.37) | collective-permute-done | bytes 65568 | tf_op jit(solution)/shard_map/ppermute | solution.py:86
  (88 shorter events, 34.0 us)
Async XLA Ops:
  2.2 12.9 %collective-permute-start.2 = (bf16[360,256]{1,0:T(8,128)(2,1)S(1)}, bf16[360,256]{1,0:T(8,128)(2,1)S(1)}, u32[]{:S(2)}, u32[]{:S(2)}) collective-permute-start(bf16[360,256]{1,0:T(8,128)(2,1)S(1)} %get-tuple-element.38), channel_id=1, source_target_pairs={{0,24},{8,16},{16,8},{24,0},{1,25},{9,17},{17,9},{25,1},{2,26},{10... | collective-permute-start | bytes 552968 | tf_op jit(solution)/shard_map/ppermute | solution.py:82
  9.4 7.6 %collective-permute-start = (bf16[360,256]{1,0:T(8,128)(2,1)S(1)}, bf16[360,256]{1,0:T(8,128)(2,1)S(1)}, u32[]{:S(2)}, u32[]{:S(2)}) collective-permute-start(bf16[360,256]{1,0:T(8,128)(2,1)S(1)} %shard_map.78), channel_id=1, source_target_pairs={{0,8},{8,0},{16,24},{24,16},{1,9},{9,1},{17,25},{25,17},{2,10},{10... | collective-permute-start | bytes 552968 | tf_op jit(solution)/shard_map/ppermute | solution.py:82
  10.0 7.2 %collective-permute-start.1 = (bf16[360,256]{1,0:T(8,128)(2,1)S(1)}, bf16[360,256]{1,0:T(8,128)(2,1)S(1)}, u32[]{:S(2)}, u32[]{:S(2)}) collective-permute-start(bf16[360,256]{1,0:T(8,128)(2,1)S(1)} %get-tuple-element.37), channel_id=1, source_target_pairs={{0,16},{8,24},{16,0},{24,8},{1,17},{9,25},{17,1},{25,9},{2,18},{10... | collective-permute-start | bytes 552968 | tf_op jit(solution)/shard_map/ppermute | solution.py:82
  10.6 10.4 %collective-permute-start.3 = (bf16[336,256]{1,0:T(8,128)(2,1)S(1)}, bf16[336,256]{1,0:T(8,128)(2,1)S(1)}, u32[]{:S(2)}, u32[]{:S(2)}) collective-permute-start(bf16[336,256]{1,0:T(8,128)(2,1)S(1)} %shard_map.80), channel_id=1, source_target_pairs={{0,8},{8,0},{16,24},{24,16},{1,9},{9,1},{17,25},{25,17},{2,10},{10... | collective-permute-start | bytes 516104 | tf_op jit(solution)/shard_map/ppermute | solution.py:82
  13.1 13.3 %collective-permute-start.4 = (bf16[336,256]{1,0:T(8,128)(2,1)S(1)}, bf16[336,256]{1,0:T(8,128)(2,1)S(1)}, u32[]{:S(2)}, u32[]{:S(2)}) collective-permute-start(bf16[336,256]{1,0:T(8,128)(2,1)S(1)} %shard_map.81), channel_id=1, source_target_pairs={{0,16},{8,24},{16,0},{24,8},{1,17},{9,25},{17,1},{25,9},{2,18},{10... | collective-permute-start | bytes 516104 | tf_op jit(solution)/shard_map/ppermute | solution.py:82
  15.1 11.2 %collective-permute-start.5 = (bf16[336,256]{1,0:T(8,128)(2,1)S(1)}, bf16[336,256]{1,0:T(8,128)(2,1)S(1)}, u32[]{:S(2)}, u32[]{:S(2)}) collective-permute-start(bf16[336,256]{1,0:T(8,128)(2,1)S(1)} %shard_map.82), channel_id=1, source_target_pairs={{0,24},{8,16},{16,8},{24,0},{1,25},{9,17},{17,9},{25,1},{2,26},{10... | collective-permute-start | bytes 516104 | tf_op jit(solution)/shard_map/ppermute | solution.py:82
  17.7 12.5 %collective-permute-start.8 = (bf16[176,256]{1,0:T(8,128)(2,1)S(1)}, bf16[176,256]{1,0:T(8,128)(2,1)S(1)}, u32[]{:S(2)}, u32[]{:S(2)}) collective-permute-start(bf16[176,256]{1,0:T(8,128)(2,1)S(1)} %get-tuple-element.40.refs_0_), channel_id=1, source_target_pairs={{0,24},{8,16},{16,8},{24,0},{1,25},{9,17},{17,9},{25,1},{2,26},{10... | collective-permute-start | bytes 270344 | tf_op jit(solution)/shard_map/ppermute | solution.py:82
  19.5 13.1 %collective-permute-start.7 = (bf16[176,256]{1,0:T(8,128)(2,1)S(1)}, bf16[176,256]{1,0:T(8,128)(2,1)S(1)}, u32[]{:S(2)}, u32[]{:S(2)}) collective-permute-start(bf16[176,256]{1,0:T(8,128)(2,1)S(1)} %get-tuple-element.40.refs_0_), channel_id=1, source_target_pairs={{0,16},{8,24},{16,0},{24,8},{1,17},{9,25},{17,1},{25,9},{2,18},{10... | collective-permute-start | bytes 270344 | tf_op jit(solution)/shard_map/ppermute | solution.py:82
  21.0 11.6 %collective-permute-start.6 = (bf16[176,256]{1,0:T(8,128)(2,1)S(1)}, bf16[176,256]{1,0:T(8,128)(2,1)S(1)}, u32[]{:S(2)}, u32[]{:S(2)}) collective-permute-start(bf16[176,256]{1,0:T(8,128)(2,1)S(1)} %get-tuple-element.40.refs_0_), channel_id=1, source_target_pairs={{0,8},{8,0},{16,24},{24,16},{1,9},{9,1},{17,25},{25,17},{2,10},{10... | collective-permute-start | bytes 270344 | tf_op jit(solution)/shard_map/ppermute | solution.py:82
  26.7 6.5 %collective-permute-start.11 = (bf16[168,256]{1,0:T(8,128)(2,1)S(1)}, bf16[168,256]{1,0:T(8,128)(2,1)S(1)}, u32[]{:S(2)}, u32[]{:S(2)}) collective-permute-start(bf16[168,256]{1,0:T(8,128)(2,1)S(1)} %shard_map.83.refs_1_), channel_id=1, source_target_pairs={{0,24},{8,16},{16,8},{24,0},{1,25},{9,17},{17,9},{25,1},{2,26},{10... | collective-permute-start | bytes 258056 | tf_op jit(solution)/shard_map/ppermute | solution.py:82
  37.0 4.9 %collective-permute-start.13 = (bf16[32,1024]{1,0:T(8,128)(2,1)S(1)}, bf16[32,1024]{1,0:T(8,128)(2,1)S(1)}, u32[]{:S(2)}, u32[]{:S(2)}) collective-permute-start(bf16[32,1024]{1,0:T(8,128)(2,1)S(1)} %get-tuple-element.47), channel_id=1, source_target_pairs={{0,2},{1,3},{2,0},{3,1},{4,6},{5,7},{6,4},{7,5},{8,10},{9,11},{10,... | collective-permute-start | bytes 196616 | tf_op jit(solution)/shard_map/ppermute | solution.py:86
  39.3 7.5 %collective-permute-start.14 = (bf16[32,1024]{1,0:T(8,128)(2,1)S(1)}, bf16[32,1024]{1,0:T(8,128)(2,1)S(1)}, u32[]{:S(2)}, u32[]{:S(2)}) collective-permute-start(bf16[32,1024]{1,0:T(8,128)(2,1)S(1)} %get-tuple-element.48), channel_id=1, source_target_pairs={{0,4},{1,5},{2,6},{3,7},{4,0},{5,1},{6,2},{7,3},{8,12},{9,13},{10,... | collective-permute-start | bytes 196616 | tf_op jit(solution)/shard_map/ppermute | solution.py:86
  41.9 6.2 %collective-permute-start.15 = (bf16[32,1024]{1,0:T(8,128)(2,1)S(1)}, bf16[32,1024]{1,0:T(8,128)(2,1)S(1)}, u32[]{:S(2)}, u32[]{:S(2)}) collective-permute-start(bf16[32,1024]{1,0:T(8,128)(2,1)S(1)} %get-tuple-element.49), channel_id=1, source_target_pairs={{0,6},{1,7},{2,4},{3,5},{4,2},{5,3},{6,0},{7,1},{8,14},{9,15},{10,... | collective-permute-start | bytes 196616 | tf_op jit(solution)/shard_map/ppermute | solution.py:86
  48.1 6.3 %collective-permute-start.18 = (bf16[32,1024]{1,0:T(8,128)(2,1)S(1)}, bf16[32,1024]{1,0:T(8,128)(2,1)S(1)}, u32[]{:S(2)}, u32[]{:S(2)}) collective-permute-start(bf16[32,1024]{1,0:T(8,128)(2,1)S(1)} %shard_map.89.refs_0_.refs_4_), channel_id=1, source_target_pairs={{0,6},{1,7},{2,4},{3,5},{4,2},{5,3},{6,0},{7,1},{8,14},{9,15},{10,... | collective-permute-start | bytes 196616 | tf_op jit(solution)/shard_map/ppermute | solution.py:86
  50.2 5.7 %collective-permute-start.17 = (bf16[32,1024]{1,0:T(8,128)(2,1)S(1)}, bf16[32,1024]{1,0:T(8,128)(2,1)S(1)}, u32[]{:S(2)}, u32[]{:S(2)}) collective-permute-start(bf16[32,1024]{1,0:T(8,128)(2,1)S(1)} %shard_map.89.refs_0_.refs_4_), channel_id=1, source_target_pairs={{0,4},{1,5},{2,6},{3,7},{4,0},{5,1},{6,2},{7,3},{8,12},{9,13},{10,... | collective-permute-start | bytes 196616 | tf_op jit(solution)/shard_map/ppermute | solution.py:86
  50.5 5.4 %collective-permute-start.16 = (bf16[32,1024]{1,0:T(8,128)(2,1)S(1)}, bf16[32,1024]{1,0:T(8,128)(2,1)S(1)}, u32[]{:S(2)}, u32[]{:S(2)}) collective-permute-start(bf16[32,1024]{1,0:T(8,128)(2,1)S(1)} %shard_map.89.refs_0_.refs_4_), channel_id=1, source_target_pairs={{0,2},{1,3},{2,0},{3,1},{4,6},{5,7},{6,4},{7,5},{8,10},{9,11},{10,... | collective-permute-start | bytes 196616 | tf_op jit(solution)/shard_map/ppermute | solution.py:86
  59.8 7.6 %collective-permute-start.20 = (bf16[360,256]{1,0:T(8,128)(2,1)S(1)}, bf16[360,256]{1,0:T(8,128)(2,1)S(1)}, u32[]{:S(2)}, u32[]{:S(2)}) collective-permute-start(bf16[360,256]{1,0:T(8,128)(2,1)S(1)} %shard_map.95), channel_id=1, source_target_pairs={{0,8},{8,0},{16,24},{24,16},{1,9},{9,1},{17,25},{25,17},{2,10},{10... | collective-permute-start | bytes 552968 | tf_op jit(solution)/shard_map/ppermute | solution.py:82
  60.9 11.5 %collective-permute-start.21 = (bf16[360,256]{1,0:T(8,128)(2,1)S(1)}, bf16[360,256]{1,0:T(8,128)(2,1)S(1)}, u32[]{:S(2)}, u32[]{:S(2)}) collective-permute-start(bf16[360,256]{1,0:T(8,128)(2,1)S(1)} %shard_map.96), channel_id=1, source_target_pairs={{0,16},{8,24},{16,0},{24,8},{1,17},{9,25},{17,1},{25,9},{2,18},{10... | collective-permute-start | bytes 552968 | tf_op jit(solution)/shard_map/ppermute | solution.py:82
  61.4 11.0 %collective-permute-start.22 = (bf16[360,256]{1,0:T(8,128)(2,1)S(1)}, bf16[360,256]{1,0:T(8,128)(2,1)S(1)}, u32[]{:S(2)}, u32[]{:S(2)}) collective-permute-start(bf16[360,256]{1,0:T(8,128)(2,1)S(1)} %get-tuple-element.52), channel_id=1, source_target_pairs={{0,24},{8,16},{16,8},{24,0},{1,25},{9,17},{17,9},{25,1},{2,26},{10... | collective-permute-start | bytes 552968 | tf_op jit(solution)/shard_map/ppermute | solution.py:82
  64.4 11.5 %collective-permute-start.23 = (bf16[336,256]{1,0:T(8,128)(2,1)S(1)}, bf16[336,256]{1,0:T(8,128)(2,1)S(1)}, u32[]{:S(2)}, u32[]{:S(2)}) collective-permute-start(bf16[336,256]{1,0:T(8,128)(2,1)S(1)} %shard_map.98), channel_id=1, source_target_pairs={{0,8},{8,0},{16,24},{24,16},{1,9},{9,1},{17,25},{25,17},{2,10},{10... | collective-permute-start | bytes 516104 | tf_op jit(solution)/shard_map/ppermute | solution.py:82
  65.5 16.2 %collective-permute-start.24 = (bf16[336,256]{1,0:T(8,128)(2,1)S(1)}, bf16[336,256]{1,0:T(8,128)(2,1)S(1)}, u32[]{:S(2)}, u32[]{:S(2)}) collective-permute-start(bf16[336,256]{1,0:T(8,128)(2,1)S(1)} %shard_map.99), channel_id=1, source_target_pairs={{0,16},{8,24},{16,0},{24,8},{1,17},{9,25},{17,1},{25,9},{2,18},{10... | collective-permute-start | bytes 516104 | tf_op jit(solution)/shard_map/ppermute | solution.py:82
  67.4 14.3 %collective-permute-start.25 = (bf16[336,256]{1,0:T(8,128)(2,1)S(1)}, bf16[336,256]{1,0:T(8,128)(2,1)S(1)}, u32[]{:S(2)}, u32[]{:S(2)}) collective-permute-start(bf16[336,256]{1,0:T(8,128)(2,1)S(1)} %shard_map.100), channel_id=1, source_target_pairs={{0,24},{8,16},{16,8},{24,0},{1,25},{9,17},{17,9},{25,1},{2,26},{10... | collective-permute-start | bytes 516104 | tf_op jit(solution)/shard_map/ppermute | solution.py:82
  72.9 12.4 %collective-permute-start.28 = (bf16[176,256]{1,0:T(8,128)(2,1)S(1)}, bf16[176,256]{1,0:T(8,128)(2,1)S(1)}, u32[]{:S(2)}, u32[]{:S(2)}) collective-permute-start(bf16[176,256]{1,0:T(8,128)(2,1)S(1)} %get-tuple-element.53.refs_0_), channel_id=1, source_target_pairs={{0,24},{8,16},{16,8},{24,0},{1,25},{9,17},{17,9},{25,1},{2,26},{10... | collective-permute-start | bytes 270344 | tf_op jit(solution)/shard_map/ppermute | solution.py:82
  73.9 14.1 %collective-permute-start.27 = (bf16[176,256]{1,0:T(8,128)(2,1)S(1)}, bf16[176,256]{1,0:T(8,128)(2,1)S(1)}, u32[]{:S(2)}, u32[]{:S(2)}) collective-permute-start(bf16[176,256]{1,0:T(8,128)(2,1)S(1)} %get-tuple-element.53.refs_0_), channel_id=1, source_target_pairs={{0,16},{8,24},{16,0},{24,8},{1,17},{9,25},{17,1},{25,9},{2,18},{10... | collective-permute-start | bytes 270344 | tf_op jit(solution)/shard_map/ppermute | solution.py:82
  75.9 12.0 %collective-permute-start.26 = (bf16[176,256]{1,0:T(8,128)(2,1)S(1)}, bf16[176,256]{1,0:T(8,128)(2,1)S(1)}, u32[]{:S(2)}, u32[]{:S(2)}) collective-permute-start(bf16[176,256]{1,0:T(8,128)(2,1)S(1)} %get-tuple-element.53.refs_0_), channel_id=1, source_target_pairs={{0,8},{8,0},{16,24},{24,16},{1,9},{9,1},{17,25},{25,17},{2,10},{10... | collective-permute-start | bytes 270344 | tf_op jit(solution)/shard_map/ppermute | solution.py:82
  82.1 6.5 %collective-permute-start.31 = (bf16[168,256]{1,0:T(8,128)(2,1)S(1)}, bf16[168,256]{1,0:T(8,128)(2,1)S(1)}, u32[]{:S(2)}, u32[]{:S(2)}) collective-permute-start(bf16[168,256]{1,0:T(8,128)(2,1)S(1)} %shard_map.101.refs_1_), channel_id=1, source_target_pairs={{0,24},{8,16},{16,8},{24,0},{1,25},{9,17},{17,9},{25,1},{2,26},{10... | collective-permute-start | bytes 258056 | tf_op jit(solution)/shard_map/ppermute | solution.py:82
  83.2 5.4 %collective-permute-start.30 = (bf16[168,256]{1,0:T(8,128)(2,1)S(1)}, bf16[168,256]{1,0:T(8,128)(2,1)S(1)}, u32[]{:S(2)}, u32[]{:S(2)}) collective-permute-start(bf16[168,256]{1,0:T(8,128)(2,1)S(1)} %shard_map.101.refs_1_), channel_id=1, source_target_pairs={{0,16},{8,24},{16,0},{24,8},{1,17},{9,25},{17,1},{25,9},{2,18},{10... | collective-permute-start | bytes 258056 | tf_op jit(solution)/shard_map/ppermute | solution.py:82
  93.0 8.3 %collective-permute-start.34 = (bf16[32,1024]{1,0:T(8,128)(2,1)S(1)}, bf16[32,1024]{1,0:T(8,128)(2,1)S(1)}, u32[]{:S(2)}, u32[]{:S(2)}) collective-permute-start(bf16[32,1024]{1,0:T(8,128)(2,1)S(1)} %get-tuple-element.59), channel_id=1, source_target_pairs={{0,4},{1,5},{2,6},{3,7},{4,0},{5,1},{6,2},{7,3},{8,12},{9,13},{10,... | collective-permute-start | bytes 196616 | tf_op jit(solution)/shard_map/ppermute | solution.py:86
  94.6 6.7 %collective-permute-start.35 = (bf16[32,1024]{1,0:T(8,128)(2,1)S(1)}, bf16[32,1024]{1,0:T(8,128)(2,1)S(1)}, u32[]{:S(2)}, u32[]{:S(2)}) collective-permute-start(bf16[32,1024]{1,0:T(8,128)(2,1)S(1)} %get-tuple-element.60), channel_id=1, source_target_pairs={{0,6},{1,7},{2,4},{3,5},{4,2},{5,3},{6,0},{7,1},{8,14},{9,15},{10,... | collective-permute-start | bytes 196616 | tf_op jit(solution)/shard_map/ppermute | solution.py:86
  101.4 6.2 %collective-permute-start.38 = (bf16[32,1024]{1,0:T(8,128)(2,1)S(1)}, bf16[32,1024]{1,0:T(8,128)(2,1)S(1)}, u32[]{:S(2)}, u32[]{:S(2)}) collective-permute-start(bf16[32,1024]{1,0:T(8,128)(2,1)S(1)} %shard_map.106.refs_0_), channel_id=1, source_target_pairs={{0,6},{1,7},{2,4},{3,5},{4,2},{5,3},{6,0},{7,1},{8,14},{9,15},{10,... | collective-permute-start | bytes 196616 | tf_op jit(solution)/shard_map/ppermute | solution.py:86
  103.4 5.9 %collective-permute-start.37 = (bf16[32,1024]{1,0:T(8,128)(2,1)S(1)}, bf16[32,1024]{1,0:T(8,128)(2,1)S(1)}, u32[]{:S(2)}, u32[]{:S(2)}) collective-permute-start(bf16[32,1024]{1,0:T(8,128)(2,1)S(1)} %shard_map.106.refs_0_), channel_id=1, source_target_pairs={{0,4},{1,5},{2,6},{3,7},{4,0},{5,1},{6,2},{7,3},{8,12},{9,13},{10,... | collective-permute-start | bytes 196616 | tf_op jit(solution)/shard_map/ppermute | solution.py:86
  104.2 5.2 %collective-permute-start.36 = (bf16[32,1024]{1,0:T(8,128)(2,1)S(1)}, bf16[32,1024]{1,0:T(8,128)(2,1)S(1)}, u32[]{:S(2)}, u32[]{:S(2)}) collective-permute-start(bf16[32,1024]{1,0:T(8,128)(2,1)S(1)} %shard_map.106.refs_0_), channel_id=1, source_target_pairs={{0,2},{1,3},{2,0},{3,1},{4,6},{5,7},{6,4},{7,5},{8,10},{9,11},{10,... | collective-permute-start | bytes 196616 | tf_op jit(solution)/shard_map/ppermute | solution.py:86
  (10 other events, 43.2 us)

commit v5 on v4

--- a/solution.py
+++ b/solution.py
@@ -94,7 +94,7 @@
         count = tokens.shape[0]
         piece = piece_of(units, n_a)
         splits = splits_of(piece)
-        step = -(-(-(-piece // splits)) // 8) * 8
+        step = piece if splits == 1 else -(-2 * piece // 24) * 8
         cuts = [(lo, min(step, piece - lo)) for lo in range(0, piece, step)]
         n_h = len(cuts)
         even = n_a * piece == units
@@ -375,21 +375,20 @@
                 2 * piece * width,
             )[0]
 
-        def down(h, weight, total, others):
+        def down(h, weight, total, others, picks, last):
             lo, size = cuts[h]
-            last = h == n_h - 1
-            n = len(others)
+            n = len(picks)
             shapes = [((count, width), F32)]
             if last:
                 shapes = [((half, width), BF16), ((half, width), F32)]
 
             def body_fn(weight_ref, sum_ref, a_ref, side_ref, *refs):
                 total = sum_ref[...]
-                for s in range(1, n_a):
+                for i, s in enumerate(picks):
                     p = source(a_ref[0], s, n_a)
                     at = pl.ds(aligned(begin(p) + lo), size)
                     keep = None if even else p * piece - begin(p) - lo
-                    total = total + term_of(refs[s - 1][...], weight_ref[at, :], keep)
+                    total = total + term_of(refs[i][...], weight_ref[at, :], keep)
                 if not last:
                     refs[n][...] = total
                     return
@@ -402,11 +401,11 @@
 
             return call(
                 body_fn,
-                [weight, total, me_a, me_c, *others],
+                [weight, total, me_a, me_c, *[others[s - 1] for s in picks]],
                 [VMEM] * 2 + [SMEM] * 2 + [VMEM] * n,
                 shapes,
-                2 * size * (n_a - 1) * width * count,
-                2 * size * (n_a - 1) * width,
+                2 * size * n * width * count,
+                2 * size * n * width,
                 [pltpu.VMEM((count, width), F32)] if last else (),
             )
 
@@ -480,8 +479,11 @@
                 mine.append(hidden)
                 others.append([send_a(hidden, s) for s in range(1, n_a)])
             total = down_own(weight, mine)
-            for h in range(n_h):
-                out = down(h, weight, total, others[h])
+            turns = [(h, list(range(1, n_a))) for h in range(n_h)]
+            if n_a == 4:
+                turns = turns[:-1] + [(n_h - 1, [3, 1]), (n_h - 1, [2])]
+            for i, (h, picks) in enumerate(turns):
+                out = down(h, weight, total, others[h], picks, i == len(turns) - 1)
                 total = out[0]
             away, kept = out
             dealt = deal(kept, send_core(away))

time: 112 us -> 112 us (level)
  starting transfers between devices: 47.5 us -> 50.6 us
  waiting for transfers between devices: 39.5 us -> 36.5 us
    ppermute x24, starting transfers between devices: 28.9 us -> 32.5 us  [send_a(): return lax.ppermute(value, 'ra', [(i, peer(i, s, n_a)) for i in range(n_a)])]
    ppermute x24, waiting for transfers between devices: 17.2 us -> 14.2 us  [send_a(): return lax.ppermute(value, 'ra', [(i, peer(i, s, n_a)) for i in range(n_a)])]
    pallas_call x36 -> x38, Pallas kernels: 24.4 us -> 24.4 us  [call(): pl.pallas_call(body, in_specs=specs, out_specs=[VMEM] * len(shapes), out_...]
  transfers between devices with their start and end apart: 40 -> 40, of which waited for: 18 -> 19; matrix products, arithmetic and copies ran while one was open for 0% -> 0% of each run, Pallas kernels for 17% -> 17%
where the time goes in v5:
time: 112 us
  starting transfers between devices  50.6 us (45%)
  waiting for transfers between devices  36.5 us (33%)
  Pallas kernels  24.4 us (22%)
    ppermute x24, starting transfers between devices, send_a(): return lax.ppermute(value, 'ra', [(i, peer(i, s, n_a)) for i in range(n_a)])  32.5 us
    pallas_call x38, Pallas kernels, call(): pl.pallas_call(body, in_specs=specs, out_specs=[VMEM] * len(shapes), out_...  24.4 us
    ppermute x12, starting transfers between devices, send_z(): return lax.ppermute(value, 'cb', pairs)  17.8 us
    ppermute x12, waiting for transfers between devices, send_z(): return lax.ppermute(value, 'cb', pairs)  17.8 us
    ppermute x24, waiting for transfers between devices, send_a(): return lax.ppermute(value, 'ra', [(i, peer(i, s, n_a)) for i in range(n_a)])  14.2 us
    ppermute x4, waiting for transfers between devices, send_core(): return lax.ppermute(value, 'cb', [(i, i ^ 1) for i in range(n_c)])  4.57 us
  transfers between devices with their start and end apart: 40, of which 19 were waited for; matrix products, arithmetic and copies ran while one was open for 0% of the time, Pallas kernels for 17%

profile of v5, /device:TPU:0, one launch (start us, length us, event | category | flops | bytes accessed | tf_op | source)
XLA Modules:
  0.0 112.0 jit_solution(9564578038347922221)
XLA Ops:
  0.0 2.2 %shard_map.73 = (bf16[472,256]{1,0:T(8,128)(2,1)S(1)}, bf16[256,1024]{1,0:T(8,128)(2,1)S(1)}, bf16[8,256]{1,0:T(8,128)(2,1)S(1)}) custom-call(s32[1]{0:T(128)} %bitcast.refs_0_.a_ref, bf16[2,1376,1024]{2,1,0:T(8,128)(2,1)} %bitcast.6, bf16[2,1376,1024]{2,1,0:T(8,128)(2,1)} %bitcast.9, bf16[256,1024]{1,0:T(8,128)(2,1)} %refs_4_.3, f32[2,1024]{1,0:T(2,128)} %refs_5_.1, ...), custom_call_target="tpu_custom_call" | custom-call | flops 243269632 | bytes 950272 | tf_op jit(solution)/shard_map/pallas_call | solution.py:29
  2.2 4.0 %collective-permute-start.2 = (bf16[472,256]{1,0:T(8,128)(2,1)S(1)}, bf16[472,256]{1,0:T(8,128)(2,1)S(1)}, u32[]{:S(2)}, u32[]{:S(2)}) collective-permute-start(bf16[472,256]{1,0:T(8,128)(2,1)S(1)} %get-tuple-element.38), channel_id=1, source_target_pairs={{0,24},{8,16},{16,8},{24,0},{1,25},{9,17},{17,9},{25,1},{2,26},{10... | collective-permute-start | bytes 725000 | tf_op jit(solution)/shard_map/ppermute | solution.py:82
  6.2 2.7 %shard_map.74 = (bf16[472,256]{1,0:T(8,128)(2,1)S(1)}, bf16[1376,1024]{1,0:T(8,128)(2,1)S(1)}, bf16[1376,1024]{1,0:T(8,128)(2,1)S(1)}, f32[344,16]{1,0:T(8,128)S(1)}) custom-call(s32[1]{0:T(128)} %bitcast.refs_0_.a_ref, bf16[2,1376,1024]{2,1,0:T(8,128)(2,1)} %bitcast.7, bf16[2,1376,1024]{2,1,0:T(8,128)(2,1)} %bitcast.10, ...), custom_call_target="tpu_custom_call" | custom-call | flops 243269632 | bytes 950272 | tf_op jit(solution)/shard_map/pallas_call | solution.py:29
  10.5 2.0 %collective-permute-start.3 = (bf16[224,256]{1,0:T(8,128)(2,1)S(1)}, bf16[224,256]{1,0:T(8,128)(2,1)S(1)}, u32[]{:S(2)}, u32[]{:S(2)}) collective-permute-start(bf16[224,256]{1,0:T(8,128)(2,1)S(1)} %shard_map.80), channel_id=1, source_target_pairs={{0,8},{8,0},{16,24},{24,16},{1,9},{9,1},{17,25},{25,17},{2,10},{10... | collective-permute-start | bytes 344072 | tf_op jit(solution)/shard_map/ppermute | solution.py:82
  13.0 1.6 %collective-permute-start.4 = (bf16[224,256]{1,0:T(8,128)(2,1)S(1)}, bf16[224,256]{1,0:T(8,128)(2,1)S(1)}, u32[]{:S(2)}, u32[]{:S(2)}) collective-permute-start(bf16[224,256]{1,0:T(8,128)(2,1)S(1)} %shard_map.81), channel_id=1, source_target_pairs={{0,16},{8,24},{16,0},{24,8},{1,17},{9,25},{17,1},{25,9},{2,18},{10... | collective-permute-start | bytes 344072 | tf_op jit(solution)/shard_map/ppermute | solution.py:82
  16.3 1.9 %collective-permute-done.refs_1_ = bf16[472,256]{1,0:T(8,128)(2,1)S(1)} collective-permute-done((bf16[472,256]{1,0:T(8,128)(2,1)S(1)}, bf16[472,256]{1,0:T(8,128)(2,1)S(1)}, u32[]{:S(2)}, u32[]{:S(2)}) %collective-permute-start) | collective-permute-done | bytes 241696 | tf_op jit(solution)/shard_map/ppermute | solution.py:82
  19.2 2.0 %collective-permute-start.8 = (bf16[232,256]{1,0:T(8,128)(2,1)S(1)}, bf16[232,256]{1,0:T(8,128)(2,1)S(1)}, u32[]{:S(2)}, u32[]{:S(2)}) collective-permute-start(bf16[232,256]{1,0:T(8,128)(2,1)S(1)} %get-tuple-element.40.refs_0_), channel_id=1, source_target_pairs={{0,24},{8,16},{16,8},{24,0},{1,25},{9,17},{17,9},{25,1},{2,26},{10... | collective-permute-start | bytes 356360 | tf_op jit(solution)/shard_map/ppermute | solution.py:82
  24.0 2.6 %collective-permute-start.10 = (bf16[112,256]{1,0:T(8,128)(2,1)S(1)}, bf16[112,256]{1,0:T(8,128)(2,1)S(1)}, u32[]{:S(2)}, u32[]{:S(2)}) collective-permute-start(bf16[112,256]{1,0:T(8,128)(2,1)S(1)} %shard_map.83.refs_1_), channel_id=1, source_target_pairs={{0,8},{8,0},{16,24},{24,16},{1,9},{9,1},{17,25},{25,17},{2,10},{10... | collective-permute-start | bytes 172040 | tf_op jit(solution)/shard_map/ppermute | solution.py:82
  27.2 1.8 %shard_map.76.weight_ref = bf16[1376,1024]{1,0:T(8,128)(2,1)S(1)} custom-call(bf16[2,1376,1024]{2,1,0:T(8,128)(2,1)} %refs_0_.3, bf16[224,256]{1,0:T(8,128)(2,1)S(1)} %shard_map.75.refs_1_.refs_0_), custom_call_target="tpu_custom_call" | custom-call | flops 240473424 | bytes 2818048 | tf_op jit(solution)/shard_map/pallas_call | solution.py:29
  35.3 1.8 %collective-permute-start.13 = (bf16[32,1024]{1,0:T(8,128)(2,1)S(1)}, bf16[32,1024]{1,0:T(8,128)(2,1)S(1)}, u32[]{:S(2)}, u32[]{:S(2)}) collective-permute-start(bf16[32,1024]{1,0:T(8,128)(2,1)S(1)} %get-tuple-element.47), channel_id=1, source_target_pairs={{0,2},{1,3},{2,0},{3,1},{4,6},{5,7},{6,4},{7,5},{8,10},{9,11},{10,... | collective-permute-start | bytes 196616 | tf_op jit(solution)/shard_map/ppermute | solution.py:86
  37.1 2.6 %collective-permute-start.14 = (bf16[32,1024]{1,0:T(8,128)(2,1)S(1)}, bf16[32,1024]{1,0:T(8,128)(2,1)S(1)}, u32[]{:S(2)}, u32[]{:S(2)}) collective-permute-start(bf16[32,1024]{1,0:T(8,128)(2,1)S(1)} %get-tuple-element.48), channel_id=1, source_target_pairs={{0,4},{1,5},{2,6},{3,7},{4,0},{5,1},{6,2},{7,3},{8,12},{9,13},{10,... | collective-permute-start | bytes 196616 | tf_op jit(solution)/shard_map/ppermute | solution.py:86
  39.8 4.9 %collective-permute-done.14.refs_1_ = bf16[32,1024]{1,0:T(8,128)(2,1)S(1)} collective-permute-done((bf16[32,1024]{1,0:T(8,128)(2,1)S(1)}, bf16[32,1024]{1,0:T(8,128)(2,1)S(1)}, u32[]{:S(2)}, u32[]{:S(2)}) %collective-permute-start.14) | collective-permute-done | bytes 65568 | tf_op jit(solution)/shard_map/ppermute | solution.py:86
  45.9 2.0 %collective-permute-start.18 = (bf16[32,1024]{1,0:T(8,128)(2,1)S(1)}, bf16[32,1024]{1,0:T(8,128)(2,1)S(1)}, u32[]{:S(2)}, u32[]{:S(2)}) collective-permute-start(bf16[32,1024]{1,0:T(8,128)(2,1)S(1)} %shard_map.90.refs_0_.refs_4_), channel_id=1, source_target_pairs={{0,6},{1,7},{2,4},{3,5},{4,2},{5,3},{6,0},{7,1},{8,14},{9,15},{10,... | collective-permute-start | bytes 196616 | tf_op jit(solution)/shard_map/ppermute | solution.py:86
  48.3 2.1 %collective-permute-start.16 = (bf16[32,1024]{1,0:T(8,128)(2,1)S(1)}, bf16[32,1024]{1,0:T(8,128)(2,1)S(1)}, u32[]{:S(2)}, u32[]{:S(2)}) collective-permute-start(bf16[32,1024]{1,0:T(8,128)(2,1)S(1)} %shard_map.90.refs_0_.refs_4_), channel_id=1, source_target_pairs={{0,2},{1,3},{2,0},{3,1},{4,6},{5,7},{6,4},{7,5},{8,10},{9,11},{10,... | collective-permute-start | bytes 196616 | tf_op jit(solution)/shard_map/ppermute | solution.py:86
  50.4 1.8 %collective-permute-done.18.refs_3_ = bf16[32,1024]{1,0:T(8,128)(2,1)S(1)} collective-permute-done((bf16[32,1024]{1,0:T(8,128)(2,1)S(1)}, bf16[32,1024]{1,0:T(8,128)(2,1)S(1)}, u32[]{:S(2)}, u32[]{:S(2)}) %collective-permute-start.18) | collective-permute-done | bytes 65568 | tf_op jit(solution)/shard_map/ppermute | solution.py:86
  52.2 1.5 %collective-permute-done.17.refs_2_ = bf16[32,1024]{1,0:T(8,128)(2,1)S(1)} collective-permute-done((bf16[32,1024]{1,0:T(8,128)(2,1)S(1)}, bf16[32,1024]{1,0:T(8,128)(2,1)S(1)}, u32[]{:S(2)}, u32[]{:S(2)}) %collective-permute-start.17) | collective-permute-done | bytes 65568 | tf_op jit(solution)/shard_map/ppermute | solution.py:86
  53.9 2.7 %shard_map.89 = (bf16[1376,1024]{1,0:T(8,128)(2,1)S(1)}, bf16[1376,1024]{1,0:T(8,128)(2,1)S(1)}) custom-call(bf16[2,1376,1024]{2,1,0:T(8,128)(2,1)} %bitcast.8, bf16[2,1376,1024]{2,1,0:T(8,128)(2,1)} %bitcast.11, f32[32,1024]{1,0:T(8,128)S(1)} %get-tuple-element.44.refs_2_.own_ref), custom_call_target="tpu_custom_call" | custom-call | flops 480946848 | bytes 5636096 | tf_op jit(solution)/shard_map/pallas_call | solution.py:29
  57.6 2.0 %collective-permute-start.20 = (bf16[472,256]{1,0:T(8,128)(2,1)S(1)}, bf16[472,256]{1,0:T(8,128)(2,1)S(1)}, u32[]{:S(2)}, u32[]{:S(2)}) collective-permute-start(bf16[472,256]{1,0:T(8,128)(2,1)S(1)} %shard_map.96), channel_id=1, source_target_pairs={{0,8},{8,0},{16,24},{24,16},{1,9},{9,1},{17,25},{25,17},{2,10},{10... | collective-permute-start | bytes 725000 | tf_op jit(solution)/shard_map/ppermute | solution.py:82
  62.1 2.0 %collective-permute-start.23 = (bf16[224,256]{1,0:T(8,128)(2,1)S(1)}, bf16[224,256]{1,0:T(8,128)(2,1)S(1)}, u32[]{:S(2)}, u32[]{:S(2)}) collective-permute-start(bf16[224,256]{1,0:T(8,128)(2,1)S(1)} %shard_map.99), channel_id=1, source_target_pairs={{0,8},{8,0},{16,24},{24,16},{1,9},{9,1},{17,25},{25,17},{2,10},{10... | collective-permute-start | bytes 344072 | tf_op jit(solution)/shard_map/ppermute | solution.py:82
  66.4 2.1 %collective-permute-start.25 = (bf16[224,256]{1,0:T(8,128)(2,1)S(1)}, bf16[224,256]{1,0:T(8,128)(2,1)S(1)}, u32[]{:S(2)}, u32[]{:S(2)}) collective-permute-start(bf16[224,256]{1,0:T(8,128)(2,1)S(1)} %shard_map.101), channel_id=1, source_target_pairs={{0,24},{8,16},{16,8},{24,0},{1,25},{9,17},{17,9},{25,1},{2,26},{10... | collective-permute-start | bytes 344072 | tf_op jit(solution)/shard_map/ppermute | solution.py:82
  69.0 5.3 %collective-permute-done.21.refs_2_ = bf16[472,256]{1,0:T(8,128)(2,1)S(1)} collective-permute-done((bf16[472,256]{1,0:T(8,128)(2,1)S(1)}, bf16[472,256]{1,0:T(8,128)(2,1)S(1)}, u32[]{:S(2)}, u32[]{:S(2)}) %collective-permute-start.21) | collective-permute-done | bytes 241696 | tf_op jit(solution)/shard_map/ppermute | solution.py:82
  76.3 2.2 %collective-permute-start.26 = (bf16[232,256]{1,0:T(8,128)(2,1)S(1)}, bf16[232,256]{1,0:T(8,128)(2,1)S(1)}, u32[]{:S(2)}, u32[]{:S(2)}) collective-permute-start(bf16[232,256]{1,0:T(8,128)(2,1)S(1)} %get-tuple-element.53.refs_0_), channel_id=1, source_target_pairs={{0,8},{8,0},{16,24},{24,16},{1,9},{9,1},{17,25},{25,17},{2,10},{10... | collective-permute-start | bytes 356360 | tf_op jit(solution)/shard_map/ppermute | solution.py:82
  78.9 2.6 %collective-permute-done.24.refs_2_ = bf16[224,256]{1,0:T(8,128)(2,1)S(1)} collective-permute-done((bf16[224,256]{1,0:T(8,128)(2,1)S(1)}, bf16[224,256]{1,0:T(8,128)(2,1)S(1)}, u32[]{:S(2)}, u32[]{:S(2)}) %collective-permute-start.24) | collective-permute-done | bytes 114720 | tf_op jit(solution)/shard_map/ppermute | solution.py:82
  81.9 2.2 %collective-permute-start.29 = (bf16[112,256]{1,0:T(8,128)(2,1)S(1)}, bf16[112,256]{1,0:T(8,128)(2,1)S(1)}, u32[]{:S(2)}, u32[]{:S(2)}) collective-permute-start(bf16[112,256]{1,0:T(8,128)(2,1)S(1)} %shard_map.102.refs_1_), channel_id=1, source_target_pairs={{0,24},{8,16},{16,8},{24,0},{1,25},{9,17},{17,9},{25,1},{2,26},{10... | collective-permute-start | bytes 172040 | tf_op jit(solution)/shard_map/ppermute | solution.py:82
  84.1 1.8 %shard_map.94.weight_ref = bf16[1376,1024]{1,0:T(8,128)(2,1)S(1)} custom-call(bf16[2,1376,1024]{2,1,0:T(8,128)(2,1)} %refs_0_.3, bf16[224,256]{1,0:T(8,128)(2,1)S(1)} %shard_map.93.refs_1_.refs_0_), custom_call_target="tpu_custom_call" | custom-call | flops 240473424 | bytes 2818048 | tf_op jit(solution)/shard_map/pallas_call | solution.py:29
  93.2 1.6 %collective-permute-start.34 = (bf16[32,1024]{1,0:T(8,128)(2,1)S(1)}, bf16[32,1024]{1,0:T(8,128)(2,1)S(1)}, u32[]{:S(2)}, u32[]{:S(2)}) collective-permute-start(bf16[32,1024]{1,0:T(8,128)(2,1)S(1)} %get-tuple-element.59), channel_id=1, source_target_pairs={{0,4},{1,5},{2,6},{3,7},{4,0},{5,1},{6,2},{7,3},{8,12},{9,13},{10,... | collective-permute-start | bytes 196616 | tf_op jit(solution)/shard_map/ppermute | solution.py:86
  94.9 1.9 %collective-permute-start.35 = (bf16[32,1024]{1,0:T(8,128)(2,1)S(1)}, bf16[32,1024]{1,0:T(8,128)(2,1)S(1)}, u32[]{:S(2)}, u32[]{:S(2)}) collective-permute-start(bf16[32,1024]{1,0:T(8,128)(2,1)S(1)} %get-tuple-element.60), channel_id=1, source_target_pairs={{0,6},{1,7},{2,4},{3,5},{4,2},{5,3},{6,0},{7,1},{8,14},{9,15},{10,... | collective-permute-start | bytes 196616 | tf_op jit(solution)/shard_map/ppermute | solution.py:86
  96.7 4.8 %collective-permute-done.34.refs_1_ = bf16[32,1024]{1,0:T(8,128)(2,1)S(1)} collective-permute-done((bf16[32,1024]{1,0:T(8,128)(2,1)S(1)}, bf16[32,1024]{1,0:T(8,128)(2,1)S(1)}, u32[]{:S(2)}, u32[]{:S(2)}) %collective-permute-start.34) | collective-permute-done | bytes 65568 | tf_op jit(solution)/shard_map/ppermute | solution.py:86
  101.6 2.1 %collective-permute-start.38 = (bf16[32,1024]{1,0:T(8,128)(2,1)S(1)}, bf16[32,1024]{1,0:T(8,128)(2,1)S(1)}, u32[]{:S(2)}, u32[]{:S(2)}) collective-permute-start(bf16[32,1024]{1,0:T(8,128)(2,1)S(1)} %shard_map.108.refs_0_), channel_id=1, source_target_pairs={{0,6},{1,7},{2,4},{3,5},{4,2},{5,3},{6,0},{7,1},{8,14},{9,15},{10,... | collective-permute-start | bytes 196616 | tf_op jit(solution)/shard_map/ppermute | solution.py:86
  104.3 1.7 %collective-permute-start.36 = (bf16[32,1024]{1,0:T(8,128)(2,1)S(1)}, bf16[32,1024]{1,0:T(8,128)(2,1)S(1)}, u32[]{:S(2)}, u32[]{:S(2)}) collective-permute-start(bf16[32,1024]{1,0:T(8,128)(2,1)S(1)} %shard_map.108.refs_0_), channel_id=1, source_target_pairs={{0,2},{1,3},{2,0},{3,1},{4,6},{5,7},{6,4},{7,5},{8,10},{9,11},{10,... | collective-permute-start | bytes 196616 | tf_op jit(solution)/shard_map/ppermute | solution.py:86
  106.0 1.9 %collective-permute-done.38.refs_3_ = bf16[32,1024]{1,0:T(8,128)(2,1)S(1)} collective-permute-done((bf16[32,1024]{1,0:T(8,128)(2,1)S(1)}, bf16[32,1024]{1,0:T(8,128)(2,1)S(1)}, u32[]{:S(2)}, u32[]{:S(2)}) %collective-permute-start.38) | collective-permute-done | bytes 65568 | tf_op jit(solution)/shard_map/ppermute | solution.py:86
  107.9 1.6 %collective-permute-done.37.refs_2_ = bf16[32,1024]{1,0:T(8,128)(2,1)S(1)} collective-permute-done((bf16[32,1024]{1,0:T(8,128)(2,1)S(1)}, bf16[32,1024]{1,0:T(8,128)(2,1)S(1)}, u32[]{:S(2)}, u32[]{:S(2)}) %collective-permute-start.37) | collective-permute-done | bytes 65568 | tf_op jit(solution)/shard_map/ppermute | solution.py:86
  (90 shorter events, 35.5 us)
Async XLA Ops:
  2.2 12.8 %collective-permute-start.2 = (bf16[472,256]{1,0:T(8,128)(2,1)S(1)}, bf16[472,256]{1,0:T(8,128)(2,1)S(1)}, u32[]{:S(2)}, u32[]{:S(2)}) collective-permute-start(bf16[472,256]{1,0:T(8,128)(2,1)S(1)} %get-tuple-element.38), channel_id=1, source_target_pairs={{0,24},{8,16},{16,8},{24,0},{1,25},{9,17},{17,9},{25,1},{2,26},{10... | collective-permute-start | bytes 725000 | tf_op jit(solution)/shard_map/ppermute | solution.py:82
  9.4 8.8 %collective-permute-start = (bf16[472,256]{1,0:T(8,128)(2,1)S(1)}, bf16[472,256]{1,0:T(8,128)(2,1)S(1)}, u32[]{:S(2)}, u32[]{:S(2)}) collective-permute-start(bf16[472,256]{1,0:T(8,128)(2,1)S(1)} %shard_map.78), channel_id=1, source_target_pairs={{0,8},{8,0},{16,24},{24,16},{1,9},{9,1},{17,25},{25,17},{2,10},{10... | collective-permute-start | bytes 725000 | tf_op jit(solution)/shard_map/ppermute | solution.py:82
  10.0 8.6 %collective-permute-start.1 = (bf16[472,256]{1,0:T(8,128)(2,1)S(1)}, bf16[472,256]{1,0:T(8,128)(2,1)S(1)}, u32[]{:S(2)}, u32[]{:S(2)}) collective-permute-start(bf16[472,256]{1,0:T(8,128)(2,1)S(1)} %get-tuple-element.37), channel_id=1, source_target_pairs={{0,16},{8,24},{16,0},{24,8},{1,17},{9,25},{17,1},{25,9},{2,18},{10... | collective-permute-start | bytes 725000 | tf_op jit(solution)/shard_map/ppermute | solution.py:82
  10.5 11.8 %collective-permute-start.3 = (bf16[224,256]{1,0:T(8,128)(2,1)S(1)}, bf16[224,256]{1,0:T(8,128)(2,1)S(1)}, u32[]{:S(2)}, u32[]{:S(2)}) collective-permute-start(bf16[224,256]{1,0:T(8,128)(2,1)S(1)} %shard_map.80), channel_id=1, source_target_pairs={{0,8},{8,0},{16,24},{24,16},{1,9},{9,1},{17,25},{25,17},{2,10},{10... | collective-permute-start | bytes 344072 | tf_op jit(solution)/shard_map/ppermute | solution.py:82
  13.0 10.7 %collective-permute-start.4 = (bf16[224,256]{1,0:T(8,128)(2,1)S(1)}, bf16[224,256]{1,0:T(8,128)(2,1)S(1)}, u32[]{:S(2)}, u32[]{:S(2)}) collective-permute-start(bf16[224,256]{1,0:T(8,128)(2,1)S(1)} %shard_map.81), channel_id=1, source_target_pairs={{0,16},{8,24},{16,0},{24,8},{1,17},{9,25},{17,1},{25,9},{2,18},{10... | collective-permute-start | bytes 344072 | tf_op jit(solution)/shard_map/ppermute | solution.py:82
  15.0 8.6 %collective-permute-start.5 = (bf16[224,256]{1,0:T(8,128)(2,1)S(1)}, bf16[224,256]{1,0:T(8,128)(2,1)S(1)}, u32[]{:S(2)}, u32[]{:S(2)}) collective-permute-start(bf16[224,256]{1,0:T(8,128)(2,1)S(1)} %shard_map.82), channel_id=1, source_target_pairs={{0,24},{8,16},{16,8},{24,0},{1,25},{9,17},{17,9},{25,1},{2,26},{10... | collective-permute-start | bytes 344072 | tf_op jit(solution)/shard_map/ppermute | solution.py:82
  19.2 9.8 %collective-permute-start.8 = (bf16[232,256]{1,0:T(8,128)(2,1)S(1)}, bf16[232,256]{1,0:T(8,128)(2,1)S(1)}, u32[]{:S(2)}, u32[]{:S(2)}) collective-permute-start(bf16[232,256]{1,0:T(8,128)(2,1)S(1)} %get-tuple-element.40.refs_0_), channel_id=1, source_target_pairs={{0,24},{8,16},{16,8},{24,0},{1,25},{9,17},{17,9},{25,1},{2,26},{10... | collective-permute-start | bytes 356360 | tf_op jit(solution)/shard_map/ppermute | solution.py:82
  21.2 9.2 %collective-permute-start.7 = (bf16[232,256]{1,0:T(8,128)(2,1)S(1)}, bf16[232,256]{1,0:T(8,128)(2,1)S(1)}, u32[]{:S(2)}, u32[]{:S(2)}) collective-permute-start(bf16[232,256]{1,0:T(8,128)(2,1)S(1)} %get-tuple-element.40.refs_0_), channel_id=1, source_target_pairs={{0,16},{8,24},{16,0},{24,8},{1,17},{9,25},{17,1},{25,9},{2,18},{10... | collective-permute-start | bytes 356360 | tf_op jit(solution)/shard_map/ppermute | solution.py:82
  22.3 8.1 %collective-permute-start.6 = (bf16[232,256]{1,0:T(8,128)(2,1)S(1)}, bf16[232,256]{1,0:T(8,128)(2,1)S(1)}, u32[]{:S(2)}, u32[]{:S(2)}) collective-permute-start(bf16[232,256]{1,0:T(8,128)(2,1)S(1)} %get-tuple-element.40.refs_0_), channel_id=1, source_target_pairs={{0,8},{8,0},{16,24},{24,16},{1,9},{9,1},{17,25},{25,17},{2,10},{10... | collective-permute-start | bytes 356360 | tf_op jit(solution)/shard_map/ppermute | solution.py:82
  24.0 7.1 %collective-permute-start.10 = (bf16[112,256]{1,0:T(8,128)(2,1)S(1)}, bf16[112,256]{1,0:T(8,128)(2,1)S(1)}, u32[]{:S(2)}, u32[]{:S(2)}) collective-permute-start(bf16[112,256]{1,0:T(8,128)(2,1)S(1)} %shard_map.83.refs_1_), channel_id=1, source_target_pairs={{0,8},{8,0},{16,24},{24,16},{1,9},{9,1},{17,25},{25,17},{2,10},{10... | collective-permute-start | bytes 172040 | tf_op jit(solution)/shard_map/ppermute | solution.py:82
  26.6 5.1 %collective-permute-start.9 = (bf16[112,256]{1,0:T(8,128)(2,1)S(1)}, bf16[112,256]{1,0:T(8,128)(2,1)S(1)}, u32[]{:S(2)}, u32[]{:S(2)}) collective-permute-start(bf16[112,256]{1,0:T(8,128)(2,1)S(1)} %shard_map.83.refs_1_), channel_id=1, source_target_pairs={{0,24},{8,16},{16,8},{24,0},{1,25},{9,17},{17,9},{25,1},{2,26},{10... | collective-permute-start | bytes 172040 | tf_op jit(solution)/shard_map/ppermute | solution.py:82
  37.1 7.5 %collective-permute-start.14 = (bf16[32,1024]{1,0:T(8,128)(2,1)S(1)}, bf16[32,1024]{1,0:T(8,128)(2,1)S(1)}, u32[]{:S(2)}, u32[]{:S(2)}) collective-permute-start(bf16[32,1024]{1,0:T(8,128)(2,1)S(1)} %get-tuple-element.48), channel_id=1, source_target_pairs={{0,4},{1,5},{2,6},{3,7},{4,0},{5,1},{6,2},{7,3},{8,12},{9,13},{10,... | collective-permute-start | bytes 196616 | tf_op jit(solution)/shard_map/ppermute | solution.py:86
  39.7 6.2 %collective-permute-start.15 = (bf16[32,1024]{1,0:T(8,128)(2,1)S(1)}, bf16[32,1024]{1,0:T(8,128)(2,1)S(1)}, u32[]{:S(2)}, u32[]{:S(2)}) collective-permute-start(bf16[32,1024]{1,0:T(8,128)(2,1)S(1)} %get-tuple-element.49), channel_id=1, source_target_pairs={{0,6},{1,7},{2,4},{3,5},{4,2},{5,3},{6,0},{7,1},{8,14},{9,15},{10,... | collective-permute-start | bytes 196616 | tf_op jit(solution)/shard_map/ppermute | solution.py:86
  45.9 6.3 %collective-permute-start.18 = (bf16[32,1024]{1,0:T(8,128)(2,1)S(1)}, bf16[32,1024]{1,0:T(8,128)(2,1)S(1)}, u32[]{:S(2)}, u32[]{:S(2)}) collective-permute-start(bf16[32,1024]{1,0:T(8,128)(2,1)S(1)} %shard_map.90.refs_0_.refs_4_), channel_id=1, source_target_pairs={{0,6},{1,7},{2,4},{3,5},{4,2},{5,3},{6,0},{7,1},{8,14},{9,15},{10,... | collective-permute-start | bytes 196616 | tf_op jit(solution)/shard_map/ppermute | solution.py:86
  48.0 5.8 %collective-permute-start.17 = (bf16[32,1024]{1,0:T(8,128)(2,1)S(1)}, bf16[32,1024]{1,0:T(8,128)(2,1)S(1)}, u32[]{:S(2)}, u32[]{:S(2)}) collective-permute-start(bf16[32,1024]{1,0:T(8,128)(2,1)S(1)} %shard_map.90.refs_0_.refs_4_), channel_id=1, source_target_pairs={{0,4},{1,5},{2,6},{3,7},{4,0},{5,1},{6,2},{7,3},{8,12},{9,13},{10,... | collective-permute-start | bytes 196616 | tf_op jit(solution)/shard_map/ppermute | solution.py:86
  48.3 5.5 %collective-permute-start.16 = (bf16[32,1024]{1,0:T(8,128)(2,1)S(1)}, bf16[32,1024]{1,0:T(8,128)(2,1)S(1)}, u32[]{:S(2)}, u32[]{:S(2)}) collective-permute-start(bf16[32,1024]{1,0:T(8,128)(2,1)S(1)} %shard_map.90.refs_0_.refs_4_), channel_id=1, source_target_pairs={{0,2},{1,3},{2,0},{3,1},{4,6},{5,7},{6,4},{7,5},{8,10},{9,11},{10,... | collective-permute-start | bytes 196616 | tf_op jit(solution)/shard_map/ppermute | solution.py:86
  57.6 8.8 %collective-permute-start.20 = (bf16[472,256]{1,0:T(8,128)(2,1)S(1)}, bf16[472,256]{1,0:T(8,128)(2,1)S(1)}, u32[]{:S(2)}, u32[]{:S(2)}) collective-permute-start(bf16[472,256]{1,0:T(8,128)(2,1)S(1)} %shard_map.96), channel_id=1, source_target_pairs={{0,8},{8,0},{16,24},{24,16},{1,9},{9,1},{17,25},{25,17},{2,10},{10... | collective-permute-start | bytes 725000 | tf_op jit(solution)/shard_map/ppermute | solution.py:82
  60.1 14.2 %collective-permute-start.21 = (bf16[472,256]{1,0:T(8,128)(2,1)S(1)}, bf16[472,256]{1,0:T(8,128)(2,1)S(1)}, u32[]{:S(2)}, u32[]{:S(2)}) collective-permute-start(bf16[472,256]{1,0:T(8,128)(2,1)S(1)} %shard_map.97), channel_id=1, source_target_pairs={{0,16},{8,24},{16,0},{24,8},{1,17},{9,25},{17,1},{25,9},{2,18},{10... | collective-permute-start | bytes 725000 | tf_op jit(solution)/shard_map/ppermute | solution.py:82
  60.9 13.4 %collective-permute-start.22 = (bf16[472,256]{1,0:T(8,128)(2,1)S(1)}, bf16[472,256]{1,0:T(8,128)(2,1)S(1)}, u32[]{:S(2)}, u32[]{:S(2)}) collective-permute-start(bf16[472,256]{1,0:T(8,128)(2,1)S(1)} %get-tuple-element.52), channel_id=1, source_target_pairs={{0,24},{8,16},{16,8},{24,0},{1,25},{9,17},{17,9},{25,1},{2,26},{10... | collective-permute-start | bytes 725000 | tf_op jit(solution)/shard_map/ppermute | solution.py:82
  62.1 14.1 %collective-permute-start.23 = (bf16[224,256]{1,0:T(8,128)(2,1)S(1)}, bf16[224,256]{1,0:T(8,128)(2,1)S(1)}, u32[]{:S(2)}, u32[]{:S(2)}) collective-permute-start(bf16[224,256]{1,0:T(8,128)(2,1)S(1)} %shard_map.99), channel_id=1, source_target_pairs={{0,8},{8,0},{16,24},{24,16},{1,9},{9,1},{17,25},{25,17},{2,10},{10... | collective-permute-start | bytes 344072 | tf_op jit(solution)/shard_map/ppermute | solution.py:82
  64.6 16.9 %collective-permute-start.24 = (bf16[224,256]{1,0:T(8,128)(2,1)S(1)}, bf16[224,256]{1,0:T(8,128)(2,1)S(1)}, u32[]{:S(2)}, u32[]{:S(2)}) collective-permute-start(bf16[224,256]{1,0:T(8,128)(2,1)S(1)} %shard_map.100), channel_id=1, source_target_pairs={{0,16},{8,24},{16,0},{24,8},{1,17},{9,25},{17,1},{25,9},{2,18},{10... | collective-permute-start | bytes 344072 | tf_op jit(solution)/shard_map/ppermute | solution.py:82
  66.4 15.1 %collective-permute-start.25 = (bf16[224,256]{1,0:T(8,128)(2,1)S(1)}, bf16[224,256]{1,0:T(8,128)(2,1)S(1)}, u32[]{:S(2)}, u32[]{:S(2)}) collective-permute-start(bf16[224,256]{1,0:T(8,128)(2,1)S(1)} %shard_map.101), channel_id=1, source_target_pairs={{0,24},{8,16},{16,8},{24,0},{1,25},{9,17},{17,9},{25,1},{2,26},{10... | collective-permute-start | bytes 344072 | tf_op jit(solution)/shard_map/ppermute | solution.py:82
  74.9 11.0 %collective-permute-start.28 = (bf16[232,256]{1,0:T(8,128)(2,1)S(1)}, bf16[232,256]{1,0:T(8,128)(2,1)S(1)}, u32[]{:S(2)}, u32[]{:S(2)}) collective-permute-start(bf16[232,256]{1,0:T(8,128)(2,1)S(1)} %get-tuple-element.53.refs_0_), channel_id=1, source_target_pairs={{0,24},{8,16},{16,8},{24,0},{1,25},{9,17},{17,9},{25,1},{2,26},{10... | collective-permute-start | bytes 356360 | tf_op jit(solution)/shard_map/ppermute | solution.py:82
  75.1 12.6 %collective-permute-start.27 = (bf16[232,256]{1,0:T(8,128)(2,1)S(1)}, bf16[232,256]{1,0:T(8,128)(2,1)S(1)}, u32[]{:S(2)}, u32[]{:S(2)}) collective-permute-start(bf16[232,256]{1,0:T(8,128)(2,1)S(1)} %get-tuple-element.53.refs_0_), channel_id=1, source_target_pairs={{0,16},{8,24},{16,0},{24,8},{1,17},{9,25},{17,1},{25,9},{2,18},{10... | collective-permute-start | bytes 356360 | tf_op jit(solution)/shard_map/ppermute | solution.py:82
  76.3 11.5 %collective-permute-start.26 = (bf16[232,256]{1,0:T(8,128)(2,1)S(1)}, bf16[232,256]{1,0:T(8,128)(2,1)S(1)}, u32[]{:S(2)}, u32[]{:S(2)}) collective-permute-start(bf16[232,256]{1,0:T(8,128)(2,1)S(1)} %get-tuple-element.53.refs_0_), channel_id=1, source_target_pairs={{0,8},{8,0},{16,24},{24,16},{1,9},{9,1},{17,25},{25,17},{2,10},{10... | collective-permute-start | bytes 356360 | tf_op jit(solution)/shard_map/ppermute | solution.py:82
  81.8 6.5 %collective-permute-start.30 = (bf16[112,256]{1,0:T(8,128)(2,1)S(1)}, bf16[112,256]{1,0:T(8,128)(2,1)S(1)}, u32[]{:S(2)}, u32[]{:S(2)}) collective-permute-start(bf16[112,256]{1,0:T(8,128)(2,1)S(1)} %shard_map.102.refs_1_), channel_id=1, source_target_pairs={{0,8},{8,0},{16,24},{24,16},{1,9},{9,1},{17,25},{25,17},{2,10},{10... | collective-permute-start | bytes 172040 | tf_op jit(solution)/shard_map/ppermute | solution.py:82
  81.9 6.5 %collective-permute-start.29 = (bf16[112,256]{1,0:T(8,128)(2,1)S(1)}, bf16[112,256]{1,0:T(8,128)(2,1)S(1)}, u32[]{:S(2)}, u32[]{:S(2)}) collective-permute-start(bf16[112,256]{1,0:T(8,128)(2,1)S(1)} %shard_map.102.refs_1_), channel_id=1, source_target_pairs={{0,24},{8,16},{16,8},{24,0},{1,25},{9,17},{17,9},{25,1},{2,26},{10... | collective-permute-start | bytes 172040 | tf_op jit(solution)/shard_map/ppermute | solution.py:82
  93.2 8.3 %collective-permute-start.34 = (bf16[32,1024]{1,0:T(8,128)(2,1)S(1)}, bf16[32,1024]{1,0:T(8,128)(2,1)S(1)}, u32[]{:S(2)}, u32[]{:S(2)}) collective-permute-start(bf16[32,1024]{1,0:T(8,128)(2,1)S(1)} %get-tuple-element.59), channel_id=1, source_target_pairs={{0,4},{1,5},{2,6},{3,7},{4,0},{5,1},{6,2},{7,3},{8,12},{9,13},{10,... | collective-permute-start | bytes 196616 | tf_op jit(solution)/shard_map/ppermute | solution.py:86
  94.9 6.7 %collective-permute-start.35 = (bf16[32,1024]{1,0:T(8,128)(2,1)S(1)}, bf16[32,1024]{1,0:T(8,128)(2,1)S(1)}, u32[]{:S(2)}, u32[]{:S(2)}) collective-permute-start(bf16[32,1024]{1,0:T(8,128)(2,1)S(1)} %get-tuple-element.60), channel_id=1, source_target_pairs={{0,6},{1,7},{2,4},{3,5},{4,2},{5,3},{6,0},{7,1},{8,14},{9,15},{10,... | collective-permute-start | bytes 196616 | tf_op jit(solution)/shard_map/ppermute | solution.py:86
  101.6 6.3 %collective-permute-start.38 = (bf16[32,1024]{1,0:T(8,128)(2,1)S(1)}, bf16[32,1024]{1,0:T(8,128)(2,1)S(1)}, u32[]{:S(2)}, u32[]{:S(2)}) collective-permute-start(bf16[32,1024]{1,0:T(8,128)(2,1)S(1)} %shard_map.108.refs_0_), channel_id=1, source_target_pairs={{0,6},{1,7},{2,4},{3,5},{4,2},{5,3},{6,0},{7,1},{8,14},{9,15},{10,... | collective-permute-start | bytes 196616 | tf_op jit(solution)/shard_map/ppermute | solution.py:86
  103.6 5.9 %collective-permute-start.37 = (bf16[32,1024]{1,0:T(8,128)(2,1)S(1)}, bf16[32,1024]{1,0:T(8,128)(2,1)S(1)}, u32[]{:S(2)}, u32[]{:S(2)}) collective-permute-start(bf16[32,1024]{1,0:T(8,128)(2,1)S(1)} %shard_map.108.refs_0_), channel_id=1, source_target_pairs={{0,4},{1,5},{2,6},{3,7},{4,0},{5,1},{6,2},{7,3},{8,12},{9,13},{10,... | collective-permute-start | bytes 196616 | tf_op jit(solution)/shard_map/ppermute | solution.py:86
  104.3 5.2 %collective-permute-start.36 = (bf16[32,1024]{1,0:T(8,128)(2,1)S(1)}, bf16[32,1024]{1,0:T(8,128)(2,1)S(1)}, u32[]{:S(2)}, u32[]{:S(2)}) collective-permute-start(bf16[32,1024]{1,0:T(8,128)(2,1)S(1)} %shard_map.108.refs_0_), channel_id=1, source_target_pairs={{0,2},{1,3},{2,0},{3,1},{4,6},{5,7},{6,4},{7,5},{8,10},{9,11},{10,... | collective-permute-start | bytes 196616 | tf_op jit(solution)/shard_map/ppermute | solution.py:86
  (10 other events, 41.5 us)

commit v6 on v5

--- a/solution.py
+++ b/solution.py
@@ -495,19 +495,33 @@
             near = gather([old] + [send_z(old, s) for s in range(1, n_z)])
             pieces = [near, send_core(near)]
 
-        def join(near_ref, far_ref, side_ref, out_ref):
-            side = side_ref[0] & 1
-            out_ref[pl.ds(aligned(side * half, half), half), :] = near_ref[...]
-            out_ref[pl.ds(aligned((1 - side) * half, half), half), :] = far_ref[...]
-
-        return call(
-            join,
-            [*pieces, me_c],
-            [VMEM, VMEM, SMEM],
-            [((count, width), BF16)],
-            count * width,
-            4 * count * width,
-        )[0]
+        def place(rows, flip, made):
+            def body_fn(*refs):
+                rows_ref, side_ref, out_ref, sem = refs[0], refs[1], refs[-2], refs[-1]
+                side = (side_ref[0] & 1) ^ flip
+                at = pl.ds(aligned(side * half, half), half)
+                copy = pltpu.make_async_copy(rows_ref, out_ref.at[at], sem)
+                copy.start()
+                copy.wait()
+
+            args, specs, alias = [rows, me_c], [VMEM, SMEM], {}
+            if made is not None:
+                args, specs, alias = args + [made], specs + [HBM], {2: 0}
+            return pl.pallas_call(
+                body_fn,
+                in_specs=specs,
+                out_specs=HBM,
+                out_shape=jax.ShapeDtypeStruct((count, width), BF16),
+                scratch_shapes=[pltpu.SemaphoreType.DMA],
+                input_output_aliases=alias,
+                cost_estimate=pl.CostEstimate(
+                    flops=half * width, bytes_accessed=4 * half * width, transcendentals=0
+                ),
+                compiler_params=pltpu.CompilerParams(vmem_limit_bytes=16 * MIB),
+            )(*args)
+
+        near, far = pieces
+        return place(far, 1, place(near, 0, None))
 
     return body
 

time: 112 us -> 112 us (level)
    pallas_call x0 -> x2, Pallas kernels: none -> 1.43 us  [place(): pl.pallas_call(body_fn, in_specs=specs, out_specs=HBM, out_shape=jax.Shap...]
    pallas_call x38 -> x37, Pallas kernels: 24.4 us -> 23.5 us  [call(): pl.pallas_call(body, in_specs=specs, out_specs=[VMEM] * len(shapes), out_...]
  transfers between devices with their start and end apart: 40 -> 40, of which waited for: 19 -> 19; matrix products, arithmetic and copies ran while one was open for 0% -> 0% of each run, Pallas kernels for 17% -> 18%
where the time goes in v6:
time: 112 us
  starting transfers between devices  50.6 us (45%)
  waiting for transfers between devices  35.8 us (32%)
  Pallas kernels  25 us (22%)
    ppermute x24, starting transfers between devices, send_a(): return lax.ppermute(value, 'ra', [(i, peer(i, s, n_a)) for i in range(n_a)])  32.5 us
    pallas_call x37, Pallas kernels, call(): pl.pallas_call(body, in_specs=specs, out_specs=[VMEM] * len(shapes), out_...  23.5 us
    ppermute x12, starting transfers between devices, send_z(): return lax.ppermute(value, 'cb', pairs)  17.8 us
    ppermute x12, waiting for transfers between devices, send_z(): return lax.ppermute(value, 'cb', pairs)  17.8 us
    ppermute x24, waiting for transfers between devices, send_a(): return lax.ppermute(value, 'ra', [(i, peer(i, s, n_a)) for i in range(n_a)])  14.2 us
    ppermute x4, waiting for transfers between devices, send_core(): return lax.ppermute(value, 'cb', [(i, i ^ 1) for i in range(n_c)])  3.84 us
  transfers between devices with their start and end apart: 40, of which 19 were waited for; matrix products, arithmetic and copies ran while one was open for 0% of the time, Pallas kernels for 18%

profile of v6, /device:TPU:0, one launch (start us, length us, event | category | flops | bytes accessed | tf_op | source)
XLA Modules:
  0.0 111.9 jit_solution(6479996127413503010)
XLA Ops:
  0.0 2.2 %shard_map.73 = (bf16[472,256]{1,0:T(8,128)(2,1)S(1)}, bf16[256,1024]{1,0:T(8,128)(2,1)S(1)}, bf16[8,256]{1,0:T(8,128)(2,1)S(1)}) custom-call(s32[1]{0:T(128)} %bitcast.refs_0_.a_ref, bf16[2,1376,1024]{2,1,0:T(8,128)(2,1)} %bitcast.6, bf16[2,1376,1024]{2,1,0:T(8,128)(2,1)} %bitcast.9, bf16[256,1024]{1,0:T(8,128)(2,1)} %refs_4_.3, f32[2,1024]{1,0:T(2,128)} %refs_5_.1, ...), custom_call_target="tpu_custom_call" | custom-call | flops 243269632 | bytes 950272 | tf_op jit(solution)/shard_map/pallas_call | solution.py:29
  2.2 4.0 %collective-permute-start.2 = (bf16[472,256]{1,0:T(8,128)(2,1)S(1)}, bf16[472,256]{1,0:T(8,128)(2,1)S(1)}, u32[]{:S(2)}, u32[]{:S(2)}) collective-permute-start(bf16[472,256]{1,0:T(8,128)(2,1)S(1)} %get-tuple-element.38), channel_id=1, source_target_pairs={{0,24},{8,16},{16,8},{24,0},{1,25},{9,17},{17,9},{25,1},{2,26},{10... | collective-permute-start | bytes 725000 | tf_op jit(solution)/shard_map/ppermute | solution.py:82
  6.2 2.7 %shard_map.74 = (bf16[472,256]{1,0:T(8,128)(2,1)S(1)}, bf16[1376,1024]{1,0:T(8,128)(2,1)S(1)}, bf16[1376,1024]{1,0:T(8,128)(2,1)S(1)}, f32[344,16]{1,0:T(8,128)S(1)}) custom-call(s32[1]{0:T(128)} %bitcast.refs_0_.a_ref, bf16[2,1376,1024]{2,1,0:T(8,128)(2,1)} %bitcast.7, bf16[2,1376,1024]{2,1,0:T(8,128)(2,1)} %bitcast.10, ...), custom_call_target="tpu_custom_call" | custom-call | flops 243269632 | bytes 950272 | tf_op jit(solution)/shard_map/pallas_call | solution.py:29
  10.5 2.0 %collective-permute-start.3 = (bf16[224,256]{1,0:T(8,128)(2,1)S(1)}, bf16[224,256]{1,0:T(8,128)(2,1)S(1)}, u32[]{:S(2)}, u32[]{:S(2)}) collective-permute-start(bf16[224,256]{1,0:T(8,128)(2,1)S(1)} %shard_map.80), channel_id=1, source_target_pairs={{0,8},{8,0},{16,24},{24,16},{1,9},{9,1},{17,25},{25,17},{2,10},{10... | collective-permute-start | bytes 344072 | tf_op jit(solution)/shard_map/ppermute | solution.py:82
  13.0 1.6 %collective-permute-start.4 = (bf16[224,256]{1,0:T(8,128)(2,1)S(1)}, bf16[224,256]{1,0:T(8,128)(2,1)S(1)}, u32[]{:S(2)}, u32[]{:S(2)}) collective-permute-start(bf16[224,256]{1,0:T(8,128)(2,1)S(1)} %shard_map.81), channel_id=1, source_target_pairs={{0,16},{8,24},{16,0},{24,8},{1,17},{9,25},{17,1},{25,9},{2,18},{10... | collective-permute-start | bytes 344072 | tf_op jit(solution)/shard_map/ppermute | solution.py:82
  16.3 1.9 %collective-permute-done.refs_1_ = bf16[472,256]{1,0:T(8,128)(2,1)S(1)} collective-permute-done((bf16[472,256]{1,0:T(8,128)(2,1)S(1)}, bf16[472,256]{1,0:T(8,128)(2,1)S(1)}, u32[]{:S(2)}, u32[]{:S(2)}) %collective-permute-start) | collective-permute-done | bytes 241696 | tf_op jit(solution)/shard_map/ppermute | solution.py:82
  19.2 2.0 %collective-permute-start.8 = (bf16[232,256]{1,0:T(8,128)(2,1)S(1)}, bf16[232,256]{1,0:T(8,128)(2,1)S(1)}, u32[]{:S(2)}, u32[]{:S(2)}) collective-permute-start(bf16[232,256]{1,0:T(8,128)(2,1)S(1)} %get-tuple-element.40.refs_0_), channel_id=1, source_target_pairs={{0,24},{8,16},{16,8},{24,0},{1,25},{9,17},{17,9},{25,1},{2,26},{10... | collective-permute-start | bytes 356360 | tf_op jit(solution)/shard_map/ppermute | solution.py:82
  24.0 2.6 %collective-permute-start.10 = (bf16[112,256]{1,0:T(8,128)(2,1)S(1)}, bf16[112,256]{1,0:T(8,128)(2,1)S(1)}, u32[]{:S(2)}, u32[]{:S(2)}) collective-permute-start(bf16[112,256]{1,0:T(8,128)(2,1)S(1)} %shard_map.83.refs_1_), channel_id=1, source_target_pairs={{0,8},{8,0},{16,24},{24,16},{1,9},{9,1},{17,25},{25,17},{2,10},{10... | collective-permute-start | bytes 172040 | tf_op jit(solution)/shard_map/ppermute | solution.py:82
  27.2 1.8 %shard_map.76.weight_ref = bf16[1376,1024]{1,0:T(8,128)(2,1)S(1)} custom-call(bf16[2,1376,1024]{2,1,0:T(8,128)(2,1)} %refs_0_.3, bf16[224,256]{1,0:T(8,128)(2,1)S(1)} %shard_map.75.refs_1_.refs_0_), custom_call_target="tpu_custom_call" | custom-call | flops 240473424 | bytes 2818048 | tf_op jit(solution)/shard_map/pallas_call | solution.py:29
  35.3 1.8 %collective-permute-start.13 = (bf16[32,1024]{1,0:T(8,128)(2,1)S(1)}, bf16[32,1024]{1,0:T(8,128)(2,1)S(1)}, u32[]{:S(2)}, u32[]{:S(2)}) collective-permute-start(bf16[32,1024]{1,0:T(8,128)(2,1)S(1)} %get-tuple-element.47), channel_id=1, source_target_pairs={{0,2},{1,3},{2,0},{3,1},{4,6},{5,7},{6,4},{7,5},{8,10},{9,11},{10,... | collective-permute-start | bytes 196616 | tf_op jit(solution)/shard_map/ppermute | solution.py:86
  37.1 2.6 %collective-permute-start.14 = (bf16[32,1024]{1,0:T(8,128)(2,1)S(1)}, bf16[32,1024]{1,0:T(8,128)(2,1)S(1)}, u32[]{:S(2)}, u32[]{:S(2)}) collective-permute-start(bf16[32,1024]{1,0:T(8,128)(2,1)S(1)} %get-tuple-element.48), channel_id=1, source_target_pairs={{0,4},{1,5},{2,6},{3,7},{4,0},{5,1},{6,2},{7,3},{8,12},{9,13},{10,... | collective-permute-start | bytes 196616 | tf_op jit(solution)/shard_map/ppermute | solution.py:86
  39.8 4.9 %collective-permute-done.14.refs_1_ = bf16[32,1024]{1,0:T(8,128)(2,1)S(1)} collective-permute-done((bf16[32,1024]{1,0:T(8,128)(2,1)S(1)}, bf16[32,1024]{1,0:T(8,128)(2,1)S(1)}, u32[]{:S(2)}, u32[]{:S(2)}) %collective-permute-start.14) | collective-permute-done | bytes 65568 | tf_op jit(solution)/shard_map/ppermute | solution.py:86
  45.9 2.0 %collective-permute-start.18 = (bf16[32,1024]{1,0:T(8,128)(2,1)S(1)}, bf16[32,1024]{1,0:T(8,128)(2,1)S(1)}, u32[]{:S(2)}, u32[]{:S(2)}) collective-permute-start(bf16[32,1024]{1,0:T(8,128)(2,1)S(1)} %shard_map.90.refs_0_.refs_4_), channel_id=1, source_target_pairs={{0,6},{1,7},{2,4},{3,5},{4,2},{5,3},{6,0},{7,1},{8,14},{9,15},{10,... | collective-permute-start | bytes 196616 | tf_op jit(solution)/shard_map/ppermute | solution.py:86
  48.3 2.1 %collective-permute-start.16 = (bf16[32,1024]{1,0:T(8,128)(2,1)S(1)}, bf16[32,1024]{1,0:T(8,128)(2,1)S(1)}, u32[]{:S(2)}, u32[]{:S(2)}) collective-permute-start(bf16[32,1024]{1,0:T(8,128)(2,1)S(1)} %shard_map.90.refs_0_.refs_4_), channel_id=1, source_target_pairs={{0,2},{1,3},{2,0},{3,1},{4,6},{5,7},{6,4},{7,5},{8,10},{9,11},{10,... | collective-permute-start | bytes 196616 | tf_op jit(solution)/shard_map/ppermute | solution.py:86
  50.4 1.8 %collective-permute-done.18.refs_3_ = bf16[32,1024]{1,0:T(8,128)(2,1)S(1)} collective-permute-done((bf16[32,1024]{1,0:T(8,128)(2,1)S(1)}, bf16[32,1024]{1,0:T(8,128)(2,1)S(1)}, u32[]{:S(2)}, u32[]{:S(2)}) %collective-permute-start.18) | collective-permute-done | bytes 65568 | tf_op jit(solution)/shard_map/ppermute | solution.py:86
  52.2 1.5 %collective-permute-done.17.refs_2_ = bf16[32,1024]{1,0:T(8,128)(2,1)S(1)} collective-permute-done((bf16[32,1024]{1,0:T(8,128)(2,1)S(1)}, bf16[32,1024]{1,0:T(8,128)(2,1)S(1)}, u32[]{:S(2)}, u32[]{:S(2)}) %collective-permute-start.17) | collective-permute-done | bytes 65568 | tf_op jit(solution)/shard_map/ppermute | solution.py:86
  53.9 2.7 %shard_map.89 = (bf16[1376,1024]{1,0:T(8,128)(2,1)S(1)}, bf16[1376,1024]{1,0:T(8,128)(2,1)S(1)}) custom-call(bf16[2,1376,1024]{2,1,0:T(8,128)(2,1)} %bitcast.8, bf16[2,1376,1024]{2,1,0:T(8,128)(2,1)} %bitcast.11, f32[32,1024]{1,0:T(8,128)S(1)} %get-tuple-element.44.refs_2_.own_ref), custom_call_target="tpu_custom_call" | custom-call | flops 480946848 | bytes 5636096 | tf_op jit(solution)/shard_map/pallas_call | solution.py:29
  57.6 2.0 %collective-permute-start.20 = (bf16[472,256]{1,0:T(8,128)(2,1)S(1)}, bf16[472,256]{1,0:T(8,128)(2,1)S(1)}, u32[]{:S(2)}, u32[]{:S(2)}) collective-permute-start(bf16[472,256]{1,0:T(8,128)(2,1)S(1)} %shard_map.96), channel_id=1, source_target_pairs={{0,8},{8,0},{16,24},{24,16},{1,9},{9,1},{17,25},{25,17},{2,10},{10... | collective-permute-start | bytes 725000 | tf_op jit(solution)/shard_map/ppermute | solution.py:82
  62.1 2.0 %collective-permute-start.23 = (bf16[224,256]{1,0:T(8,128)(2,1)S(1)}, bf16[224,256]{1,0:T(8,128)(2,1)S(1)}, u32[]{:S(2)}, u32[]{:S(2)}) collective-permute-start(bf16[224,256]{1,0:T(8,128)(2,1)S(1)} %shard_map.99), channel_id=1, source_target_pairs={{0,8},{8,0},{16,24},{24,16},{1,9},{9,1},{17,25},{25,17},{2,10},{10... | collective-permute-start | bytes 344072 | tf_op jit(solution)/shard_map/ppermute | solution.py:82
  66.4 2.1 %collective-permute-start.25 = (bf16[224,256]{1,0:T(8,128)(2,1)S(1)}, bf16[224,256]{1,0:T(8,128)(2,1)S(1)}, u32[]{:S(2)}, u32[]{:S(2)}) collective-permute-start(bf16[224,256]{1,0:T(8,128)(2,1)S(1)} %shard_map.101), channel_id=1, source_target_pairs={{0,24},{8,16},{16,8},{24,0},{1,25},{9,17},{17,9},{25,1},{2,26},{10... | collective-permute-start | bytes 344072 | tf_op jit(solution)/shard_map/ppermute | solution.py:82
  69.0 5.3 %collective-permute-done.21.refs_2_ = bf16[472,256]{1,0:T(8,128)(2,1)S(1)} collective-permute-done((bf16[472,256]{1,0:T(8,128)(2,1)S(1)}, bf16[472,256]{1,0:T(8,128)(2,1)S(1)}, u32[]{:S(2)}, u32[]{:S(2)}) %collective-permute-start.21) | collective-permute-done | bytes 241696 | tf_op jit(solution)/shard_map/ppermute | solution.py:82
  76.3 2.2 %collective-permute-start.26 = (bf16[232,256]{1,0:T(8,128)(2,1)S(1)}, bf16[232,256]{1,0:T(8,128)(2,1)S(1)}, u32[]{:S(2)}, u32[]{:S(2)}) collective-permute-start(bf16[232,256]{1,0:T(8,128)(2,1)S(1)} %get-tuple-element.53.refs_0_), channel_id=1, source_target_pairs={{0,8},{8,0},{16,24},{24,16},{1,9},{9,1},{17,25},{25,17},{2,10},{10... | collective-permute-start | bytes 356360 | tf_op jit(solution)/shard_map/ppermute | solution.py:82
  78.9 2.6 %collective-permute-done.24.refs_2_ = bf16[224,256]{1,0:T(8,128)(2,1)S(1)} collective-permute-done((bf16[224,256]{1,0:T(8,128)(2,1)S(1)}, bf16[224,256]{1,0:T(8,128)(2,1)S(1)}, u32[]{:S(2)}, u32[]{:S(2)}) %collective-permute-start.24) | collective-permute-done | bytes 114720 | tf_op jit(solution)/shard_map/ppermute | solution.py:82
  81.9 2.2 %collective-permute-start.29 = (bf16[112,256]{1,0:T(8,128)(2,1)S(1)}, bf16[112,256]{1,0:T(8,128)(2,1)S(1)}, u32[]{:S(2)}, u32[]{:S(2)}) collective-permute-start(bf16[112,256]{1,0:T(8,128)(2,1)S(1)} %shard_map.102.refs_1_), channel_id=1, source_target_pairs={{0,24},{8,16},{16,8},{24,0},{1,25},{9,17},{17,9},{25,1},{2,26},{10... | collective-permute-start | bytes 172040 | tf_op jit(solution)/shard_map/ppermute | solution.py:82
  84.1 1.8 %shard_map.94.weight_ref = bf16[1376,1024]{1,0:T(8,128)(2,1)S(1)} custom-call(bf16[2,1376,1024]{2,1,0:T(8,128)(2,1)} %refs_0_.3, bf16[224,256]{1,0:T(8,128)(2,1)S(1)} %shard_map.93.refs_1_.refs_0_), custom_call_target="tpu_custom_call" | custom-call | flops 240473424 | bytes 2818048 | tf_op jit(solution)/shard_map/pallas_call | solution.py:29
  93.2 1.6 %collective-permute-start.34 = (bf16[32,1024]{1,0:T(8,128)(2,1)S(1)}, bf16[32,1024]{1,0:T(8,128)(2,1)S(1)}, u32[]{:S(2)}, u32[]{:S(2)}) collective-permute-start(bf16[32,1024]{1,0:T(8,128)(2,1)S(1)} %get-tuple-element.59), channel_id=1, source_target_pairs={{0,4},{1,5},{2,6},{3,7},{4,0},{5,1},{6,2},{7,3},{8,12},{9,13},{10,... | collective-permute-start | bytes 196616 | tf_op jit(solution)/shard_map/ppermute | solution.py:86
  94.9 1.9 %collective-permute-start.35 = (bf16[32,1024]{1,0:T(8,128)(2,1)S(1)}, bf16[32,1024]{1,0:T(8,128)(2,1)S(1)}, u32[]{:S(2)}, u32[]{:S(2)}) collective-permute-start(bf16[32,1024]{1,0:T(8,128)(2,1)S(1)} %get-tuple-element.60), channel_id=1, source_target_pairs={{0,6},{1,7},{2,4},{3,5},{4,2},{5,3},{6,0},{7,1},{8,14},{9,15},{10,... | collective-permute-start | bytes 196616 | tf_op jit(solution)/shard_map/ppermute | solution.py:86
  96.7 4.8 %collective-permute-done.34.refs_1_ = bf16[32,1024]{1,0:T(8,128)(2,1)S(1)} collective-permute-done((bf16[32,1024]{1,0:T(8,128)(2,1)S(1)}, bf16[32,1024]{1,0:T(8,128)(2,1)S(1)}, u32[]{:S(2)}, u32[]{:S(2)}) %collective-permute-start.34) | collective-permute-done | bytes 65568 | tf_op jit(solution)/shard_map/ppermute | solution.py:86
  101.6 2.1 %collective-permute-start.38 = (bf16[32,1024]{1,0:T(8,128)(2,1)S(1)}, bf16[32,1024]{1,0:T(8,128)(2,1)S(1)}, u32[]{:S(2)}, u32[]{:S(2)}) collective-permute-start(bf16[32,1024]{1,0:T(8,128)(2,1)S(1)} %shard_map.108.refs_0_), channel_id=1, source_target_pairs={{0,6},{1,7},{2,4},{3,5},{4,2},{5,3},{6,0},{7,1},{8,14},{9,15},{10,... | collective-permute-start | bytes 196616 | tf_op jit(solution)/shard_map/ppermute | solution.py:86
  104.3 1.7 %collective-permute-start.36 = (bf16[32,1024]{1,0:T(8,128)(2,1)S(1)}, bf16[32,1024]{1,0:T(8,128)(2,1)S(1)}, u32[]{:S(2)}, u32[]{:S(2)}) collective-permute-start(bf16[32,1024]{1,0:T(8,128)(2,1)S(1)} %shard_map.108.refs_0_), channel_id=1, source_target_pairs={{0,2},{1,3},{2,0},{3,1},{4,6},{5,7},{6,4},{7,5},{8,10},{9,11},{10,... | collective-permute-start | bytes 196616 | tf_op jit(solution)/shard_map/ppermute | solution.py:86
  106.0 1.9 %collective-permute-done.38.refs_3_ = bf16[32,1024]{1,0:T(8,128)(2,1)S(1)} collective-permute-done((bf16[32,1024]{1,0:T(8,128)(2,1)S(1)}, bf16[32,1024]{1,0:T(8,128)(2,1)S(1)}, u32[]{:S(2)}, u32[]{:S(2)}) %collective-permute-start.38) | collective-permute-done | bytes 65568 | tf_op jit(solution)/shard_map/ppermute | solution.py:86
  107.9 1.6 %collective-permute-done.37.refs_2_ = bf16[32,1024]{1,0:T(8,128)(2,1)S(1)} collective-permute-done((bf16[32,1024]{1,0:T(8,128)(2,1)S(1)}, bf16[32,1024]{1,0:T(8,128)(2,1)S(1)}, u32[]{:S(2)}, u32[]{:S(2)}) %collective-permute-start.37) | collective-permute-done | bytes 65568 | tf_op jit(solution)/shard_map/ppermute | solution.py:86
  (91 shorter events, 35.3 us)
Async XLA Ops:
  2.2 12.8 %collective-permute-start.2 = (bf16[472,256]{1,0:T(8,128)(2,1)S(1)}, bf16[472,256]{1,0:T(8,128)(2,1)S(1)}, u32[]{:S(2)}, u32[]{:S(2)}) collective-permute-start(bf16[472,256]{1,0:T(8,128)(2,1)S(1)} %get-tuple-element.38), channel_id=1, source_target_pairs={{0,24},{8,16},{16,8},{24,0},{1,25},{9,17},{17,9},{25,1},{2,26},{10... | collective-permute-start | bytes 725000 | tf_op jit(solution)/shard_map/ppermute | solution.py:82
  9.4 8.8 %collective-permute-start = (bf16[472,256]{1,0:T(8,128)(2,1)S(1)}, bf16[472,256]{1,0:T(8,128)(2,1)S(1)}, u32[]{:S(2)}, u32[]{:S(2)}) collective-permute-start(bf16[472,256]{1,0:T(8,128)(2,1)S(1)} %shard_map.78), channel_id=1, source_target_pairs={{0,8},{8,0},{16,24},{24,16},{1,9},{9,1},{17,25},{25,17},{2,10},{10... | collective-permute-start | bytes 725000 | tf_op jit(solution)/shard_map/ppermute | solution.py:82
  10.0 8.6 %collective-permute-start.1 = (bf16[472,256]{1,0:T(8,128)(2,1)S(1)}, bf16[472,256]{1,0:T(8,128)(2,1)S(1)}, u32[]{:S(2)}, u32[]{:S(2)}) collective-permute-start(bf16[472,256]{1,0:T(8,128)(2,1)S(1)} %get-tuple-element.37), channel_id=1, source_target_pairs={{0,16},{8,24},{16,0},{24,8},{1,17},{9,25},{17,1},{25,9},{2,18},{10... | collective-permute-start | bytes 725000 | tf_op jit(solution)/shard_map/ppermute | solution.py:82
  10.5 11.8 %collective-permute-start.3 = (bf16[224,256]{1,0:T(8,128)(2,1)S(1)}, bf16[224,256]{1,0:T(8,128)(2,1)S(1)}, u32[]{:S(2)}, u32[]{:S(2)}) collective-permute-start(bf16[224,256]{1,0:T(8,128)(2,1)S(1)} %shard_map.80), channel_id=1, source_target_pairs={{0,8},{8,0},{16,24},{24,16},{1,9},{9,1},{17,25},{25,17},{2,10},{10... | collective-permute-start | bytes 344072 | tf_op jit(solution)/shard_map/ppermute | solution.py:82
  13.0 10.7 %collective-permute-start.4 = (bf16[224,256]{1,0:T(8,128)(2,1)S(1)}, bf16[224,256]{1,0:T(8,128)(2,1)S(1)}, u32[]{:S(2)}, u32[]{:S(2)}) collective-permute-start(bf16[224,256]{1,0:T(8,128)(2,1)S(1)} %shard_map.81), channel_id=1, source_target_pairs={{0,16},{8,24},{16,0},{24,8},{1,17},{9,25},{17,1},{25,9},{2,18},{10... | collective-permute-start | bytes 344072 | tf_op jit(solution)/shard_map/ppermute | solution.py:82
  15.0 8.6 %collective-permute-start.5 = (bf16[224,256]{1,0:T(8,128)(2,1)S(1)}, bf16[224,256]{1,0:T(8,128)(2,1)S(1)}, u32[]{:S(2)}, u32[]{:S(2)}) collective-permute-start(bf16[224,256]{1,0:T(8,128)(2,1)S(1)} %shard_map.82), channel_id=1, source_target_pairs={{0,24},{8,16},{16,8},{24,0},{1,25},{9,17},{17,9},{25,1},{2,26},{10... | collective-permute-start | bytes 344072 | tf_op jit(solution)/shard_map/ppermute | solution.py:82
  19.2 9.8 %collective-permute-start.8 = (bf16[232,256]{1,0:T(8,128)(2,1)S(1)}, bf16[232,256]{1,0:T(8,128)(2,1)S(1)}, u32[]{:S(2)}, u32[]{:S(2)}) collective-permute-start(bf16[232,256]{1,0:T(8,128)(2,1)S(1)} %get-tuple-element.40.refs_0_), channel_id=1, source_target_pairs={{0,24},{8,16},{16,8},{24,0},{1,25},{9,17},{17,9},{25,1},{2,26},{10... | collective-permute-start | bytes 356360 | tf_op jit(solution)/shard_map/ppermute | solution.py:82
  21.2 9.2 %collective-permute-start.7 = (bf16[232,256]{1,0:T(8,128)(2,1)S(1)}, bf16[232,256]{1,0:T(8,128)(2,1)S(1)}, u32[]{:S(2)}, u32[]{:S(2)}) collective-permute-start(bf16[232,256]{1,0:T(8,128)(2,1)S(1)} %get-tuple-element.40.refs_0_), channel_id=1, source_target_pairs={{0,16},{8,24},{16,0},{24,8},{1,17},{9,25},{17,1},{25,9},{2,18},{10... | collective-permute-start | bytes 356360 | tf_op jit(solution)/shard_map/ppermute | solution.py:82
  22.3 8.1 %collective-permute-start.6 = (bf16[232,256]{1,0:T(8,128)(2,1)S(1)}, bf16[232,256]{1,0:T(8,128)(2,1)S(1)}, u32[]{:S(2)}, u32[]{:S(2)}) collective-permute-start(bf16[232,256]{1,0:T(8,128)(2,1)S(1)} %get-tuple-element.40.refs_0_), channel_id=1, source_target_pairs={{0,8},{8,0},{16,24},{24,16},{1,9},{9,1},{17,25},{25,17},{2,10},{10... | collective-permute-start | bytes 356360 | tf_op jit(solution)/shard_map/ppermute | solution.py:82
  24.0 7.1 %collective-permute-start.10 = (bf16[112,256]{1,0:T(8,128)(2,1)S(1)}, bf16[112,256]{1,0:T(8,128)(2,1)S(1)}, u32[]{:S(2)}, u32[]{:S(2)}) collective-permute-start(bf16[112,256]{1,0:T(8,128)(2,1)S(1)} %shard_map.83.refs_1_), channel_id=1, source_target_pairs={{0,8},{8,0},{16,24},{24,16},{1,9},{9,1},{17,25},{25,17},{2,10},{10... | collective-permute-start | bytes 172040 | tf_op jit(solution)/shard_map/ppermute | solution.py:82
  26.6 5.1 %collective-permute-start.9 = (bf16[112,256]{1,0:T(8,128)(2,1)S(1)}, bf16[112,256]{1,0:T(8,128)(2,1)S(1)}, u32[]{:S(2)}, u32[]{:S(2)}) collective-permute-start(bf16[112,256]{1,0:T(8,128)(2,1)S(1)} %shard_map.83.refs_1_), channel_id=1, source_target_pairs={{0,24},{8,16},{16,8},{24,0},{1,25},{9,17},{17,9},{25,1},{2,26},{10... | collective-permute-start | bytes 172040 | tf_op jit(solution)/shard_map/ppermute | solution.py:82
  37.1 7.5 %collective-permute-start.14 = (bf16[32,1024]{1,0:T(8,128)(2,1)S(1)}, bf16[32,1024]{1,0:T(8,128)(2,1)S(1)}, u32[]{:S(2)}, u32[]{:S(2)}) collective-permute-start(bf16[32,1024]{1,0:T(8,128)(2,1)S(1)} %get-tuple-element.48), channel_id=1, source_target_pairs={{0,4},{1,5},{2,6},{3,7},{4,0},{5,1},{6,2},{7,3},{8,12},{9,13},{10,... | collective-permute-start | bytes 196616 | tf_op jit(solution)/shard_map/ppermute | solution.py:86
  39.7 6.2 %collective-permute-start.15 = (bf16[32,1024]{1,0:T(8,128)(2,1)S(1)}, bf16[32,1024]{1,0:T(8,128)(2,1)S(1)}, u32[]{:S(2)}, u32[]{:S(2)}) collective-permute-start(bf16[32,1024]{1,0:T(8,128)(2,1)S(1)} %get-tuple-element.49), channel_id=1, source_target_pairs={{0,6},{1,7},{2,4},{3,5},{4,2},{5,3},{6,0},{7,1},{8,14},{9,15},{10,... | collective-permute-start | bytes 196616 | tf_op jit(solution)/shard_map/ppermute | solution.py:86
  45.9 6.3 %collective-permute-start.18 = (bf16[32,1024]{1,0:T(8,128)(2,1)S(1)}, bf16[32,1024]{1,0:T(8,128)(2,1)S(1)}, u32[]{:S(2)}, u32[]{:S(2)}) collective-permute-start(bf16[32,1024]{1,0:T(8,128)(2,1)S(1)} %shard_map.90.refs_0_.refs_4_), channel_id=1, source_target_pairs={{0,6},{1,7},{2,4},{3,5},{4,2},{5,3},{6,0},{7,1},{8,14},{9,15},{10,... | collective-permute-start | bytes 196616 | tf_op jit(solution)/shard_map/ppermute | solution.py:86
  48.0 5.8 %collective-permute-start.17 = (bf16[32,1024]{1,0:T(8,128)(2,1)S(1)}, bf16[32,1024]{1,0:T(8,128)(2,1)S(1)}, u32[]{:S(2)}, u32[]{:S(2)}) collective-permute-start(bf16[32,1024]{1,0:T(8,128)(2,1)S(1)} %shard_map.90.refs_0_.refs_4_), channel_id=1, source_target_pairs={{0,4},{1,5},{2,6},{3,7},{4,0},{5,1},{6,2},{7,3},{8,12},{9,13},{10,... | collective-permute-start | bytes 196616 | tf_op jit(solution)/shard_map/ppermute | solution.py:86
  48.3 5.5 %collective-permute-start.16 = (bf16[32,1024]{1,0:T(8,128)(2,1)S(1)}, bf16[32,1024]{1,0:T(8,128)(2,1)S(1)}, u32[]{:S(2)}, u32[]{:S(2)}) collective-permute-start(bf16[32,1024]{1,0:T(8,128)(2,1)S(1)} %shard_map.90.refs_0_.refs_4_), channel_id=1, source_target_pairs={{0,2},{1,3},{2,0},{3,1},{4,6},{5,7},{6,4},{7,5},{8,10},{9,11},{10,... | collective-permute-start | bytes 196616 | tf_op jit(solution)/shard_map/ppermute | solution.py:86
  57.6 8.8 %collective-permute-start.20 = (bf16[472,256]{1,0:T(8,128)(2,1)S(1)}, bf16[472,256]{1,0:T(8,128)(2,1)S(1)}, u32[]{:S(2)}, u32[]{:S(2)}) collective-permute-start(bf16[472,256]{1,0:T(8,128)(2,1)S(1)} %shard_map.96), channel_id=1, source_target_pairs={{0,8},{8,0},{16,24},{24,16},{1,9},{9,1},{17,25},{25,17},{2,10},{10... | collective-permute-start | bytes 725000 | tf_op jit(solution)/shard_map/ppermute | solution.py:82
  60.1 14.2 %collective-permute-start.21 = (bf16[472,256]{1,0:T(8,128)(2,1)S(1)}, bf16[472,256]{1,0:T(8,128)(2,1)S(1)}, u32[]{:S(2)}, u32[]{:S(2)}) collective-permute-start(bf16[472,256]{1,0:T(8,128)(2,1)S(1)} %shard_map.97), channel_id=1, source_target_pairs={{0,16},{8,24},{16,0},{24,8},{1,17},{9,25},{17,1},{25,9},{2,18},{10... | collective-permute-start | bytes 725000 | tf_op jit(solution)/shard_map/ppermute | solution.py:82
  60.9 13.4 %collective-permute-start.22 = (bf16[472,256]{1,0:T(8,128)(2,1)S(1)}, bf16[472,256]{1,0:T(8,128)(2,1)S(1)}, u32[]{:S(2)}, u32[]{:S(2)}) collective-permute-start(bf16[472,256]{1,0:T(8,128)(2,1)S(1)} %get-tuple-element.52), channel_id=1, source_target_pairs={{0,24},{8,16},{16,8},{24,0},{1,25},{9,17},{17,9},{25,1},{2,26},{10... | collective-permute-start | bytes 725000 | tf_op jit(solution)/shard_map/ppermute | solution.py:82
  62.1 14.1 %collective-permute-start.23 = (bf16[224,256]{1,0:T(8,128)(2,1)S(1)}, bf16[224,256]{1,0:T(8,128)(2,1)S(1)}, u32[]{:S(2)}, u32[]{:S(2)}) collective-permute-start(bf16[224,256]{1,0:T(8,128)(2,1)S(1)} %shard_map.99), channel_id=1, source_target_pairs={{0,8},{8,0},{16,24},{24,16},{1,9},{9,1},{17,25},{25,17},{2,10},{10... | collective-permute-start | bytes 344072 | tf_op jit(solution)/shard_map/ppermute | solution.py:82
  64.6 16.9 %collective-permute-start.24 = (bf16[224,256]{1,0:T(8,128)(2,1)S(1)}, bf16[224,256]{1,0:T(8,128)(2,1)S(1)}, u32[]{:S(2)}, u32[]{:S(2)}) collective-permute-start(bf16[224,256]{1,0:T(8,128)(2,1)S(1)} %shard_map.100), channel_id=1, source_target_pairs={{0,16},{8,24},{16,0},{24,8},{1,17},{9,25},{17,1},{25,9},{2,18},{10... | collective-permute-start | bytes 344072 | tf_op jit(solution)/shard_map/ppermute | solution.py:82
  66.4 15.1 %collective-permute-start.25 = (bf16[224,256]{1,0:T(8,128)(2,1)S(1)}, bf16[224,256]{1,0:T(8,128)(2,1)S(1)}, u32[]{:S(2)}, u32[]{:S(2)}) collective-permute-start(bf16[224,256]{1,0:T(8,128)(2,1)S(1)} %shard_map.101), channel_id=1, source_target_pairs={{0,24},{8,16},{16,8},{24,0},{1,25},{9,17},{17,9},{25,1},{2,26},{10... | collective-permute-start | bytes 344072 | tf_op jit(solution)/shard_map/ppermute | solution.py:82
  74.9 11.0 %collective-permute-start.28 = (bf16[232,256]{1,0:T(8,128)(2,1)S(1)}, bf16[232,256]{1,0:T(8,128)(2,1)S(1)}, u32[]{:S(2)}, u32[]{:S(2)}) collective-permute-start(bf16[232,256]{1,0:T(8,128)(2,1)S(1)} %get-tuple-element.53.refs_0_), channel_id=1, source_target_pairs={{0,24},{8,16},{16,8},{24,0},{1,25},{9,17},{17,9},{25,1},{2,26},{10... | collective-permute-start | bytes 356360 | tf_op jit(solution)/shard_map/ppermute | solution.py:82
  75.1 12.6 %collective-permute-start.27 = (bf16[232,256]{1,0:T(8,128)(2,1)S(1)}, bf16[232,256]{1,0:T(8,128)(2,1)S(1)}, u32[]{:S(2)}, u32[]{:S(2)}) collective-permute-start(bf16[232,256]{1,0:T(8,128)(2,1)S(1)} %get-tuple-element.53.refs_0_), channel_id=1, source_target_pairs={{0,16},{8,24},{16,0},{24,8},{1,17},{9,25},{17,1},{25,9},{2,18},{10... | collective-permute-start | bytes 356360 | tf_op jit(solution)/shard_map/ppermute | solution.py:82
  76.3 11.5 %collective-permute-start.26 = (bf16[232,256]{1,0:T(8,128)(2,1)S(1)}, bf16[232,256]{1,0:T(8,128)(2,1)S(1)}, u32[]{:S(2)}, u32[]{:S(2)}) collective-permute-start(bf16[232,256]{1,0:T(8,128)(2,1)S(1)} %get-tuple-element.53.refs_0_), channel_id=1, source_target_pairs={{0,8},{8,0},{16,24},{24,16},{1,9},{9,1},{17,25},{25,17},{2,10},{10... | collective-permute-start | bytes 356360 | tf_op jit(solution)/shard_map/ppermute | solution.py:82
  81.8 6.5 %collective-permute-start.30 = (bf16[112,256]{1,0:T(8,128)(2,1)S(1)}, bf16[112,256]{1,0:T(8,128)(2,1)S(1)}, u32[]{:S(2)}, u32[]{:S(2)}) collective-permute-start(bf16[112,256]{1,0:T(8,128)(2,1)S(1)} %shard_map.102.refs_1_), channel_id=1, source_target_pairs={{0,8},{8,0},{16,24},{24,16},{1,9},{9,1},{17,25},{25,17},{2,10},{10... | collective-permute-start | bytes 172040 | tf_op jit(solution)/shard_map/ppermute | solution.py:82
  81.9 6.5 %collective-permute-start.29 = (bf16[112,256]{1,0:T(8,128)(2,1)S(1)}, bf16[112,256]{1,0:T(8,128)(2,1)S(1)}, u32[]{:S(2)}, u32[]{:S(2)}) collective-permute-start(bf16[112,256]{1,0:T(8,128)(2,1)S(1)} %shard_map.102.refs_1_), channel_id=1, source_target_pairs={{0,24},{8,16},{16,8},{24,0},{1,25},{9,17},{17,9},{25,1},{2,26},{10... | collective-permute-start | bytes 172040 | tf_op jit(solution)/shard_map/ppermute | solution.py:82
  93.2 8.3 %collective-permute-start.34 = (bf16[32,1024]{1,0:T(8,128)(2,1)S(1)}, bf16[32,1024]{1,0:T(8,128)(2,1)S(1)}, u32[]{:S(2)}, u32[]{:S(2)}) collective-permute-start(bf16[32,1024]{1,0:T(8,128)(2,1)S(1)} %get-tuple-element.59), channel_id=1, source_target_pairs={{0,4},{1,5},{2,6},{3,7},{4,0},{5,1},{6,2},{7,3},{8,12},{9,13},{10,... | collective-permute-start | bytes 196616 | tf_op jit(solution)/shard_map/ppermute | solution.py:86
  94.9 6.7 %collective-permute-start.35 = (bf16[32,1024]{1,0:T(8,128)(2,1)S(1)}, bf16[32,1024]{1,0:T(8,128)(2,1)S(1)}, u32[]{:S(2)}, u32[]{:S(2)}) collective-permute-start(bf16[32,1024]{1,0:T(8,128)(2,1)S(1)} %get-tuple-element.60), channel_id=1, source_target_pairs={{0,6},{1,7},{2,4},{3,5},{4,2},{5,3},{6,0},{7,1},{8,14},{9,15},{10,... | collective-permute-start | bytes 196616 | tf_op jit(solution)/shard_map/ppermute | solution.py:86
  101.6 6.3 %collective-permute-start.38 = (bf16[32,1024]{1,0:T(8,128)(2,1)S(1)}, bf16[32,1024]{1,0:T(8,128)(2,1)S(1)}, u32[]{:S(2)}, u32[]{:S(2)}) collective-permute-start(bf16[32,1024]{1,0:T(8,128)(2,1)S(1)} %shard_map.108.refs_0_), channel_id=1, source_target_pairs={{0,6},{1,7},{2,4},{3,5},{4,2},{5,3},{6,0},{7,1},{8,14},{9,15},{10,... | collective-permute-start | bytes 196616 | tf_op jit(solution)/shard_map/ppermute | solution.py:86
  103.6 5.9 %collective-permute-start.37 = (bf16[32,1024]{1,0:T(8,128)(2,1)S(1)}, bf16[32,1024]{1,0:T(8,128)(2,1)S(1)}, u32[]{:S(2)}, u32[]{:S(2)}) collective-permute-start(bf16[32,1024]{1,0:T(8,128)(2,1)S(1)} %shard_map.108.refs_0_), channel_id=1, source_target_pairs={{0,4},{1,5},{2,6},{3,7},{4,0},{5,1},{6,2},{7,3},{8,12},{9,13},{10,... | collective-permute-start | bytes 196616 | tf_op jit(solution)/shard_map/ppermute | solution.py:86
  104.3 5.2 %collective-permute-start.36 = (bf16[32,1024]{1,0:T(8,128)(2,1)S(1)}, bf16[32,1024]{1,0:T(8,128)(2,1)S(1)}, u32[]{:S(2)}, u32[]{:S(2)}) collective-permute-start(bf16[32,1024]{1,0:T(8,128)(2,1)S(1)} %shard_map.108.refs_0_), channel_id=1, source_target_pairs={{0,2},{1,3},{2,0},{3,1},{4,6},{5,7},{6,4},{7,5},{8,10},{9,11},{10,... | collective-permute-start | bytes 196616 | tf_op jit(solution)/shard_map/ppermute | solution.py:86
  (10 other events, 41.5 us)

commit v7 on v6

--- a/solution.py
+++ b/solution.py
@@ -409,6 +409,27 @@
                 [pltpu.VMEM((count, width), F32)] if last else (),
             )
 
+        def down_half(h, weight, total, others, s, flip):
+            lo, size = cuts[h]
+
+            def body_fn(weight_ref, sum_ref, a_ref, side_ref, hidden_ref, out_ref):
+                side = (side_ref[0] & 1) ^ flip
+                mine = pl.ds(aligned(side * half, half), half)
+                p = source(a_ref[0], s, n_a)
+                at = pl.ds(aligned(begin(p) + lo), size)
+                keep = None if even else p * piece - begin(p) - lo
+                term = term_of(hidden_ref[:, mine], weight_ref[at, :], keep)
+                out_ref[...] = (sum_ref[mine, :] + term).astype(out_ref.dtype)
+
+            return call(
+                body_fn,
+                [weight, total, me_a, me_c, others[s - 1]],
+                [VMEM] * 2 + [SMEM] * 2 + [VMEM],
+                [((half, width), BF16 if flip else F32)],
+                2 * size * half * width,
+                2 * size * width,
+            )[0]
+
         def deal(kept, came):
             def body_fn(kept_ref, came_ref, z_ref, *refs):
                 for s in range(n_z):
@@ -482,9 +503,13 @@
             turns = [(h, list(range(1, n_a))) for h in range(n_h)]
             if n_a == 4:
                 turns = turns[:-1] + [(n_h - 1, [3, 1]), (n_h - 1, [2])]
-            for i, (h, picks) in enumerate(turns):
+            halves = n_a == 4 and half % 128 == 0
+            for i, (h, picks) in enumerate(turns[: len(turns) - halves]):
                 out = down(h, weight, total, others[h], picks, i == len(turns) - 1)
                 total = out[0]
+            if halves:
+                h, (s,) = turns[-1]
+                out = [down_half(h, weight, total, others[h], s, flip) for flip in (1, 0)]
             away, kept = out
             dealt = deal(kept, send_core(away))
             came = [send_z(dealt[s], s) for s in range(1, n_z)]

time: 112 us -> 112 us (level)
    pallas_call x37 -> x39, Pallas kernels: 23.5 us -> 23.7 us  [call(): pl.pallas_call(body, in_specs=specs, out_specs=[VMEM] * len(shapes), out_...]
where the time goes in v7:
time: 112 us
  starting transfers between devices  50.6 us (45%)
  waiting for transfers between devices  35.3 us (32%)
  Pallas kernels  25.2 us (22%)
    ppermute x24, starting transfers between devices, send_a(): return lax.ppermute(value, 'ra', [(i, peer(i, s, n_a)) for i in range(n_a)])  32.5 us
    pallas_call x39, Pallas kernels, call(): pl.pallas_call(body, in_specs=specs, out_specs=[VMEM] * len(shapes), out_...  23.7 us
    ppermute x12, starting transfers between devices, send_z(): return lax.ppermute(value, 'cb', pairs)  17.8 us
    ppermute x12, waiting for transfers between devices, send_z(): return lax.ppermute(value, 'cb', pairs)  17.8 us
    ppermute x24, waiting for transfers between devices, send_a(): return lax.ppermute(value, 'ra', [(i, peer(i, s, n_a)) for i in range(n_a)])  14.2 us
    ppermute x4, waiting for transfers between devices, send_core(): return lax.ppermute(value, 'cb', [(i, i ^ 1) for i in range(n_c)])  3.32 us
  transfers between devices with their start and end apart: 40, of which 19 were waited for; matrix products, arithmetic and copies ran while one was open for 0% of the time, Pallas kernels for 18%

profile of v7, /device:TPU:0, one launch (start us, length us, event | category | flops | bytes accessed | tf_op | source)
XLA Modules:
  0.0 111.5 jit_solution(5549529325094856413)
XLA Ops:
  0.0 2.2 %shard_map.73 = (bf16[472,256]{1,0:T(8,128)(2,1)S(1)}, bf16[256,1024]{1,0:T(8,128)(2,1)S(1)}, bf16[8,256]{1,0:T(8,128)(2,1)S(1)}) custom-call(s32[1]{0:T(128)} %bitcast.refs_0_.a_ref, bf16[2,1376,1024]{2,1,0:T(8,128)(2,1)} %bitcast.6, bf16[2,1376,1024]{2,1,0:T(8,128)(2,1)} %bitcast.9, bf16[256,1024]{1,0:T(8,128)(2,1)} %refs_4_.3, f32[2,1024]{1,0:T(2,128)} %refs_5_.1, ...), custom_call_target="tpu_custom_call" | custom-call | flops 243269632 | bytes 950272 | tf_op jit(solution)/shard_map/pallas_call | solution.py:29
  2.2 4.0 %collective-permute-start.2 = (bf16[472,256]{1,0:T(8,128)(2,1)S(1)}, bf16[472,256]{1,0:T(8,128)(2,1)S(1)}, u32[]{:S(2)}, u32[]{:S(2)}) collective-permute-start(bf16[472,256]{1,0:T(8,128)(2,1)S(1)} %get-tuple-element.34), channel_id=1, source_target_pairs={{0,24},{8,16},{16,8},{24,0},{1,25},{9,17},{17,9},{25,1},{2,26},{10... | collective-permute-start | bytes 725000 | tf_op jit(solution)/shard_map/ppermute | solution.py:82
  6.2 2.7 %shard_map.74 = (bf16[472,256]{1,0:T(8,128)(2,1)S(1)}, bf16[1376,1024]{1,0:T(8,128)(2,1)S(1)}, bf16[1376,1024]{1,0:T(8,128)(2,1)S(1)}, f32[344,16]{1,0:T(8,128)S(1)}) custom-call(s32[1]{0:T(128)} %bitcast.refs_0_.a_ref, bf16[2,1376,1024]{2,1,0:T(8,128)(2,1)} %bitcast.7, bf16[2,1376,1024]{2,1,0:T(8,128)(2,1)} %bitcast.10, ...), custom_call_target="tpu_custom_call" | custom-call | flops 243269632 | bytes 950272 | tf_op jit(solution)/shard_map/pallas_call | solution.py:29
  10.5 2.0 %collective-permute-start.3 = (bf16[224,256]{1,0:T(8,128)(2,1)S(1)}, bf16[224,256]{1,0:T(8,128)(2,1)S(1)}, u32[]{:S(2)}, u32[]{:S(2)}) collective-permute-start(bf16[224,256]{1,0:T(8,128)(2,1)S(1)} %shard_map.80), channel_id=1, source_target_pairs={{0,8},{8,0},{16,24},{24,16},{1,9},{9,1},{17,25},{25,17},{2,10},{10... | collective-permute-start | bytes 344072 | tf_op jit(solution)/shard_map/ppermute | solution.py:82
  13.0 1.6 %collective-permute-start.4 = (bf16[224,256]{1,0:T(8,128)(2,1)S(1)}, bf16[224,256]{1,0:T(8,128)(2,1)S(1)}, u32[]{:S(2)}, u32[]{:S(2)}) collective-permute-start(bf16[224,256]{1,0:T(8,128)(2,1)S(1)} %shard_map.81), channel_id=1, source_target_pairs={{0,16},{8,24},{16,0},{24,8},{1,17},{9,25},{17,1},{25,9},{2,18},{10... | collective-permute-start | bytes 344072 | tf_op jit(solution)/shard_map/ppermute | solution.py:82
  16.3 1.9 %collective-permute-done.refs_1_ = bf16[472,256]{1,0:T(8,128)(2,1)S(1)} collective-permute-done((bf16[472,256]{1,0:T(8,128)(2,1)S(1)}, bf16[472,256]{1,0:T(8,128)(2,1)S(1)}, u32[]{:S(2)}, u32[]{:S(2)}) %collective-permute-start) | collective-permute-done | bytes 241696 | tf_op jit(solution)/shard_map/ppermute | solution.py:82
  19.2 2.0 %collective-permute-start.8 = (bf16[232,256]{1,0:T(8,128)(2,1)S(1)}, bf16[232,256]{1,0:T(8,128)(2,1)S(1)}, u32[]{:S(2)}, u32[]{:S(2)}) collective-permute-start(bf16[232,256]{1,0:T(8,128)(2,1)S(1)} %get-tuple-element.36.refs_0_), channel_id=1, source_target_pairs={{0,24},{8,16},{16,8},{24,0},{1,25},{9,17},{17,9},{25,1},{2,26},{10... | collective-permute-start | bytes 356360 | tf_op jit(solution)/shard_map/ppermute | solution.py:82
  24.0 2.6 %collective-permute-start.10 = (bf16[112,256]{1,0:T(8,128)(2,1)S(1)}, bf16[112,256]{1,0:T(8,128)(2,1)S(1)}, u32[]{:S(2)}, u32[]{:S(2)}) collective-permute-start(bf16[112,256]{1,0:T(8,128)(2,1)S(1)} %shard_map.83.refs_1_), channel_id=1, source_target_pairs={{0,8},{8,0},{16,24},{24,16},{1,9},{9,1},{17,25},{25,17},{2,10},{10... | collective-permute-start | bytes 172040 | tf_op jit(solution)/shard_map/ppermute | solution.py:82
  27.2 1.8 %shard_map.76.weight_ref = bf16[1376,1024]{1,0:T(8,128)(2,1)S(1)} custom-call(bf16[2,1376,1024]{2,1,0:T(8,128)(2,1)} %refs_0_.3, bf16[224,256]{1,0:T(8,128)(2,1)S(1)} %shard_map.75.refs_1_.refs_0_), custom_call_target="tpu_custom_call" | custom-call | flops 240473424 | bytes 2818048 | tf_op jit(solution)/shard_map/pallas_call | solution.py:29
  35.2 1.8 %collective-permute-start.13 = (bf16[32,1024]{1,0:T(8,128)(2,1)S(1)}, bf16[32,1024]{1,0:T(8,128)(2,1)S(1)}, u32[]{:S(2)}, u32[]{:S(2)}) collective-permute-start(bf16[32,1024]{1,0:T(8,128)(2,1)S(1)} %get-tuple-element.41), channel_id=1, source_target_pairs={{0,2},{1,3},{2,0},{3,1},{4,6},{5,7},{6,4},{7,5},{8,10},{9,11},{10,... | collective-permute-start | bytes 196616 | tf_op jit(solution)/shard_map/ppermute | solution.py:86
  37.0 2.6 %collective-permute-start.14 = (bf16[32,1024]{1,0:T(8,128)(2,1)S(1)}, bf16[32,1024]{1,0:T(8,128)(2,1)S(1)}, u32[]{:S(2)}, u32[]{:S(2)}) collective-permute-start(bf16[32,1024]{1,0:T(8,128)(2,1)S(1)} %get-tuple-element.42), channel_id=1, source_target_pairs={{0,4},{1,5},{2,6},{3,7},{4,0},{5,1},{6,2},{7,3},{8,12},{9,13},{10,... | collective-permute-start | bytes 196616 | tf_op jit(solution)/shard_map/ppermute | solution.py:86
  39.6 4.9 %collective-permute-done.14.refs_1_ = bf16[32,1024]{1,0:T(8,128)(2,1)S(1)} collective-permute-done((bf16[32,1024]{1,0:T(8,128)(2,1)S(1)}, bf16[32,1024]{1,0:T(8,128)(2,1)S(1)}, u32[]{:S(2)}, u32[]{:S(2)}) %collective-permute-start.14) | collective-permute-done | bytes 65568 | tf_op jit(solution)/shard_map/ppermute | solution.py:86
  45.8 2.0 %collective-permute-start.18 = (bf16[32,1024]{1,0:T(8,128)(2,1)S(1)}, bf16[32,1024]{1,0:T(8,128)(2,1)S(1)}, u32[]{:S(2)}, u32[]{:S(2)}) collective-permute-start(bf16[32,1024]{1,0:T(8,128)(2,1)S(1)} %shard_map.91.refs_0_.refs_4_), channel_id=1, source_target_pairs={{0,6},{1,7},{2,4},{3,5},{4,2},{5,3},{6,0},{7,1},{8,14},{9,15},{10,... | collective-permute-start | bytes 196616 | tf_op jit(solution)/shard_map/ppermute | solution.py:86
  48.1 2.1 %collective-permute-start.16 = (bf16[32,1024]{1,0:T(8,128)(2,1)S(1)}, bf16[32,1024]{1,0:T(8,128)(2,1)S(1)}, u32[]{:S(2)}, u32[]{:S(2)}) collective-permute-start(bf16[32,1024]{1,0:T(8,128)(2,1)S(1)} %shard_map.91.refs_0_.refs_4_), channel_id=1, source_target_pairs={{0,2},{1,3},{2,0},{3,1},{4,6},{5,7},{6,4},{7,5},{8,10},{9,11},{10,... | collective-permute-start | bytes 196616 | tf_op jit(solution)/shard_map/ppermute | solution.py:86
  50.2 1.8 %collective-permute-done.18.refs_3_ = bf16[32,1024]{1,0:T(8,128)(2,1)S(1)} collective-permute-done((bf16[32,1024]{1,0:T(8,128)(2,1)S(1)}, bf16[32,1024]{1,0:T(8,128)(2,1)S(1)}, u32[]{:S(2)}, u32[]{:S(2)}) %collective-permute-start.18) | collective-permute-done | bytes 65568 | tf_op jit(solution)/shard_map/ppermute | solution.py:86
  52.0 1.5 %collective-permute-done.17.refs_2_ = bf16[32,1024]{1,0:T(8,128)(2,1)S(1)} collective-permute-done((bf16[32,1024]{1,0:T(8,128)(2,1)S(1)}, bf16[32,1024]{1,0:T(8,128)(2,1)S(1)}, u32[]{:S(2)}, u32[]{:S(2)}) %collective-permute-start.17) | collective-permute-done | bytes 65568 | tf_op jit(solution)/shard_map/ppermute | solution.py:86
  53.7 2.7 %shard_map.90 = (bf16[1376,1024]{1,0:T(8,128)(2,1)S(1)}, bf16[1376,1024]{1,0:T(8,128)(2,1)S(1)}) custom-call(bf16[2,1376,1024]{2,1,0:T(8,128)(2,1)} %bitcast.8, bf16[2,1376,1024]{2,1,0:T(8,128)(2,1)} %bitcast.11, f32[32,1024]{1,0:T(8,128)S(1)} %get-tuple-element.38.refs_2_.own_ref), custom_call_target="tpu_custom_call" | custom-call | flops 480946848 | bytes 5636096 | tf_op jit(solution)/shard_map/pallas_call | solution.py:29
  57.5 2.0 %collective-permute-start.20 = (bf16[472,256]{1,0:T(8,128)(2,1)S(1)}, bf16[472,256]{1,0:T(8,128)(2,1)S(1)}, u32[]{:S(2)}, u32[]{:S(2)}) collective-permute-start(bf16[472,256]{1,0:T(8,128)(2,1)S(1)} %shard_map.97), channel_id=1, source_target_pairs={{0,8},{8,0},{16,24},{24,16},{1,9},{9,1},{17,25},{25,17},{2,10},{10... | collective-permute-start | bytes 725000 | tf_op jit(solution)/shard_map/ppermute | solution.py:82
  62.0 2.0 %collective-permute-start.23 = (bf16[224,256]{1,0:T(8,128)(2,1)S(1)}, bf16[224,256]{1,0:T(8,128)(2,1)S(1)}, u32[]{:S(2)}, u32[]{:S(2)}) collective-permute-start(bf16[224,256]{1,0:T(8,128)(2,1)S(1)} %shard_map.100), channel_id=1, source_target_pairs={{0,8},{8,0},{16,24},{24,16},{1,9},{9,1},{17,25},{25,17},{2,10},{10... | collective-permute-start | bytes 344072 | tf_op jit(solution)/shard_map/ppermute | solution.py:82
  66.3 2.1 %collective-permute-start.25 = (bf16[224,256]{1,0:T(8,128)(2,1)S(1)}, bf16[224,256]{1,0:T(8,128)(2,1)S(1)}, u32[]{:S(2)}, u32[]{:S(2)}) collective-permute-start(bf16[224,256]{1,0:T(8,128)(2,1)S(1)} %shard_map.102), channel_id=1, source_target_pairs={{0,24},{8,16},{16,8},{24,0},{1,25},{9,17},{17,9},{25,1},{2,26},{10... | collective-permute-start | bytes 344072 | tf_op jit(solution)/shard_map/ppermute | solution.py:82
  68.9 5.3 %collective-permute-done.21.refs_2_ = bf16[472,256]{1,0:T(8,128)(2,1)S(1)} collective-permute-done((bf16[472,256]{1,0:T(8,128)(2,1)S(1)}, bf16[472,256]{1,0:T(8,128)(2,1)S(1)}, u32[]{:S(2)}, u32[]{:S(2)}) %collective-permute-start.21) | collective-permute-done | bytes 241696 | tf_op jit(solution)/shard_map/ppermute | solution.py:82
  76.1 2.2 %collective-permute-start.26 = (bf16[232,256]{1,0:T(8,128)(2,1)S(1)}, bf16[232,256]{1,0:T(8,128)(2,1)S(1)}, u32[]{:S(2)}, u32[]{:S(2)}) collective-permute-start(bf16[232,256]{1,0:T(8,128)(2,1)S(1)} %get-tuple-element.47.refs_0_), channel_id=1, source_target_pairs={{0,8},{8,0},{16,24},{24,16},{1,9},{9,1},{17,25},{25,17},{2,10},{10... | collective-permute-start | bytes 356360 | tf_op jit(solution)/shard_map/ppermute | solution.py:82
  78.8 2.6 %collective-permute-done.24.refs_2_ = bf16[224,256]{1,0:T(8,128)(2,1)S(1)} collective-permute-done((bf16[224,256]{1,0:T(8,128)(2,1)S(1)}, bf16[224,256]{1,0:T(8,128)(2,1)S(1)}, u32[]{:S(2)}, u32[]{:S(2)}) %collective-permute-start.24) | collective-permute-done | bytes 114720 | tf_op jit(solution)/shard_map/ppermute | solution.py:82
  81.8 2.2 %collective-permute-start.29 = (bf16[112,256]{1,0:T(8,128)(2,1)S(1)}, bf16[112,256]{1,0:T(8,128)(2,1)S(1)}, u32[]{:S(2)}, u32[]{:S(2)}) collective-permute-start(bf16[112,256]{1,0:T(8,128)(2,1)S(1)} %shard_map.103.refs_1_), channel_id=1, source_target_pairs={{0,24},{8,16},{16,8},{24,0},{1,25},{9,17},{17,9},{25,1},{2,26},{10... | collective-permute-start | bytes 172040 | tf_op jit(solution)/shard_map/ppermute | solution.py:82
  84.0 1.8 %shard_map.95.weight_ref = bf16[1376,1024]{1,0:T(8,128)(2,1)S(1)} custom-call(bf16[2,1376,1024]{2,1,0:T(8,128)(2,1)} %refs_0_.3, bf16[224,256]{1,0:T(8,128)(2,1)S(1)} %shard_map.94.refs_1_.refs_0_), custom_call_target="tpu_custom_call" | custom-call | flops 240473424 | bytes 2818048 | tf_op jit(solution)/shard_map/pallas_call | solution.py:29
  92.9 1.6 %collective-permute-start.34 = (bf16[32,1024]{1,0:T(8,128)(2,1)S(1)}, bf16[32,1024]{1,0:T(8,128)(2,1)S(1)}, u32[]{:S(2)}, u32[]{:S(2)}) collective-permute-start(bf16[32,1024]{1,0:T(8,128)(2,1)S(1)} %get-tuple-element.51), channel_id=1, source_target_pairs={{0,4},{1,5},{2,6},{3,7},{4,0},{5,1},{6,2},{7,3},{8,12},{9,13},{10,... | collective-permute-start | bytes 196616 | tf_op jit(solution)/shard_map/ppermute | solution.py:86
  94.5 1.9 %collective-permute-start.35 = (bf16[32,1024]{1,0:T(8,128)(2,1)S(1)}, bf16[32,1024]{1,0:T(8,128)(2,1)S(1)}, u32[]{:S(2)}, u32[]{:S(2)}) collective-permute-start(bf16[32,1024]{1,0:T(8,128)(2,1)S(1)} %get-tuple-element.52), channel_id=1, source_target_pairs={{0,6},{1,7},{2,4},{3,5},{4,2},{5,3},{6,0},{7,1},{8,14},{9,15},{10,... | collective-permute-start | bytes 196616 | tf_op jit(solution)/shard_map/ppermute | solution.py:86
  96.4 4.8 %collective-permute-done.34.refs_1_ = bf16[32,1024]{1,0:T(8,128)(2,1)S(1)} collective-permute-done((bf16[32,1024]{1,0:T(8,128)(2,1)S(1)}, bf16[32,1024]{1,0:T(8,128)(2,1)S(1)}, u32[]{:S(2)}, u32[]{:S(2)}) %collective-permute-start.34) | collective-permute-done | bytes 65568 | tf_op jit(solution)/shard_map/ppermute | solution.py:86
  101.2 2.1 %collective-permute-start.38 = (bf16[32,1024]{1,0:T(8,128)(2,1)S(1)}, bf16[32,1024]{1,0:T(8,128)(2,1)S(1)}, u32[]{:S(2)}, u32[]{:S(2)}) collective-permute-start(bf16[32,1024]{1,0:T(8,128)(2,1)S(1)} %shard_map.110.refs_0_), channel_id=1, source_target_pairs={{0,6},{1,7},{2,4},{3,5},{4,2},{5,3},{6,0},{7,1},{8,14},{9,15},{10,... | collective-permute-start | bytes 196616 | tf_op jit(solution)/shard_map/ppermute | solution.py:86
  104.0 1.7 %collective-permute-start.36 = (bf16[32,1024]{1,0:T(8,128)(2,1)S(1)}, bf16[32,1024]{1,0:T(8,128)(2,1)S(1)}, u32[]{:S(2)}, u32[]{:S(2)}) collective-permute-start(bf16[32,1024]{1,0:T(8,128)(2,1)S(1)} %shard_map.110.refs_0_), channel_id=1, source_target_pairs={{0,2},{1,3},{2,0},{3,1},{4,6},{5,7},{6,4},{7,5},{8,10},{9,11},{10,... | collective-permute-start | bytes 196616 | tf_op jit(solution)/shard_map/ppermute | solution.py:86
  105.7 1.9 %collective-permute-done.38.refs_3_ = bf16[32,1024]{1,0:T(8,128)(2,1)S(1)} collective-permute-done((bf16[32,1024]{1,0:T(8,128)(2,1)S(1)}, bf16[32,1024]{1,0:T(8,128)(2,1)S(1)}, u32[]{:S(2)}, u32[]{:S(2)}) %collective-permute-start.38) | collective-permute-done | bytes 65568 | tf_op jit(solution)/shard_map/ppermute | solution.py:86
  107.6 1.7 %collective-permute-done.37.refs_2_ = bf16[32,1024]{1,0:T(8,128)(2,1)S(1)} collective-permute-done((bf16[32,1024]{1,0:T(8,128)(2,1)S(1)}, bf16[32,1024]{1,0:T(8,128)(2,1)S(1)}, u32[]{:S(2)}, u32[]{:S(2)}) %collective-permute-start.37) | collective-permute-done | bytes 65568 | tf_op jit(solution)/shard_map/ppermute | solution.py:86
  (93 shorter events, 35.0 us)
Async XLA Ops:
  2.2 12.8 %collective-permute-start.2 = (bf16[472,256]{1,0:T(8,128)(2,1)S(1)}, bf16[472,256]{1,0:T(8,128)(2,1)S(1)}, u32[]{:S(2)}, u32[]{:S(2)}) collective-permute-start(bf16[472,256]{1,0:T(8,128)(2,1)S(1)} %get-tuple-element.34), channel_id=1, source_target_pairs={{0,24},{8,16},{16,8},{24,0},{1,25},{9,17},{17,9},{25,1},{2,26},{10... | collective-permute-start | bytes 725000 | tf_op jit(solution)/shard_map/ppermute | solution.py:82
  9.4 8.8 %collective-permute-start = (bf16[472,256]{1,0:T(8,128)(2,1)S(1)}, bf16[472,256]{1,0:T(8,128)(2,1)S(1)}, u32[]{:S(2)}, u32[]{:S(2)}) collective-permute-start(bf16[472,256]{1,0:T(8,128)(2,1)S(1)} %shard_map.78), channel_id=1, source_target_pairs={{0,8},{8,0},{16,24},{24,16},{1,9},{9,1},{17,25},{25,17},{2,10},{10... | collective-permute-start | bytes 725000 | tf_op jit(solution)/shard_map/ppermute | solution.py:82
  10.0 8.6 %collective-permute-start.1 = (bf16[472,256]{1,0:T(8,128)(2,1)S(1)}, bf16[472,256]{1,0:T(8,128)(2,1)S(1)}, u32[]{:S(2)}, u32[]{:S(2)}) collective-permute-start(bf16[472,256]{1,0:T(8,128)(2,1)S(1)} %get-tuple-element.33), channel_id=1, source_target_pairs={{0,16},{8,24},{16,0},{24,8},{1,17},{9,25},{17,1},{25,9},{2,18},{10... | collective-permute-start | bytes 725000 | tf_op jit(solution)/shard_map/ppermute | solution.py:82
  10.5 11.8 %collective-permute-start.3 = (bf16[224,256]{1,0:T(8,128)(2,1)S(1)}, bf16[224,256]{1,0:T(8,128)(2,1)S(1)}, u32[]{:S(2)}, u32[]{:S(2)}) collective-permute-start(bf16[224,256]{1,0:T(8,128)(2,1)S(1)} %shard_map.80), channel_id=1, source_target_pairs={{0,8},{8,0},{16,24},{24,16},{1,9},{9,1},{17,25},{25,17},{2,10},{10... | collective-permute-start | bytes 344072 | tf_op jit(solution)/shard_map/ppermute | solution.py:82
  13.0 10.7 %collective-permute-start.4 = (bf16[224,256]{1,0:T(8,128)(2,1)S(1)}, bf16[224,256]{1,0:T(8,128)(2,1)S(1)}, u32[]{:S(2)}, u32[]{:S(2)}) collective-permute-start(bf16[224,256]{1,0:T(8,128)(2,1)S(1)} %shard_map.81), channel_id=1, source_target_pairs={{0,16},{8,24},{16,0},{24,8},{1,17},{9,25},{17,1},{25,9},{2,18},{10... | collective-permute-start | bytes 344072 | tf_op jit(solution)/shard_map/ppermute | solution.py:82
  15.0 8.6 %collective-permute-start.5 = (bf16[224,256]{1,0:T(8,128)(2,1)S(1)}, bf16[224,256]{1,0:T(8,128)(2,1)S(1)}, u32[]{:S(2)}, u32[]{:S(2)}) collective-permute-start(bf16[224,256]{1,0:T(8,128)(2,1)S(1)} %shard_map.82), channel_id=1, source_target_pairs={{0,24},{8,16},{16,8},{24,0},{1,25},{9,17},{17,9},{25,1},{2,26},{10... | collective-permute-start | bytes 344072 | tf_op jit(solution)/shard_map/ppermute | solution.py:82
  19.2 9.8 %collective-permute-start.8 = (bf16[232,256]{1,0:T(8,128)(2,1)S(1)}, bf16[232,256]{1,0:T(8,128)(2,1)S(1)}, u32[]{:S(2)}, u32[]{:S(2)}) collective-permute-start(bf16[232,256]{1,0:T(8,128)(2,1)S(1)} %get-tuple-element.36.refs_0_), channel_id=1, source_target_pairs={{0,24},{8,16},{16,8},{24,0},{1,25},{9,17},{17,9},{25,1},{2,26},{10... | collective-permute-start | bytes 356360 | tf_op jit(solution)/shard_map/ppermute | solution.py:82
  21.2 9.2 %collective-permute-start.7 = (bf16[232,256]{1,0:T(8,128)(2,1)S(1)}, bf16[232,256]{1,0:T(8,128)(2,1)S(1)}, u32[]{:S(2)}, u32[]{:S(2)}) collective-permute-start(bf16[232,256]{1,0:T(8,128)(2,1)S(1)} %get-tuple-element.36.refs_0_), channel_id=1, source_target_pairs={{0,16},{8,24},{16,0},{24,8},{1,17},{9,25},{17,1},{25,9},{2,18},{10... | collective-permute-start | bytes 356360 | tf_op jit(solution)/shard_map/ppermute | solution.py:82
  22.3 8.1 %collective-permute-start.6 = (bf16[232,256]{1,0:T(8,128)(2,1)S(1)}, bf16[232,256]{1,0:T(8,128)(2,1)S(1)}, u32[]{:S(2)}, u32[]{:S(2)}) collective-permute-start(bf16[232,256]{1,0:T(8,128)(2,1)S(1)} %get-tuple-element.36.refs_0_), channel_id=1, source_target_pairs={{0,8},{8,0},{16,24},{24,16},{1,9},{9,1},{17,25},{25,17},{2,10},{10... | collective-permute-start | bytes 356360 | tf_op jit(solution)/shard_map/ppermute | solution.py:82
  24.0 7.1 %collective-permute-start.10 = (bf16[112,256]{1,0:T(8,128)(2,1)S(1)}, bf16[112,256]{1,0:T(8,128)(2,1)S(1)}, u32[]{:S(2)}, u32[]{:S(2)}) collective-permute-start(bf16[112,256]{1,0:T(8,128)(2,1)S(1)} %shard_map.83.refs_1_), channel_id=1, source_target_pairs={{0,8},{8,0},{16,24},{24,16},{1,9},{9,1},{17,25},{25,17},{2,10},{10... | collective-permute-start | bytes 172040 | tf_op jit(solution)/shard_map/ppermute | solution.py:82
  26.6 5.1 %collective-permute-start.9 = (bf16[112,256]{1,0:T(8,128)(2,1)S(1)}, bf16[112,256]{1,0:T(8,128)(2,1)S(1)}, u32[]{:S(2)}, u32[]{:S(2)}) collective-permute-start(bf16[112,256]{1,0:T(8,128)(2,1)S(1)} %shard_map.83.refs_1_), channel_id=1, source_target_pairs={{0,24},{8,16},{16,8},{24,0},{1,25},{9,17},{17,9},{25,1},{2,26},{10... | collective-permute-start | bytes 172040 | tf_op jit(solution)/shard_map/ppermute | solution.py:82
  37.0 7.5 %collective-permute-start.14 = (bf16[32,1024]{1,0:T(8,128)(2,1)S(1)}, bf16[32,1024]{1,0:T(8,128)(2,1)S(1)}, u32[]{:S(2)}, u32[]{:S(2)}) collective-permute-start(bf16[32,1024]{1,0:T(8,128)(2,1)S(1)} %get-tuple-element.42), channel_id=1, source_target_pairs={{0,4},{1,5},{2,6},{3,7},{4,0},{5,1},{6,2},{7,3},{8,12},{9,13},{10,... | collective-permute-start | bytes 196616 | tf_op jit(solution)/shard_map/ppermute | solution.py:86
  39.6 6.2 %collective-permute-start.15 = (bf16[32,1024]{1,0:T(8,128)(2,1)S(1)}, bf16[32,1024]{1,0:T(8,128)(2,1)S(1)}, u32[]{:S(2)}, u32[]{:S(2)}) collective-permute-start(bf16[32,1024]{1,0:T(8,128)(2,1)S(1)} %get-tuple-element.43), channel_id=1, source_target_pairs={{0,6},{1,7},{2,4},{3,5},{4,2},{5,3},{6,0},{7,1},{8,14},{9,15},{10,... | collective-permute-start | bytes 196616 | tf_op jit(solution)/shard_map/ppermute | solution.py:86
  45.8 6.3 %collective-permute-start.18 = (bf16[32,1024]{1,0:T(8,128)(2,1)S(1)}, bf16[32,1024]{1,0:T(8,128)(2,1)S(1)}, u32[]{:S(2)}, u32[]{:S(2)}) collective-permute-start(bf16[32,1024]{1,0:T(8,128)(2,1)S(1)} %shard_map.91.refs_0_.refs_4_), channel_id=1, source_target_pairs={{0,6},{1,7},{2,4},{3,5},{4,2},{5,3},{6,0},{7,1},{8,14},{9,15},{10,... | collective-permute-start | bytes 196616 | tf_op jit(solution)/shard_map/ppermute | solution.py:86
  47.8 5.8 %collective-permute-start.17 = (bf16[32,1024]{1,0:T(8,128)(2,1)S(1)}, bf16[32,1024]{1,0:T(8,128)(2,1)S(1)}, u32[]{:S(2)}, u32[]{:S(2)}) collective-permute-start(bf16[32,1024]{1,0:T(8,128)(2,1)S(1)} %shard_map.91.refs_0_.refs_4_), channel_id=1, source_target_pairs={{0,4},{1,5},{2,6},{3,7},{4,0},{5,1},{6,2},{7,3},{8,12},{9,13},{10,... | collective-permute-start | bytes 196616 | tf_op jit(solution)/shard_map/ppermute | solution.py:86
  48.1 5.5 %collective-permute-start.16 = (bf16[32,1024]{1,0:T(8,128)(2,1)S(1)}, bf16[32,1024]{1,0:T(8,128)(2,1)S(1)}, u32[]{:S(2)}, u32[]{:S(2)}) collective-permute-start(bf16[32,1024]{1,0:T(8,128)(2,1)S(1)} %shard_map.91.refs_0_.refs_4_), channel_id=1, source_target_pairs={{0,2},{1,3},{2,0},{3,1},{4,6},{5,7},{6,4},{7,5},{8,10},{9,11},{10,... | collective-permute-start | bytes 196616 | tf_op jit(solution)/shard_map/ppermute | solution.py:86
  57.5 8.8 %collective-permute-start.20 = (bf16[472,256]{1,0:T(8,128)(2,1)S(1)}, bf16[472,256]{1,0:T(8,128)(2,1)S(1)}, u32[]{:S(2)}, u32[]{:S(2)}) collective-permute-start(bf16[472,256]{1,0:T(8,128)(2,1)S(1)} %shard_map.97), channel_id=1, source_target_pairs={{0,8},{8,0},{16,24},{24,16},{1,9},{9,1},{17,25},{25,17},{2,10},{10... | collective-permute-start | bytes 725000 | tf_op jit(solution)/shard_map/ppermute | solution.py:82
  59.9 14.3 %collective-permute-start.21 = (bf16[472,256]{1,0:T(8,128)(2,1)S(1)}, bf16[472,256]{1,0:T(8,128)(2,1)S(1)}, u32[]{:S(2)}, u32[]{:S(2)}) collective-permute-start(bf16[472,256]{1,0:T(8,128)(2,1)S(1)} %shard_map.98), channel_id=1, source_target_pairs={{0,16},{8,24},{16,0},{24,8},{1,17},{9,25},{17,1},{25,9},{2,18},{10... | collective-permute-start | bytes 725000 | tf_op jit(solution)/shard_map/ppermute | solution.py:82
  60.7 13.4 %collective-permute-start.22 = (bf16[472,256]{1,0:T(8,128)(2,1)S(1)}, bf16[472,256]{1,0:T(8,128)(2,1)S(1)}, u32[]{:S(2)}, u32[]{:S(2)}) collective-permute-start(bf16[472,256]{1,0:T(8,128)(2,1)S(1)} %get-tuple-element.46), channel_id=1, source_target_pairs={{0,24},{8,16},{16,8},{24,0},{1,25},{9,17},{17,9},{25,1},{2,26},{10... | collective-permute-start | bytes 725000 | tf_op jit(solution)/shard_map/ppermute | solution.py:82
  62.0 14.1 %collective-permute-start.23 = (bf16[224,256]{1,0:T(8,128)(2,1)S(1)}, bf16[224,256]{1,0:T(8,128)(2,1)S(1)}, u32[]{:S(2)}, u32[]{:S(2)}) collective-permute-start(bf16[224,256]{1,0:T(8,128)(2,1)S(1)} %shard_map.100), channel_id=1, source_target_pairs={{0,8},{8,0},{16,24},{24,16},{1,9},{9,1},{17,25},{25,17},{2,10},{10... | collective-permute-start | bytes 344072 | tf_op jit(solution)/shard_map/ppermute | solution.py:82
  64.5 16.9 %collective-permute-start.24 = (bf16[224,256]{1,0:T(8,128)(2,1)S(1)}, bf16[224,256]{1,0:T(8,128)(2,1)S(1)}, u32[]{:S(2)}, u32[]{:S(2)}) collective-permute-start(bf16[224,256]{1,0:T(8,128)(2,1)S(1)} %shard_map.101), channel_id=1, source_target_pairs={{0,16},{8,24},{16,0},{24,8},{1,17},{9,25},{17,1},{25,9},{2,18},{10... | collective-permute-start | bytes 344072 | tf_op jit(solution)/shard_map/ppermute | solution.py:82
  66.3 15.1 %collective-permute-start.25 = (bf16[224,256]{1,0:T(8,128)(2,1)S(1)}, bf16[224,256]{1,0:T(8,128)(2,1)S(1)}, u32[]{:S(2)}, u32[]{:S(2)}) collective-permute-start(bf16[224,256]{1,0:T(8,128)(2,1)S(1)} %shard_map.102), channel_id=1, source_target_pairs={{0,24},{8,16},{16,8},{24,0},{1,25},{9,17},{17,9},{25,1},{2,26},{10... | collective-permute-start | bytes 344072 | tf_op jit(solution)/shard_map/ppermute | solution.py:82
  74.8 11.0 %collective-permute-start.28 = (bf16[232,256]{1,0:T(8,128)(2,1)S(1)}, bf16[232,256]{1,0:T(8,128)(2,1)S(1)}, u32[]{:S(2)}, u32[]{:S(2)}) collective-permute-start(bf16[232,256]{1,0:T(8,128)(2,1)S(1)} %get-tuple-element.47.refs_0_), channel_id=1, source_target_pairs={{0,24},{8,16},{16,8},{24,0},{1,25},{9,17},{17,9},{25,1},{2,26},{10... | collective-permute-start | bytes 356360 | tf_op jit(solution)/shard_map/ppermute | solution.py:82
  75.0 12.6 %collective-permute-start.27 = (bf16[232,256]{1,0:T(8,128)(2,1)S(1)}, bf16[232,256]{1,0:T(8,128)(2,1)S(1)}, u32[]{:S(2)}, u32[]{:S(2)}) collective-permute-start(bf16[232,256]{1,0:T(8,128)(2,1)S(1)} %get-tuple-element.47.refs_0_), channel_id=1, source_target_pairs={{0,16},{8,24},{16,0},{24,8},{1,17},{9,25},{17,1},{25,9},{2,18},{10... | collective-permute-start | bytes 356360 | tf_op jit(solution)/shard_map/ppermute | solution.py:82
  76.1 11.5 %collective-permute-start.26 = (bf16[232,256]{1,0:T(8,128)(2,1)S(1)}, bf16[232,256]{1,0:T(8,128)(2,1)S(1)}, u32[]{:S(2)}, u32[]{:S(2)}) collective-permute-start(bf16[232,256]{1,0:T(8,128)(2,1)S(1)} %get-tuple-element.47.refs_0_), channel_id=1, source_target_pairs={{0,8},{8,0},{16,24},{24,16},{1,9},{9,1},{17,25},{25,17},{2,10},{10... | collective-permute-start | bytes 356360 | tf_op jit(solution)/shard_map/ppermute | solution.py:82
  81.7 6.5 %collective-permute-start.30 = (bf16[112,256]{1,0:T(8,128)(2,1)S(1)}, bf16[112,256]{1,0:T(8,128)(2,1)S(1)}, u32[]{:S(2)}, u32[]{:S(2)}) collective-permute-start(bf16[112,256]{1,0:T(8,128)(2,1)S(1)} %shard_map.103.refs_1_), channel_id=1, source_target_pairs={{0,8},{8,0},{16,24},{24,16},{1,9},{9,1},{17,25},{25,17},{2,10},{10... | collective-permute-start | bytes 172040 | tf_op jit(solution)/shard_map/ppermute | solution.py:82
  81.8 6.5 %collective-permute-start.29 = (bf16[112,256]{1,0:T(8,128)(2,1)S(1)}, bf16[112,256]{1,0:T(8,128)(2,1)S(1)}, u32[]{:S(2)}, u32[]{:S(2)}) collective-permute-start(bf16[112,256]{1,0:T(8,128)(2,1)S(1)} %shard_map.103.refs_1_), channel_id=1, source_target_pairs={{0,24},{8,16},{16,8},{24,0},{1,25},{9,17},{17,9},{25,1},{2,26},{10... | collective-permute-start | bytes 172040 | tf_op jit(solution)/shard_map/ppermute | solution.py:82
  92.9 8.3 %collective-permute-start.34 = (bf16[32,1024]{1,0:T(8,128)(2,1)S(1)}, bf16[32,1024]{1,0:T(8,128)(2,1)S(1)}, u32[]{:S(2)}, u32[]{:S(2)}) collective-permute-start(bf16[32,1024]{1,0:T(8,128)(2,1)S(1)} %get-tuple-element.51), channel_id=1, source_target_pairs={{0,4},{1,5},{2,6},{3,7},{4,0},{5,1},{6,2},{7,3},{8,12},{9,13},{10,... | collective-permute-start | bytes 196616 | tf_op jit(solution)/shard_map/ppermute | solution.py:86
  94.5 6.7 %collective-permute-start.35 = (bf16[32,1024]{1,0:T(8,128)(2,1)S(1)}, bf16[32,1024]{1,0:T(8,128)(2,1)S(1)}, u32[]{:S(2)}, u32[]{:S(2)}) collective-permute-start(bf16[32,1024]{1,0:T(8,128)(2,1)S(1)} %get-tuple-element.52), channel_id=1, source_target_pairs={{0,6},{1,7},{2,4},{3,5},{4,2},{5,3},{6,0},{7,1},{8,14},{9,15},{10,... | collective-permute-start | bytes 196616 | tf_op jit(solution)/shard_map/ppermute | solution.py:86
  101.2 6.3 %collective-permute-start.38 = (bf16[32,1024]{1,0:T(8,128)(2,1)S(1)}, bf16[32,1024]{1,0:T(8,128)(2,1)S(1)}, u32[]{:S(2)}, u32[]{:S(2)}) collective-permute-start(bf16[32,1024]{1,0:T(8,128)(2,1)S(1)} %shard_map.110.refs_0_), channel_id=1, source_target_pairs={{0,6},{1,7},{2,4},{3,5},{4,2},{5,3},{6,0},{7,1},{8,14},{9,15},{10,... | collective-permute-start | bytes 196616 | tf_op jit(solution)/shard_map/ppermute | solution.py:86
  103.3 5.9 %collective-permute-start.37 = (bf16[32,1024]{1,0:T(8,128)(2,1)S(1)}, bf16[32,1024]{1,0:T(8,128)(2,1)S(1)}, u32[]{:S(2)}, u32[]{:S(2)}) collective-permute-start(bf16[32,1024]{1,0:T(8,128)(2,1)S(1)} %shard_map.110.refs_0_), channel_id=1, source_target_pairs={{0,4},{1,5},{2,6},{3,7},{4,0},{5,1},{6,2},{7,3},{8,12},{9,13},{10,... | collective-permute-start | bytes 196616 | tf_op jit(solution)/shard_map/ppermute | solution.py:86
  104.0 5.2 %collective-permute-start.36 = (bf16[32,1024]{1,0:T(8,128)(2,1)S(1)}, bf16[32,1024]{1,0:T(8,128)(2,1)S(1)}, u32[]{:S(2)}, u32[]{:S(2)}) collective-permute-start(bf16[32,1024]{1,0:T(8,128)(2,1)S(1)} %shard_map.110.refs_0_), channel_id=1, source_target_pairs={{0,2},{1,3},{2,0},{3,1},{4,6},{5,7},{6,4},{7,5},{8,10},{9,11},{10,... | collective-permute-start | bytes 196616 | tf_op jit(solution)/shard_map/ppermute | solution.py:86
  (10 other events, 40.0 us)
